TPU v7x, 256 devices: a whole 4x4x8 slice. The times are simulated.
256 devices in a mesh: ep: 64 (over z, x, core), tp: 4 (over y).
Axes of the slice: x: 4, y: 4, z: 8, core: 2. Of those that a mesh axis runs over, the one named last changes fastest.
Arguments:
- pool_in: bfloat16 [65536, 1024], P(('ep', 'tp')), may hold values from -6 to 6
- w_pool: bfloat16 [8, 128, 128], replicated, may hold values from -0.5 to 0.5
- pool_scale: float32 [1024], replicated, may hold values from 0.1 to 1.9
- w_out: bfloat16 [1024, 2048], replicated, may hold values from -0.1875 to 0.1875
- expert_in: bfloat16 [32768, 2048], P('ep'), may hold values from -6 to 6
- ffn_gain: float32 [2048], replicated, may hold values from 0.1 to 1.9
- routes: int32 [32768, 2], P('ep'), may hold values from 0 to 63, all different within a row; in each aligned block of 128 rows (0 to 127, 128 to 255, ...) at most 6 rows name the same one
- route_weight: float32 [32768, 2], P('ep'), may hold values from 0.25 to 1
- w_gate: bfloat16 [64, 2048, 1024], P('ep', None, 'tp'), may hold values from -0.125 to 0.125
- w_up: bfloat16 [64, 2048, 1024], P('ep', None, 'tp'), may hold values from -0.125 to 0.125
- w_down: bfloat16 [64, 1024, 2048], P('ep', 'tp'), may hold values from -0.1875 to 0.1875
Outputs:
- mixer_out: bfloat16 [65536, 2048], P(('ep', 'tp'))
- expert_out: bfloat16 [32768, 2048], P(('ep', 'tp'))
Inputs may be any that keep to these rules, and one draw needn't show every extreme that they name: `routes`: each row names 2 different experts. In each aligned block of 128 rows no expert is named by more than 6 rows, and in some block some expert is named by exactly 6 rows.
All inputs are finite; a program needn't handle non-finite values.
Results may differ from a plain program's by a relative error of at most 0.012.
Values may be sent and summed in bfloat16 or wider, within the bound.
No kernel may reach another device: no remote copies, remote signals or barrier semaphores. Data moves between devices by JAX's collectives and lax.ppermute only.
A program may use at most 128 MiB of HBM per device.

v0:
```python
from functools import partial

import jax
import jax.numpy as jnp
from jax import lax
from jax.sharding import PartitionSpec as P

GDIM = 128
WMAX = 16
K = 2


EPS = 0.05


def passed_along(array, axis, by):
    length = lax.axis_size(axis)
    pairs = [(i, i + by) for i in range(length) if 0 <= i + by < length]
    return lax.ppermute(array, axis, pairs)


def rows_first(arrays, axis, dims):
    turned = [jnp.moveaxis(a, dim, 0) for a, dim in zip(arrays, dims)]
    both = jnp.concatenate([t.reshape(len(t), -1) for t in turned], axis=1)
    out, at, gathered = (lax.all_gather(both, axis, axis=0, tiled=True), 0, [])
    for t, dim in zip(turned, dims):
        piece = out[:, at : at + t[0].size].reshape(-1, *t.shape[1:])
        gathered.append(jnp.moveaxis(piece, 0, dim))
        at += t[0].size
    return tuple(gathered)


def window_sizes(width):
    group_of = jnp.arange(width) // GDIM
    level = group_of % 4
    return jnp.where(
        level == 0, 2.0, jnp.where(level == 1, 4.0, jnp.where(level == 2, 8.0, 16.0))
    ).astype(jnp.float32)


def pooled_rows(extended, positions):
    extent = extended.shape[0] - (WMAX - 1)
    window = window_sizes(extended.shape[1])
    running = jnp.zeros((extent, extended.shape[1]), jnp.float32)
    picked = running
    for offset in range(WMAX):
        running = running + extended[WMAX - 1 - offset : WMAX - 1 - offset + extent]
        if offset + 1 in (2, 4, 8, 16):
            picked = jnp.where(window[None, :] == offset + 1, running, picked)
    counted = jnp.minimum(positions[:, None] + 1.0, window[None, :])
    return (picked / counted - extended[WMAX - 1 :]).astype(jnp.bfloat16)


def normalize(features_in, gain):
    features = features_in.astype(jnp.float32)
    inverse = lax.rsqrt(jnp.mean(features * features, axis=-1, keepdims=True) + EPS)
    return (features * inverse * gain).astype(jnp.bfloat16)


def slot_places(expert_ids, experts, capacity):
    onehot = (expert_ids[:, None] == jnp.arange(experts)[None, :]).astype(jnp.int32)
    earlier = jnp.cumsum(onehot, axis=0) - onehot
    slot_rank = jnp.sum(earlier * onehot, axis=1)
    return expert_ids * capacity + slot_rank


def send_block(normed_block, places, experts, capacity):
    pairs = places.shape[0]
    table = (
        jnp.full((experts * capacity,), pairs, jnp.int32)
        .at[places]
        .set(jnp.arange(pairs, dtype=jnp.int32))
    )
    source = jnp.where(table < pairs, table // K, normed_block.shape[0])
    padded = jnp.concatenate(
        [normed_block, jnp.zeros((1, normed_block.shape[1]), normed_block.dtype)], axis=0
    )
    return padded[source].reshape(experts, capacity, normed_block.shape[1])


def on_device(
    pool_in,
    w_pool,
    pool_scale,
    w_out,
    expert_in,
    ffn_gain,
    routes,
    route_weight,
    w_gate,
    w_up,
    w_down,
):
    rows_here = pool_in.shape[0]
    before = passed_along(pool_in[rows_here - (WMAX - 1) :], ("ep", "tp"), 1)
    extended = jnp.concatenate([before, pool_in], axis=0).astype(jnp.float32)
    positions = (lax.axis_index(("ep", "tp")) * rows_here + jnp.arange(rows_here)).astype(
        jnp.float32
    )
    pooled = pooled_rows(extended, positions)
    group_count = w_pool.shape[0]
    grouped = jnp.einsum(
        "tgc,gcd->tgd",
        pooled.reshape(rows_here, group_count, GDIM),
        w_pool,
        preferred_element_type=jnp.float32,
    )
    scaled = (grouped.reshape(rows_here, -1) * pool_scale).astype(jnp.bfloat16)
    mixer_out = jnp.dot(scaled, w_out, preferred_element_type=jnp.float32).astype(jnp.bfloat16)
    parts = lax.axis_size("tp")
    own = lax.axis_index("tp")
    experts = lax.axis_size("ep") * w_gate.shape[0]
    block_rows = routes.shape[0] // parts
    capacity = 3 * block_rows * K // (2 * experts)
    width = expert_in.shape[1]
    route_blocks = routes.reshape(parts, block_rows * K)
    weight_blocks = route_weight.reshape(parts, block_rows * K)
    places = jax.vmap(partial(slot_places, experts=experts, capacity=capacity))(route_blocks)
    gate_local = w_gate[0]
    up_local = w_up[0]
    down_local = w_down[0]
    gate_whole, up_whole, down_whole = rows_first(
        (gate_local, up_local, down_local), "tp", (1, 1, 0)
    )
    mine = lax.dynamic_slice_in_dim(expert_in, own * block_rows, block_rows, 0)
    own_places = lax.dynamic_index_in_dim(places, own, 0, keepdims=False)
    outgoing = send_block(normalize(mine, ffn_gain), own_places, experts, capacity)[None]
    arrived = lax.all_to_all(outgoing, "ep", split_axis=1, concat_axis=1, tiled=True)
    slot_rows = arrived.reshape(-1, width)
    gate_val = jnp.dot(slot_rows, gate_whole, preferred_element_type=jnp.float32)
    up_val = jnp.dot(slot_rows, up_whole, preferred_element_type=jnp.float32)
    hidden = (jax.nn.silu(gate_val) * up_val).astype(jnp.bfloat16)
    quarter = down_local.shape[0]
    total = jnp.zeros((slot_rows.shape[0], width), jnp.float32)
    for block in range(parts):
        partial_val = jnp.dot(
            hidden[:, block * quarter : (block + 1) * quarter],
            down_whole[block * quarter : (block + 1) * quarter],
            preferred_element_type=jnp.float32,
        ).astype(jnp.bfloat16)
        partial_val = lax.optimization_barrier(partial_val)
        total = total + partial_val.astype(jnp.float32)
    results = total.astype(jnp.bfloat16).reshape(experts, capacity, width)
    returned = lax.all_to_all(results, "ep", split_axis=0, concat_axis=0, tiled=True)
    mine_places = lax.dynamic_index_in_dim(places, own, 0, keepdims=False)
    mine_weights = lax.dynamic_index_in_dim(weight_blocks, own, 0, keepdims=False)
    values = returned.reshape(experts * capacity, width)[mine_places]
    weighted = values.astype(jnp.float32) * mine_weights[:, None]
    expert_out = jnp.sum(weighted.reshape(block_rows, K, width), axis=1).astype(jnp.bfloat16)
    return (mixer_out, expert_out)


def solution(mesh):
    placed = (
        P(("ep", "tp"), None),
        P(),
        P(),
        P(),
        P("ep", None),
        P(),
        P("ep", None),
        P("ep", None),
        P("ep", None, "tp"),
        P("ep", None, "tp"),
        P("ep", "tp", None),
    )
    return jax.shard_map(
        on_device,
        mesh=mesh,
        in_specs=placed,
        out_specs=(P(("ep", "tp"), None), P(("ep", "tp"), None)),
        check_vma=False,
    )
```

profile of v0, /device:TPU:96, one launch (start us, length us, event | category | flops | bytes accessed | tf_op | source)
XLA Modules:
  0.0 234.7 jit_solution(8038040765326191246)
XLA Ops:
  7.2 1.6 copy.36
  9.5 2.8 %pad_maximum_fusion = bf16[256,6144]{1,0:T(8,128)(2,1)} fusion(bf16[256,2048]{1,0:T(8,128)(2,1)} %bitcast.58, bf16[256,2048]{1,0:T(8,128)(2,1)S(1)} %bitcast.56, bf16[256,2048]{1,0:T(8,128)(2,1)S(1)} %bitcast.57), kind=kLoop, calls=%fused_computation.7 | loop fusion | flops 9437184 | bytes 6291456 | tf_op jit(solution)/shard_map/concatenate | solution.py:24
  13.5 2.4 %reduce-window.6 = s32[4,64,2,128]{3,1,2,0:T(8,128)S(1)} reduce-window(s32[4,64,2,128]{3,1,2,0:T(8,128)S(1)} %fusion.25, s32[]{:T(128)} %constant.95.clone.1), window={size=1x1x1x128 pad=0_0x0_0x0_0x127_0}, to_apply=%region_1.2 | reduce-window | flops 8323072 | bytes 524292 | tf_op jit(solution)/shard_map/reduce-window
  16.9 1.4 scatter_custom_fusion
  18.3 3.1 %gather_fusion = bf16[384,2048]{1,0:T(8,128)(2,1)} fusion(bf16[129,2048]{1,0:T(8,128)(2,1)S(1)} %concatenate.10, s32[1024]{0:T(1024)S(1)} %pad_clamp_fusion.1), kind=kCustom, calls=%fused_computation | custom fusion | bytes 3147264 | tf_op jit(solution)/shard_map/gather | solution.py:78
  21.4 2.5 %broadcast_in_dim_reshape.4 = bf16[1,64,6,2048]{3,2,1,0:T(8,128)(2,1)S(1)} reshape(bf16[384,2048]{1,0:T(8,128)(2,1)} %gather_fusion) | data formatting | bytes 3145728 | tf_op jit(solution)/shard_map/broadcast_in_dim;reshape | solution.py:127
  23.9 60.0 %all_to_all.10 = bf16[1,64,6,2048]{3,2,0,1:T(8,128)(2,1)} all-to-all(bf16[1,64,6,2048]{3,2,0,1:T(8,128)(2,1)S(1)} %bitcast.55), channel_id=1, replica_groups=mesh['ep'=64,'tp'=4] {'ep'}, dimensions={1} | all-to-all | bytes 3145728 | tf_op jit(solution)/shard_map/all_to_all | solution.py:128
  84.0 2.6 %reshape.143 = bf16[384,2048]{1,0:T(8,128)(2,1)S(1)} reshape(bf16[1,64,6,2048]{3,2,0,1:T(8,128)(2,1)} %all_to_all.10) | data formatting | bytes 3145728 | tf_op jit(solution)/shard_map/reshape | solution.py:129
  86.6 48.9 %all-gather.2.cloned.1.call-done = bf16[1024,6144]{1,0:T(8,128)(2,1)} async-done(((bf16[256,6144]{1,0:T(8,128)(2,1)}), bf16[1024,6144]{1,0:T(8,128)(2,1)}) %all-gather.2.cloned.1.call-update) | async-done | bytes 12582928 | tf_op jit(solution)/shard_map/all_gather | solution.py:25
  135.5 4.0 %fusion.2 = f32[384,1024]{1,0:T(8,128)S(1)} fusion(bf16[384,2048]{1,0:T(8,128)(2,1)S(1)} %reshape.143, bf16[1024,6144]{1,0:T(8,128)(2,1)} %all-gather.2.cloned.1.call-done), kind=kOutput, calls=%fused_computation.5 | convolution fusion | flops 1610612736 | bytes 7340032 | tf_op jit(solution)/shard_map/dot_general | solution.py:130
  139.5 4.1 %multiply_convert_fusion = bf16[384,1024]{1,0:T(8,128)(2,1)S(1)} fusion(f32[384,1024]{1,0:T(8,128)S(1)} %fusion.2, bf16[384,2048]{1,0:T(8,128)(2,1)S(1)} %reshape.143, bf16[1024,6144]{1,0:T(8,128)(2,1)} %all-gather.2.cloned.1.call-done), kind=kOutput, calls=%fused_computation.15 | convolution fusion | flops 1612972032 | bytes 8126464 | tf_op jit(solution)/shard_map/dot_general | solution.py:131
  143.6 1.8 convolution_convert_fusion.3
  145.4 1.8 convolution_convert_fusion.2
  147.2 1.8 convolution_convert_fusion.1
  149.0 1.8 convolution_convert_fusion
  152.1 1.6 reshape.144
  153.6 10.6 %all-to-all-start.1 = ((bf16[64,6,2048]{2,1,0:T(8,128)(2,1)}), bf16[64,6,2048]{2,1,0:T(8,128)(2,1)}, u32[]{:S(2)}, u32[]{:S(2)}) async-start(bf16[64,6,2048]{2,1,0:T(8,128)(2,1)} %reshape.144), calls=%async_computation.1 | async-start | bytes 4194304 | tf_op jit(solution)/shard_map/all_to_all | solution.py:144
  164.3 3.6 %collective-permute-start = (bf16[15,1024]{1,0:T(8,128)(2,1)S(1)}, bf16[15,1024]{1,0:T(8,128)(2,1)S(1)}, u32[]{:S(2)}, u32[]{:S(2)}) collective-permute-start(bf16[15,1024]{1,0:T(8,128)(2,1)S(1)} %slice.93), channel_id=1, source_target_pairs={{0,1},{1,2},{2,3},{3,4},{4,5},{5,6},{6,7},{7,8},{8,9},{9,10},{10,1... | collective-permute-start | bytes 92168 | tf_op jit(solution)/shard_map/ppermute | solution.py:19
  168.5 45.4 %collective-permute-done = bf16[15,1024]{1,0:T(8,128)(2,1)S(1)} collective-permute-done((bf16[15,1024]{1,0:T(8,128)(2,1)S(1)}, bf16[15,1024]{1,0:T(8,128)(2,1)S(1)}, u32[]{:S(2)}, u32[]{:S(2)}) %collective-permute-start) | collective-permute-done | bytes 30752 | tf_op jit(solution)/shard_map/ppermute | solution.py:19
  214.2 1.9 fusion.18
  216.3 2.2 convolution_convert_fusion.4
  218.6 2.6 %reshape.145 = bf16[384,2048]{1,0:T(8,128)(2,1)S(1)} reshape(bf16[64,6,2048]{2,1,0:T(8,128)(2,1)} %all-to-all-done.1) | data formatting | bytes 3145728 | tf_op jit(solution)/shard_map/reshape | solution.py:147
  221.2 1.4 gather_fusion.1
  223.9 3.9 %multiply_reduce_fusion = bf16[128,2048]{1,0:T(8,128)(2,1)} fusion(f32[128,2,2048]{2,1,0:T(2,128)S(1)} %reshape.147, f32[128,2]{1,0:T(8,128)S(1)} %mul.78), kind=kLoop, calls=%fused_computation.14 | loop fusion | flops 786432 | bytes 2622464 | tf_op jit(solution)/shard_map/reduce_sum | solution.py:149
  (54 shorter events, 6.3 us)
Async XLA Ops:
  7.2 207.0 %copy-start = (bf16[8,128,128]{2,1,0:T(8,128)(2,1)S(1)}, bf16[8,128,128]{2,1,0:T(8,128)(2,1)}, u32[]{:S(2)}) copy-start(bf16[8,128,128]{2,1,0:T(8,128)(2,1)} %param.12) | copy-start | bytes 786436
  7.2 1.6 copy-start.1
  7.2 128.3 %all-gather.2.cloned.1.call-start = ((), (), s32[]{:S(2)}) async-start(), calls=%async_computation.2 | async-start | bytes 15728640 | tf_op jit(solution)/shard_map/all_gather | solution.py:25
  12.3 0.7 copy-start.5
  12.3 3.9 %copy-start.3 = (bf16[512,2048]{1,0:T(8,128)(2,1)S(1)}, bf16[512,2048]{1,0:T(8,128)(2,1)}, u32[]{:S(2)}) copy-start(bf16[512,2048]{1,0:T(8,128)(2,1)} %param.15) | copy-start | bytes 6291460
  12.4 4.1 %copy-start.4 = (f32[2048]{0:T(1024)S(1)}, f32[2048]{0:T(1024)}, u32[]{:S(2)}) copy-start(f32[2048]{0:T(1024)} %param.16) | copy-start | bytes 24580
  153.6 10.7 %copy-start.2 = (bf16[256,1024]{1,0:T(8,128)(2,1)S(1)}, bf16[256,1024]{1,0:T(8,128)(2,1)}, u32[]{:S(2)}) copy-start(bf16[256,1024]{1,0:T(8,128)(2,1)} %param.11) | copy-start | bytes 1572868
  153.6 14.4 %copy-start.6 = (f32[512,2]{0,1:T(2,128)S(1)}, f32[512,2]{0,1:T(2,128)}, u32[]{:S(2)}) copy-start(f32[512,2]{0,1:T(2,128)} %param.18) | copy-start | bytes 12292
  153.6 65.0 %all-to-all-start.1 = ((bf16[64,6,2048]{2,1,0:T(8,128)(2,1)}), bf16[64,6,2048]{2,1,0:T(8,128)(2,1)}, u32[]{:S(2)}, u32[]{:S(2)}) async-start(bf16[64,6,2048]{2,1,0:T(8,128)(2,1)} %reshape.144), calls=%async_computation.1 | async-start | bytes 4194304 | tf_op jit(solution)/shard_map/all_to_all | solution.py:144
  164.3 49.7 %collective-permute-start = (bf16[15,1024]{1,0:T(8,128)(2,1)S(1)}, bf16[15,1024]{1,0:T(8,128)(2,1)S(1)}, u32[]{:S(2)}, u32[]{:S(2)}) collective-permute-start(bf16[15,1024]{1,0:T(8,128)(2,1)S(1)} %slice.93), channel_id=1, source_target_pairs={{0,1},{1,2},{2,3},{3,4},{4,5},{5,6},{6,7},{7,8},{8,9},{9,10},{10,1... | collective-permute-start | bytes 92168 | tf_op jit(solution)/shard_map/ppermute | solution.py:19
  214.1 2.0 copy-start.7
  214.1 2.2 copy-start.8
Sparse Core Ops, SparseCore 0:
  12.5 122.9 all-gather.1
where the time goes:
time: 235 us
  waiting for transfers between devices  94.4 us (40%)
  blocking collectives  60 us (26%)
  local copies, waits for them, and re-layouts  20.7 us (9%)
  matrix products  19.5 us (8%)
  between operations  14.4 us (6%)
  starting transfers between devices  14.3 us (6%)
  other arithmetic  11.4 us (5%)
    all_to_all x1, blocking collectives, on_device(): lax.all_to_all(outgoing, 'ep', split_axis=1, concat_axis=1, tiled=True)  60 us
    all_gather x1, waiting for transfers between devices, rows_first(): out, at, gathered = (lax.all_gather(both, axis, axis=0, tiled=True), 0, [])  48.9 us
    ppermute x1, waiting for transfers between devices, passed_along(): return lax.ppermute(array, axis, pairs)  45.4 us
    all_to_all x1, starting transfers between devices, on_device(): lax.all_to_all(results, 'ep', split_axis=0, concat_axis=0, tiled=True)  10.6 us
    dot_general x4, matrix products, on_device(): jnp.dot(hidden[:, block * quarter:(block + 1) * quarter], down_whole[bloc...  7.21 us
  transfers between devices with their start and end apart: 3, of which 2 were waited for; matrix products, arithmetic and copies ran while one was open for 8% of the time, Pallas kernels for 0%

commit v1 on v0

v1 whole, which is shorter than its diff:
```python
from functools import partial

import jax
import jax.numpy as jnp
from jax import lax
from jax.experimental import pallas as pl
from jax.experimental.pallas import tpu as pltpu
from jax.sharding import PartitionSpec as P

GDIM = 128
WMAX = 16
K = 2
EPS = 0.05

CAP = 6
SUB = 8
MAIN = 1536
TAIL = 512
FOLD = MAIN // TAIL
BF16 = jnp.bfloat16
F32 = jnp.float32


def passed_along(array, axis, by):
    length = lax.axis_size(axis)
    pairs = [(i, i + by) for i in range(length) if 0 <= i + by < length]
    return lax.ppermute(array, axis, pairs)


def swapped(array, flip):
    eps, tps = lax.axis_size("ep"), lax.axis_size("tp")
    pairs = []
    for e in range(eps):
        for y in range(tps):
            other = y ^ 1 if (e + flip) % 2 == 0 else tps - 1 - y
            pairs.append((e * tps + y, e * tps + other))
    return lax.ppermute(array, ("ep", "tp"), pairs)


def window_sizes(width):
    group_of = jnp.arange(width) // GDIM
    level = group_of % 4
    return jnp.where(
        level == 0, 2.0, jnp.where(level == 1, 4.0, jnp.where(level == 2, 8.0, 16.0))
    ).astype(F32)


def pooled_rows(extended, positions):
    extent = extended.shape[0] - (WMAX - 1)
    window = window_sizes(extended.shape[1])
    running = jnp.zeros((extent, extended.shape[1]), F32)
    picked = running
    for offset in range(WMAX):
        running = running + extended[WMAX - 1 - offset : WMAX - 1 - offset + extent]
        if offset + 1 in (2, 4, 8, 16):
            picked = jnp.where(window[None, :] == offset + 1, running, picked)
    counted = jnp.minimum(positions[:, None] + 1.0, window[None, :])
    return (picked / counted - extended[WMAX - 1 :]).astype(BF16)


def slot_ranks(routes_ref, rows, tokens):
    first, second = routes_ref[0:1, :], routes_ref[1:2, :]
    row = lax.broadcasted_iota(jnp.int32, (rows, tokens), 0)
    expert, sub = row // SUB, row % SUB
    by_first, by_second = expert == first, expert == second
    named = by_first | by_second
    before = lax.broadcasted_iota(jnp.int32, (tokens, tokens), 0) < lax.broadcasted_iota(
        jnp.int32, (tokens, tokens), 1
    )
    rank = jnp.dot(
        named.astype(F32).astype(BF16), before.astype(F32).astype(BF16), preferred_element_type=F32
    ).astype(jnp.int32)
    return by_first, named, rank, sub


def send_kernel(own_ref, rows_ref, gain_ref, routes_ref, out_ref):
    del own_ref
    tokens = rows_ref.shape[0]
    features = rows_ref[...].astype(F32)
    inverse = lax.rsqrt(jnp.mean(features * features, axis=-1, keepdims=True) + EPS)
    normed = (features * inverse * gain_ref[...]).astype(BF16)
    _, named, rank, sub = slot_ranks(routes_ref, out_ref.shape[0], tokens)
    head = (named & (rank == sub) & (sub < CAP)).astype(F32).astype(BF16)
    for c in range(FOLD):
        tail = (named & (sub >= CAP) & (rank == (sub - CAP) * FOLD + c)).astype(F32).astype(BF16)
        out_ref[:, c * TAIL : (c + 1) * TAIL] = (
            jnp.dot(head, normed[:, c * TAIL : (c + 1) * TAIL], preferred_element_type=F32)
            + jnp.dot(tail, normed[:, MAIN:], preferred_element_type=F32)
        ).astype(BF16)


def send_rows(expert_in, gain, routes_t, own, experts):
    tokens = expert_in.shape[0] // lax.axis_size("tp")
    width = expert_in.shape[1]
    return pl.pallas_call(
        send_kernel,
        out_shape=jax.ShapeDtypeStruct((experts * SUB, MAIN), BF16),
        grid_spec=pltpu.PrefetchScalarGridSpec(
            num_scalar_prefetch=1,
            grid=(1,),
            in_specs=[
                pl.BlockSpec((tokens, width), lambda i, own: (own[0], 0)),
                pl.BlockSpec((1, width), lambda i, own: (0, 0)),
                pl.BlockSpec((K, tokens), lambda i, own: (0, own[0])),
            ],
            out_specs=pl.BlockSpec((experts * SUB, MAIN), lambda i, own: (0, 0)),
        ),
        cost_estimate=pl.CostEstimate(flops=400_000_000, bytes_accessed=2_100_000, transcendentals=128),
        name="send_rows",
    )(own, expert_in, gain.reshape(1, width), routes_t)


def spread(rows, c, turned):
    a = lax.broadcasted_iota(jnp.int32, (rows, rows), 1 if turned else 0)
    b = lax.broadcasted_iota(jnp.int32, (rows, rows), 0 if turned else 1)
    k, s = a % SUB, b % SUB
    return (
        ((a // SUB) == (b // SUB)) & (k < CAP) & (s >= CAP) & (k == (s - CAP) * FOLD + c)
    ).astype(F32).astype(BF16)


def ffn_kernel(x_ref, ga_ref, gb_ref, ua_ref, ub_ref, da_ref, db_ref, out_ref):
    rows = x_ref.shape[0]
    part = 128
    tails = []
    gathers = [spread(part, c, False) for c in range(FOLD)]
    for r in range(rows // part):
        here = slice(r * part, (r + 1) * part)
        tails.append(
            sum(
                jnp.dot(gathers[c], x_ref[here, c * TAIL : (c + 1) * TAIL], preferred_element_type=F32)
                for c in range(FOLD)
            ).astype(BF16)
        )
    tail = jnp.concatenate(tails, axis=0)
    x = x_ref[...]

    def times(w_ref):
        return jnp.dot(x, w_ref[:MAIN, :], preferred_element_type=F32) + jnp.dot(
            tail, w_ref[MAIN:, :], preferred_element_type=F32
        )

    hidden_a = (jax.nn.silu(times(ga_ref)) * times(ua_ref)).astype(BF16)
    hidden_b = (jax.nn.silu(times(gb_ref)) * times(ub_ref)).astype(BF16)

    def down(columns):
        return (
            jnp.dot(hidden_a, da_ref[:, columns], preferred_element_type=F32)
            + jnp.dot(hidden_b, db_ref[:, columns], preferred_element_type=F32)
        ).astype(BF16)

    last = down(slice(MAIN, MAIN + TAIL))
    keep = (lax.broadcasted_iota(jnp.int32, (part, TAIL), 0) % SUB) < CAP
    scatters = [spread(part, c, True) for c in range(FOLD)]
    for c in range(FOLD):
        columns = slice(c * TAIL, (c + 1) * TAIL)
        block = down(columns).astype(F32)
        for r in range(rows // part):
            here = slice(r * part, (r + 1) * part)
            folded = jnp.dot(scatters[c], last[here], preferred_element_type=F32)
            out_ref[here, columns] = jnp.where(keep, block[here], folded).astype(BF16)


def half_ffn(x, ga, gb, ua, ub, da, db):
    rows = x.shape[0]
    step = min(rows, 256)
    whole = lambda w: pl.BlockSpec(w.shape, lambda i: (0, 0))
    hidden = ga.shape[1] + gb.shape[1]
    return pl.pallas_call(
        ffn_kernel,
        out_shape=jax.ShapeDtypeStruct(x.shape, BF16),
        grid=(rows // step,),
        in_specs=[pl.BlockSpec((step, MAIN), lambda i: (i, 0))]
        + [whole(w) for w in (ga, gb, ua, ub, da, db)],
        out_specs=pl.BlockSpec((step, MAIN), lambda i: (i, 0)),
        cost_estimate=pl.CostEstimate(
            flops=rows * hidden * (MAIN + TAIL) * 6,
            bytes_accessed=rows * MAIN * 4 + 6 * ga.size * 2,
            transcendentals=rows * hidden,
        ),
        compiler_params=pltpu.CompilerParams(vmem_limit_bytes=40 * 1024 * 1024),
        name="half_ffn",
    )(x, ga, gb, ua, ub, da, db)


def combine_kernel(own_ref, values_ref, routes_ref, weight_ref, out_ref):
    del own_ref
    rows, tokens = values_ref.shape[0], out_ref.shape[0]
    by_first, named, rank, sub = slot_ranks(routes_ref, rows, tokens)
    weight = jnp.where(by_first, weight_ref[0:1, :], weight_ref[1:2, :])

    def taken(chosen, columns):
        picked = jnp.where(chosen, weight, 0.0).T
        high = picked.astype(BF16)
        low = (picked - high.astype(F32)).astype(BF16)
        values = values_ref[:, columns]
        return jnp.dot(high, values, preferred_element_type=F32) + jnp.dot(
            low, values, preferred_element_type=F32
        )

    head = named & (rank == sub) & (sub < CAP)
    tail = jnp.zeros((tokens, TAIL), F32)
    for c in range(FOLD):
        columns = slice(c * TAIL, (c + 1) * TAIL)
        out_ref[:, columns] = taken(head, columns).astype(BF16)
        tail += taken(named & (sub >= CAP) & (rank == (sub - CAP) * FOLD + c), columns)
    out_ref[:, MAIN:] = tail.astype(BF16)


def combine(values, routes_t, weight_t, own, tokens):
    rows = values.shape[0]
    width = MAIN + TAIL
    return pl.pallas_call(
        combine_kernel,
        out_shape=jax.ShapeDtypeStruct((tokens, width), BF16),
        grid_spec=pltpu.PrefetchScalarGridSpec(
            num_scalar_prefetch=1,
            grid=(1,),
            in_specs=[
                pl.BlockSpec((rows, MAIN), lambda i, own: (0, 0)),
                pl.BlockSpec((K, tokens), lambda i, own: (0, own[0])),
                pl.BlockSpec((K, tokens), lambda i, own: (0, own[0])),
            ],
            out_specs=pl.BlockSpec((tokens, width), lambda i, own: (0, 0)),
        ),
        cost_estimate=pl.CostEstimate(flops=600_000_000, bytes_accessed=2_100_000, transcendentals=0),
        name="combine",
    )(own, values, routes_t, weight_t)


def on_device(
    pool_in,
    w_pool,
    pool_scale,
    w_out,
    expert_in,
    ffn_gain,
    routes,
    route_weight,
    w_gate,
    w_up,
    w_down,
):
    rows_here = pool_in.shape[0]
    tokens = routes.shape[0] // lax.axis_size("tp")
    experts = lax.axis_size("ep") * w_gate.shape[0]
    own = lax.axis_index("tp").astype(jnp.int32).reshape(1)
    routes_t, weight_t = routes.T, route_weight.T

    sent = send_rows(expert_in, ffn_gain, routes_t, own, experts)
    mine = lax.all_to_all(
        sent.reshape(experts, SUB, MAIN), "ep", split_axis=0, concat_axis=0, tiled=True
    ).reshape(experts * SUB, MAIN)

    gate, up, down = w_gate[0], w_up[0], w_down[0]
    gate_b, up_b, down_b = swapped(gate, 0), swapped(up, 0), swapped(down, 0)
    ffn = lambda x: half_ffn(x, gate, gate_b, up, up_b, down, down_b)

    chunks = 2
    size = mine.shape[0] // chunks
    theirs = [swapped(mine[i * size : (i + 1) * size], 1) for i in range(chunks)]
    kept = ffn(mine)
    back = [swapped(ffn(t), 1) for t in theirs]
    results = (kept.astype(F32) + jnp.concatenate(back, axis=0).astype(F32)).astype(BF16)

    returned = lax.all_to_all(
        results.reshape(experts, SUB, MAIN), "ep", split_axis=0, concat_axis=0, tiled=True
    ).reshape(experts * SUB, MAIN)
    expert_out = combine(returned, routes_t, weight_t, own, tokens)

    before = passed_along(pool_in[rows_here - (WMAX - 1) :], ("ep", "tp"), 1)
    extended = jnp.concatenate([before, pool_in], axis=0).astype(F32)
    positions = (lax.axis_index(("ep", "tp")) * rows_here + jnp.arange(rows_here)).astype(F32)
    pooled = pooled_rows(extended, positions)
    group_count = w_pool.shape[0]
    grouped = jnp.einsum(
        "tgc,gcd->tgd",
        pooled.reshape(rows_here, group_count, GDIM),
        w_pool,
        preferred_element_type=F32,
    )
    scaled = (grouped.reshape(rows_here, -1) * pool_scale).astype(BF16)
    mixer_out = jnp.dot(scaled, w_out, preferred_element_type=F32).astype(BF16)
    return (mixer_out, expert_out)


def solution(mesh):
    placed = (
        P(("ep", "tp"), None),
        P(),
        P(),
        P(),
        P("ep", None),
        P(),
        P("ep", None),
        P("ep", None),
        P("ep", None, "tp"),
        P("ep", None, "tp"),
        P("ep", "tp", None),
    )
    return jax.shard_map(
        on_device,
        mesh=mesh,
        in_specs=placed,
        out_specs=(P(("ep", "tp"), None), P(("ep", "tp"), None)),
        check_vma=False,
    )
```

time: 235 us -> 151 us (0.64)
  blocking collectives: 60 us -> 0 us
  Pallas kernels: 0 us -> 21.9 us
  local copies, waits for them, and re-layouts: 20.7 us -> 1.34 us
  starting transfers between devices: 14.3 us -> 32.8 us
  matrix products: 19.5 us -> 4.18 us
  between operations: 14.4 us -> 0.83 us
  other arithmetic: 11.4 us -> 1.93 us
  waiting for transfers between devices: 94.4 us -> 87.7 us
    all_to_all x1 -> x0, blocking collectives: 60 us -> none  [on_device(): lax.all_to_all(outgoing, 'ep', split_axis=1, concat_axis=1, tiled=True)]
    all_gather x1 -> x0, waiting for transfers between devices: 48.9 us -> none  [rows_first(): out, at, gathered = (lax.all_gather(both, axis, axis=0, tiled=True), 0, [])]
    all_to_all x1 -> x2, waiting for transfers between devices: 0.01 us -> 35 us  [the longest x1 35 us: on_device(): lax.all_to_all(sent.reshape(experts, SUB, MAIN), 'ep', split_axis=0, conc...]
    pallas_call x0 -> x5, Pallas kernels: none -> 21.9 us  [the longest x3 15 us: half_ffn(): pl.pallas_call(ffn_kernel, out_shape=jax.ShapeDtypeStruct(x.shape, BF16),...]
    dot_general x7 -> x1, matrix products: 17.6 us -> 2.25 us  [on_device(): mixer_out = jnp.dot(scaled, w_out, preferred_element_type=F32).astype(BF16)]
    ppermute x0 -> x7, waiting for transfers between devices: none -> 14.7 us  [swapped(): return lax.ppermute(array, ('ep', 'tp'), pairs)]
    ppermute x0 -> x7, starting transfers between devices: none -> 13.2 us  [swapped(): return lax.ppermute(array, ('ep', 'tp'), pairs)]
    ppermute x1, waiting for transfers between devices: 45.4 us -> 38 us  [passed_along(): return lax.ppermute(array, axis, pairs)]
  transfers between devices with their start and end apart: 3 -> 10, of which waited for: 2 -> 5; matrix products, arithmetic and copies ran while one was open for 8% -> 3% of each run, Pallas kernels for 0% -> 10%
where the time goes in v1:
time: 151 us
  waiting for transfers between devices  87.7 us (58%)
  starting transfers between devices  32.8 us (22%)
  Pallas kernels  21.9 us (15%)
  matrix products  4.18 us (3%)
  other arithmetic  1.93 us (1%)
    ppermute x1, waiting for transfers between devices, passed_along(): return lax.ppermute(array, axis, pairs)  38 us
    all_to_all x1, waiting for transfers between devices, on_device(): lax.all_to_all(sent.reshape(experts, SUB, MAIN), 'ep', split_axis=0, conc...  35 us
    pallas_call x3, Pallas kernels, half_ffn(): pl.pallas_call(ffn_kernel, out_shape=jax.ShapeDtypeStruct(x.shape, BF16),...  15 us
    ppermute x7, waiting for transfers between devices, swapped(): return lax.ppermute(array, ('ep', 'tp'), pairs)  14.7 us
    ppermute x7, starting transfers between devices, swapped(): return lax.ppermute(array, ('ep', 'tp'), pairs)  13.2 us
    all_to_all x1, starting transfers between devices, on_device(): lax.all_to_all(sent.reshape(experts, SUB, MAIN), 'ep', split_axis=0, conc...  10.9 us
    all_to_all x1, starting transfers between devices, on_device(): lax.all_to_all(results.reshape(experts, SUB, MAIN), 'ep', split_axis=0, c...  6.84 us
    pallas_call x1, Pallas kernels, combine(): pl.pallas_call(combine_kernel, out_shape=jax.ShapeDtypeStruct((tokens, wi...  3.48 us
  transfers between devices with their start and end apart: 10, of which 5 were waited for; matrix products, arithmetic and copies ran while one was open for 3% of the time, Pallas kernels for 10%

profile of v1, /device:TPU:96, one launch (start us, length us, event | category | flops | bytes accessed | tf_op | source)
XLA Modules:
  0.0 150.7 jit_solution(8479231976530313541)
XLA Ops:
  0.7 3.5 %send_rows.1 = bf16[512,1536]{1,0:T(8,128)(2,1)} custom-call(s32[1]{0:T(128)} %bitcast.2.own_ref, bf16[512,2048]{1,0:T(8,128)(2,1)} %rows_ref.1, f32[1,2048]{1,0:T(1,128)} %bitcast.47, s32[2,512]{1,0:T(2,128)} %bitcast.48), custom_call_target="tpu_custom_call" | custom-call | flops 400000000 | bytes 2100000 | tf_op jit(solution)/shard_map/send_rows/pallas_call | solution.py:95
  4.1 10.9 %all-to-all-start = ((bf16[64,8,1536]{2,1,0:T(8,128)(2,1)}), bf16[64,8,1536]{2,1,0:T(8,128)(2,1)S(1)}, u32[]{:S(2)}, u32[]{:S(2)}) async-start(bf16[64,8,1536]{2,1,0:T(8,128)(2,1)} %bitcast.45), calls=%async_computation | async-start | bytes 3145728 | tf_op jit(solution)/shard_map/all_to_all | solution.py:251
  15.0 1.7 %collective-permute-start.1 = (bf16[2048,256]{1,0:T(8,128)(2,1)S(1)}, bf16[2048,256]{1,0:T(8,128)(2,1)}, u32[]{:S(2)}, u32[]{:S(2)}) collective-permute-start(bf16[2048,256]{1,0:T(8,128)(2,1)S(1)} %bitcast.33), channel_id=1, source_target_pairs={{0,1},{1,0},{2,3},{3,2},{4,7},{5,6},{6,5},{7,4},{8,9},{9,8},{10,11... | collective-permute-start | bytes 3145736 | tf_op jit(solution)/shard_map/ppermute | solution.py:37
  16.6 0.4 collective-permute-start.2
  17.1 1.6 %collective-permute-start.3 = (bf16[256,2048]{1,0:T(8,128)(2,1)}, bf16[256,2048]{1,0:T(8,128)(2,1)}, u32[]{:S(2)}, u32[]{:S(2)}) collective-permute-start(bf16[256,2048]{1,0:T(8,128)(2,1)} %bitcast.41), channel_id=1, source_target_pairs={{0,1},{1,0},{2,3},{3,2},{4,7},{5,6},{6,5},{7,4},{8,9},{9,8},{10,11... | collective-permute-start | bytes 3145736 | tf_op jit(solution)/shard_map/ppermute | solution.py:37
  18.7 35.0 %all-to-all-done = bf16[64,8,1536]{2,1,0:T(8,128)(2,1)S(1)} async-done(((bf16[64,8,1536]{2,1,0:T(8,128)(2,1)}), bf16[64,8,1536]{2,1,0:T(8,128)(2,1)S(1)}, u32[]{:S(2)}, u32[]{:S(2)}) %all-to-all-start) | async-done | bytes 1572896 | tf_op jit(solution)/shard_map/all_to_all | solution.py:251
  53.8 3.1 %collective-permute-start.4 = (bf16[256,1536]{1,0:T(8,128)(2,1)S(1)}, bf16[256,1536]{1,0:T(8,128)(2,1)S(1)}, u32[]{:S(2)}, u32[]{:S(2)}) collective-permute-start(bf16[256,1536]{1,0:T(8,128)(2,1)S(1)} %get-tuple-element.2), channel_id=1, source_target_pairs={{0,3},{1,2},{2,1},{3,0},{4,5},{5,4},{6,7},{7,6},{8,11},{9,10},{10,... | collective-permute-start | bytes 2359304 | tf_op jit(solution)/shard_map/ppermute | solution.py:37
  56.9 0.2 collective-permute-start.6
  57.1 10.0 %collective-permute-done.4.x_ref = bf16[256,1536]{1,0:T(8,128)(2,1)S(1)} collective-permute-done((bf16[256,1536]{1,0:T(8,128)(2,1)S(1)}, bf16[256,1536]{1,0:T(8,128)(2,1)S(1)}, u32[]{:S(2)}, u32[]{:S(2)}) %collective-permute-start.4) | collective-permute-done | bytes 786464 | tf_op jit(solution)/shard_map/ppermute | solution.py:37
  67.1 4.2 %half_ffn.4 = bf16[256,1536]{1,0:T(8,128)(2,1)S(1)} custom-call(bf16[256,1536]{1,0:T(8,128)(2,1)S(1)} %collective-permute-done.4.x_ref, bf16[2048,256]{1,0:T(8,128)(2,1)S(1)} %bitcast.34, bf16[2048,256]{1,0:T(8,128)(2,1)} %collective-permute-done.1.gb_ref, bf16[2048,256]{1,0:T(8,128)(2,1)S(1)} %bitcast.38, bf16[2048,256]{1,0:T(8,128)(2,1)} %collective-permute-done.2.ub_ref, ...), custom_call_target="tpu_custom_call" | custom-call | flops 1610612736 | bytes 7864320 | tf_op jit(solution)/shard_map/half_ffn/pallas_call | solution.py:169
  71.3 3.1 %collective-permute-start.5 = (bf16[256,1536]{1,0:T(8,128)(2,1)S(1)}, bf16[256,1536]{1,0:T(8,128)(2,1)S(1)}, u32[]{:S(2)}, u32[]{:S(2)}) collective-permute-start(bf16[256,1536]{1,0:T(8,128)(2,1)S(1)} %half_ffn.4), channel_id=1, source_target_pairs={{0,3},{1,2},{2,1},{3,0},{4,5},{5,4},{6,7},{7,6},{8,11},{9,10},{10,... | collective-permute-start | bytes 2359304 | tf_op jit(solution)/shard_map/ppermute | solution.py:37
  74.4 1.1 collective-permute-done.6.x_ref
  75.5 4.2 %half_ffn.5 = bf16[256,1536]{1,0:T(8,128)(2,1)S(1)} custom-call(bf16[256,1536]{1,0:T(8,128)(2,1)S(1)} %collective-permute-done.6.x_ref, bf16[2048,256]{1,0:T(8,128)(2,1)S(1)} %bitcast.35, bf16[2048,256]{1,0:T(8,128)(2,1)} %collective-permute-done.1.gb_ref, bf16[2048,256]{1,0:T(8,128)(2,1)S(1)} %bitcast.39, bf16[2048,256]{1,0:T(8,128)(2,1)} %collective-permute-done.2.ub_ref, ...), custom_call_target="tpu_custom_call" | custom-call | flops 1610612736 | bytes 7864320 | tf_op jit(solution)/shard_map/half_ffn/pallas_call | solution.py:169
  79.7 3.1 %collective-permute-start.7 = (bf16[256,1536]{1,0:T(8,128)(2,1)S(1)}, bf16[256,1536]{1,0:T(8,128)(2,1)S(1)}, u32[]{:S(2)}, u32[]{:S(2)}) collective-permute-start(bf16[256,1536]{1,0:T(8,128)(2,1)S(1)} %half_ffn.5), channel_id=1, source_target_pairs={{0,3},{1,2},{2,1},{3,0},{4,5},{5,4},{6,7},{7,6},{8,11},{9,10},{10,... | collective-permute-start | bytes 2359304 | tf_op jit(solution)/shard_map/ppermute | solution.py:37
  82.8 6.6 %half_ffn.3 = bf16[512,1536]{1,0:T(8,128)(2,1)S(1)} custom-call(bf16[512,1536]{1,0:T(8,128)(2,1)S(1)} %bitcast.32, bf16[2048,256]{1,0:T(8,128)(2,1)S(1)} %bitcast.36, bf16[2048,256]{1,0:T(8,128)(2,1)} %collective-permute-done.1.gb_ref, bf16[2048,256]{1,0:T(8,128)(2,1)S(1)} %bitcast.40, bf16[2048,256]{1,0:T(8,128)(2,1)} %collective-permute-done.2.ub_ref, ...), custom_call_target="tpu_custom_call" | custom-call | flops 3221225472 | bytes 9437184 | tf_op jit(solution)/shard_map/half_ffn/pallas_call | solution.py:169
  89.4 3.6 %collective-permute-done.7 = bf16[256,1536]{1,0:T(8,128)(2,1)S(1)} collective-permute-done((bf16[256,1536]{1,0:T(8,128)(2,1)S(1)}, bf16[256,1536]{1,0:T(8,128)(2,1)S(1)}, u32[]{:S(2)}, u32[]{:S(2)}) %collective-permute-start.7) | collective-permute-done | bytes 786464 | tf_op jit(solution)/shard_map/ppermute | solution.py:37
  93.0 1.5 %fusion = bf16[64,8,1536]{2,1,0:T(8,128)(2,1)} fusion(bf16[512,1536]{1,0:T(8,128)(2,1)S(1)} %half_ffn.3, bf16[256,1536]{1,0:T(8,128)(2,1)S(1)} %collective-permute-done.7, bf16[256,1536]{1,0:T(8,128)(2,1)S(1)} %collective-permute-done.5), kind=kLoop, calls=%fused_computation.2 | loop fusion | flops 5505024 | bytes 4718592 | tf_op jit(solution)/shard_map/reshape | solution.py:267
  94.6 6.8 %all-to-all-start.1 = ((bf16[64,8,1536]{2,1,0:T(8,128)(2,1)}), bf16[64,8,1536]{2,1,0:T(8,128)(2,1)S(1)}, u32[]{:S(2)}, u32[]{:S(2)}) async-start(bf16[64,8,1536]{2,1,0:T(8,128)(2,1)} %fusion), calls=%async_computation.1 | async-start | bytes 3145728 | tf_op jit(solution)/shard_map/all_to_all | solution.py:266
  101.4 1.9 %collective-permute-start = (bf16[15,1024]{1,0:T(8,128)(2,1)S(1)}, bf16[15,1024]{1,0:T(8,128)(2,1)S(1)}, u32[]{:S(2)}, u32[]{:S(2)}) collective-permute-start(bf16[15,1024]{1,0:T(8,128)(2,1)S(1)} %slice.64), channel_id=1, source_target_pairs={{0,1},{1,2},{2,3},{3,4},{4,5},{5,6},{6,7},{7,8},{8,9},{9,10},{10,1... | collective-permute-start | bytes 92168 | tf_op jit(solution)/shard_map/ppermute | solution.py:27
  103.4 38.0 %collective-permute-done = bf16[15,1024]{1,0:T(8,128)(2,1)S(1)} collective-permute-done((bf16[15,1024]{1,0:T(8,128)(2,1)S(1)}, bf16[15,1024]{1,0:T(8,128)(2,1)S(1)}, u32[]{:S(2)}, u32[]{:S(2)}) %collective-permute-start) | collective-permute-done | bytes 30752 | tf_op jit(solution)/shard_map/ppermute | solution.py:27
  141.6 1.9 %fusion.6 = f32[8,256,128]{1,2,0:T(8,128)S(1)} fusion(bf16[8,128,128]{2,1,0:T(8,128)(2,1)S(1)} %copy-done, f32[1024]{0:T(1024)S(1)} %select_select_fusion, f32[256]{0:T(256)S(1)} %convert_add_fusion, pred[1024]{0:T(1024)(128)(4,1)S(1)} %get-tuple-element.7, pred[1024]{0:T(1024)(128)(4,1)S(1)} %get-tuple-element.6, ...), kind=kOutput, calls=%fused_computation.27 | convolution fusion | flops 73138176 | bytes 18097152 | tf_op jit(solution)/shard_map/tgc,gcd->tgd/dot_general | solution.py:276
  143.8 2.2 %convolution_convert_fusion = bf16[256,2048]{1,0:T(8,128)(2,1)} fusion(bf16[256,1024]{0,1:T(8,128)(2,1)S(1)} %fusion.4, bf16[1024,2048]{1,0:T(8,128)(2,1)S(1)} %copy-done.7), kind=kOutput, calls=%fused_computation.1 | convolution fusion | flops 1074266112 | bytes 5767168 | tf_op jit(solution)/shard_map/dot_general | solution.py:283
  146.0 1.2 copy-done.4
  147.2 3.5 %combine.1 = bf16[128,2048]{1,0:T(8,128)(2,1)} custom-call(s32[1]{0:T(128)} %bitcast.2.own_ref, bf16[512,1536]{1,0:T(8,128)(2,1)} %bitcast.46, s32[2,512]{1,0:T(2,128)} %bitcast.49, f32[2,512]{1,0:T(2,128)} %bitcast.50), custom_call_target="tpu_custom_call" | custom-call | flops 600000000 | bytes 2100000 | tf_op jit(solution)/shard_map/combine/pallas_call | solution.py:213
  (28 shorter events, 0.6 us)
Async XLA Ops:
  0.6 140.9 %copy-start = (bf16[8,128,128]{2,1,0:T(8,128)(2,1)S(1)}, bf16[8,128,128]{2,1,0:T(8,128)(2,1)}, u32[]{:S(2)}) copy-start(bf16[8,128,128]{2,1,0:T(8,128)(2,1)} %param.12) | copy-start | bytes 786436
  4.1 10.9 %copy-start.1 = (bf16[1,2048,256]{2,1,0:T(8,128)(2,1)S(1)}, bf16[1,2048,256]{2,1,0:T(8,128)(2,1)}, u32[]{:S(2)}) copy-start(bf16[1,2048,256]{2,1,0:T(8,128)(2,1)} %param.19) | copy-start | bytes 3145732
  4.1 49.6 %all-to-all-start = ((bf16[64,8,1536]{2,1,0:T(8,128)(2,1)}), bf16[64,8,1536]{2,1,0:T(8,128)(2,1)S(1)}, u32[]{:S(2)}, u32[]{:S(2)}) async-start(bf16[64,8,1536]{2,1,0:T(8,128)(2,1)} %bitcast.45), calls=%async_computation | async-start | bytes 3145728 | tf_op jit(solution)/shard_map/all_to_all | solution.py:251
  15.0 42.2 %collective-permute-start.1 = (bf16[2048,256]{1,0:T(8,128)(2,1)S(1)}, bf16[2048,256]{1,0:T(8,128)(2,1)}, u32[]{:S(2)}, u32[]{:S(2)}) collective-permute-start(bf16[2048,256]{1,0:T(8,128)(2,1)S(1)} %bitcast.33), channel_id=1, source_target_pairs={{0,1},{1,0},{2,3},{3,2},{4,7},{5,6},{6,5},{7,4},{8,9},{9,8},{10,11... | collective-permute-start | bytes 3145736 | tf_op jit(solution)/shard_map/ppermute | solution.py:37
  16.6 40.5 %collective-permute-start.2 = (bf16[2048,256]{1,0:T(8,128)(2,1)}, bf16[2048,256]{1,0:T(8,128)(2,1)}, u32[]{:S(2)}, u32[]{:S(2)}) collective-permute-start(bf16[2048,256]{1,0:T(8,128)(2,1)} %bitcast.37), channel_id=1, source_target_pairs={{0,1},{1,0},{2,3},{3,2},{4,7},{5,6},{6,5},{7,4},{8,9},{9,8},{10,11... | collective-permute-start | bytes 3145736 | tf_op jit(solution)/shard_map/ppermute | solution.py:37
  17.1 40.0 %collective-permute-start.3 = (bf16[256,2048]{1,0:T(8,128)(2,1)}, bf16[256,2048]{1,0:T(8,128)(2,1)}, u32[]{:S(2)}, u32[]{:S(2)}) collective-permute-start(bf16[256,2048]{1,0:T(8,128)(2,1)} %bitcast.41), channel_id=1, source_target_pairs={{0,1},{1,0},{2,3},{3,2},{4,7},{5,6},{6,5},{7,4},{8,9},{9,8},{10,11... | collective-permute-start | bytes 3145736 | tf_op jit(solution)/shard_map/ppermute | solution.py:37
  53.7 13.4 %copy-start.2 = (bf16[1,2048,256]{2,1,0:T(8,128)(2,1)S(1)}, bf16[1,2048,256]{2,1,0:T(8,128)(2,1)}, u32[]{:S(2)}) copy-start(bf16[1,2048,256]{2,1,0:T(8,128)(2,1)} %param.20) | copy-start | bytes 3145732
  53.7 13.4 %copy-start.3 = (bf16[1,256,2048]{2,1,0:T(8,128)(2,1)S(1)}, bf16[1,256,2048]{2,1,0:T(8,128)(2,1)}, u32[]{:S(2)}) copy-start(bf16[1,256,2048]{2,1,0:T(8,128)(2,1)} %param.21) | copy-start | bytes 3145732
  53.8 13.3 %collective-permute-start.4 = (bf16[256,1536]{1,0:T(8,128)(2,1)S(1)}, bf16[256,1536]{1,0:T(8,128)(2,1)S(1)}, u32[]{:S(2)}, u32[]{:S(2)}) collective-permute-start(bf16[256,1536]{1,0:T(8,128)(2,1)S(1)} %get-tuple-element.2), channel_id=1, source_target_pairs={{0,3},{1,2},{2,1},{3,0},{4,5},{5,4},{6,7},{7,6},{8,11},{9,10},{10,... | collective-permute-start | bytes 2359304 | tf_op jit(solution)/shard_map/ppermute | solution.py:37
  56.9 18.6 %collective-permute-start.6 = (bf16[256,1536]{1,0:T(8,128)(2,1)S(1)}, bf16[256,1536]{1,0:T(8,128)(2,1)S(1)}, u32[]{:S(2)}, u32[]{:S(2)}) collective-permute-start(bf16[256,1536]{1,0:T(8,128)(2,1)S(1)} %get-tuple-element.3), channel_id=1, source_target_pairs={{0,3},{1,2},{2,1},{3,0},{4,5},{5,4},{6,7},{7,6},{8,11},{9,10},{10,... | collective-permute-start | bytes 2359304 | tf_op jit(solution)/shard_map/ppermute | solution.py:37
  71.3 18.1 %collective-permute-start.5 = (bf16[256,1536]{1,0:T(8,128)(2,1)S(1)}, bf16[256,1536]{1,0:T(8,128)(2,1)S(1)}, u32[]{:S(2)}, u32[]{:S(2)}) collective-permute-start(bf16[256,1536]{1,0:T(8,128)(2,1)S(1)} %half_ffn.4), channel_id=1, source_target_pairs={{0,3},{1,2},{2,1},{3,0},{4,5},{5,4},{6,7},{7,6},{8,11},{9,10},{10,... | collective-permute-start | bytes 2359304 | tf_op jit(solution)/shard_map/ppermute | solution.py:37
  79.7 13.3 %collective-permute-start.7 = (bf16[256,1536]{1,0:T(8,128)(2,1)S(1)}, bf16[256,1536]{1,0:T(8,128)(2,1)S(1)}, u32[]{:S(2)}, u32[]{:S(2)}) collective-permute-start(bf16[256,1536]{1,0:T(8,128)(2,1)S(1)} %half_ffn.5), channel_id=1, source_target_pairs={{0,3},{1,2},{2,1},{3,0},{4,5},{5,4},{6,7},{7,6},{8,11},{9,10},{10,... | collective-permute-start | bytes 2359304 | tf_op jit(solution)/shard_map/ppermute | solution.py:37
  94.6 6.8 %copy-start.5 = (bf16[256,1024]{1,0:T(8,128)(2,1)S(1)}, bf16[256,1024]{1,0:T(8,128)(2,1)}, u32[]{:S(2)}) copy-start(bf16[256,1024]{1,0:T(8,128)(2,1)} %param.11) | copy-start | bytes 1572868
  94.6 51.5 %all-to-all-start.1 = ((bf16[64,8,1536]{2,1,0:T(8,128)(2,1)}), bf16[64,8,1536]{2,1,0:T(8,128)(2,1)S(1)}, u32[]{:S(2)}, u32[]{:S(2)}) async-start(bf16[64,8,1536]{2,1,0:T(8,128)(2,1)} %fusion), calls=%async_computation.1 | async-start | bytes 3145728 | tf_op jit(solution)/shard_map/all_to_all | solution.py:266
  101.4 40.0 %collective-permute-start = (bf16[15,1024]{1,0:T(8,128)(2,1)S(1)}, bf16[15,1024]{1,0:T(8,128)(2,1)S(1)}, u32[]{:S(2)}, u32[]{:S(2)}) collective-permute-start(bf16[15,1024]{1,0:T(8,128)(2,1)S(1)} %slice.64), channel_id=1, source_target_pairs={{0,1},{1,2},{2,3},{3,4},{4,5},{5,6},{6,7},{7,8},{8,9},{9,10},{10,1... | collective-permute-start | bytes 92168 | tf_op jit(solution)/shard_map/ppermute | solution.py:27
  141.6 2.0 %copy-start.6 = (f32[1024]{0:T(1024)S(1)}, f32[1024]{0:T(1024)}, u32[]{:S(2)}) copy-start(f32[1024]{0:T(1024)} %param.13) | copy-start | bytes 12292
  141.6 2.2 %copy-start.7 = (bf16[1024,2048]{1,0:T(8,128)(2,1)S(1)}, bf16[1024,2048]{1,0:T(8,128)(2,1)}, u32[]{:S(2)}) copy-start(bf16[1024,2048]{1,0:T(8,128)(2,1)} %param.14) | copy-start | bytes 12582916
  146.0 1.2 copy-start.4

commit v2 on v1

v2 whole, which is shorter than its diff:
```python
from functools import partial

import jax
import jax.numpy as jnp
from jax import lax
from jax.experimental import pallas as pl
from jax.experimental.pallas import tpu as pltpu
from jax.sharding import PartitionSpec as P


GDIM = 128
WMAX = 16
K = 2
EPS = 0.05

CHUNKS = 2
SLOTS = 3
SUB = 8
LANES = 768
PIECE = 256
FOLD = LANES // PIECE
MAIN = 2 * LANES
WIDTH = MAIN + 2 * PIECE
GROUP = 128
DENSE = GROUP // SUB * SLOTS
BF16 = jnp.bfloat16
F32 = jnp.float32
VMEM = pl.BlockSpec(memory_space=pltpu.VMEM)


def passed_along(array, axis, by):
    length = lax.axis_size(axis)
    pairs = [(i, i + by) for i in range(length) if 0 <= i + by < length]
    return lax.ppermute(array, axis, pairs)


def swapped(array, flip):
    eps, tps = lax.axis_size("ep"), lax.axis_size("tp")
    pairs = []
    for e in range(eps):
        for y in range(tps):
            other = y ^ 1 if (e + flip) % 2 == 0 else tps - 1 - y
            pairs.append((e * tps + y, e * tps + other))
    return lax.ppermute(array, ("ep", "tp"), pairs)


def window_sizes(width):
    group_of = jnp.arange(width) // GDIM
    level = group_of % 4
    return jnp.where(
        level == 0, 2.0, jnp.where(level == 1, 4.0, jnp.where(level == 2, 8.0, 16.0))
    ).astype(F32)


def pooled_rows(extended, positions):
    extent = extended.shape[0] - (WMAX - 1)
    window = window_sizes(extended.shape[1])
    running = jnp.zeros((extent, extended.shape[1]), F32)
    picked = running
    for offset in range(WMAX):
        running = running + extended[WMAX - 1 - offset : WMAX - 1 - offset + extent]
        if offset + 1 in (2, 4, 8, 16):
            picked = jnp.where(window[None, :] == offset + 1, running, picked)
    counted = jnp.minimum(positions[:, None] + 1.0, window[None, :])
    return (picked / counted - extended[WMAX - 1 :]).astype(BF16)


def as_bf16(mask):
    return mask.astype(F32).astype(BF16)


def dot(a, b):
    return jnp.dot(a, b, preferred_element_type=F32)


def slot_ranks(routes_ref, rows, tokens, base):
    first, second = routes_ref[0:1, :], routes_ref[1:2, :]
    row = lax.broadcasted_iota(jnp.int32, (rows, tokens), 0)
    expert, sub = row // SUB, row % SUB
    by_first, by_second = expert == first, expert == second
    named = by_first | by_second
    before = lax.broadcasted_iota(jnp.int32, (tokens, tokens), 0) < lax.broadcasted_iota(
        jnp.int32, (tokens, tokens), 1
    )
    rank = dot(as_bf16(named), as_bf16(before)).astype(jnp.int32) - base
    return by_first, named, rank, sub


def main_place(sub, slot, half):
    return (sub == 2 * slot + half) & (sub < 2 * SLOTS) & (slot >= 0)


def tail_place(sub, slot, piece, c):
    return (sub >= 2 * SLOTS) & ((sub - 2 * SLOTS) * FOLD + c == 2 * slot + piece) & (slot >= 0)


def tail_used(piece, c):
    return any((r * FOLD + c - piece) % 2 == 0 for r in range(SUB - 2 * SLOTS))


def send_kernel(base, own_ref, rows_ref, gain_ref, routes_ref, out_ref):
    del own_ref
    tokens = rows_ref.shape[0]
    features = rows_ref[...].astype(F32)
    inverse = lax.rsqrt(jnp.mean(features * features, axis=-1, keepdims=True) + EPS)
    normed = (features * inverse * gain_ref[...]).astype(BF16)
    _, named, rank, sub = slot_ranks(routes_ref, out_ref.shape[0], tokens, base)
    low = as_bf16(named & main_place(sub, rank, 0))
    high = as_bf16(named & main_place(sub, rank, 1))
    for c in range(FOLD):
        columns = slice(c * PIECE, (c + 1) * PIECE)
        total = dot(low, normed[:, columns]) + dot(high, normed[:, LANES:][:, columns])
        for u in range(2):
            if tail_used(u, c):
                tail = as_bf16(named & tail_place(sub, rank, u, c))
                total += dot(tail, normed[:, MAIN + u * PIECE : MAIN + (u + 1) * PIECE])
        out_ref[:, columns] = total.astype(BF16)


def send_rows(expert_in, gain, routes_t, own, experts, chunk):
    tokens = expert_in.shape[0] // lax.axis_size("tp")
    width = expert_in.shape[1]
    return pl.pallas_call(
        partial(send_kernel, chunk * SLOTS),
        out_shape=jax.ShapeDtypeStruct((experts * SUB, LANES), BF16),
        grid_spec=pltpu.PrefetchScalarGridSpec(
            num_scalar_prefetch=1,
            grid=(1,),
            in_specs=[
                pl.BlockSpec((tokens, width), lambda i, own: (own[0], 0)),
                pl.BlockSpec((1, width), lambda i, own: (0, 0)),
                pl.BlockSpec((K, tokens), lambda i, own: (0, own[0])),
            ],
            out_specs=pl.BlockSpec((experts * SUB, LANES), lambda i, own: (0, 0)),
        ),
        cost_estimate=pl.CostEstimate(flops=2_000_000_000, bytes_accessed=2_100_000, transcendentals=128),
        name="send_rows",
    )(own, expert_in, gain.reshape(1, width), routes_t)


def group_place(shape, dense_axis, where):
    dense = lax.broadcasted_iota(jnp.int32, shape, dense_axis)
    row = lax.broadcasted_iota(jnp.int32, shape, 1 - dense_axis)
    return as_bf16((dense // SLOTS == row // SUB) & where(row % SUB, dense % SLOTS))


def ffn_kernel(x_ref, ga_ref, gb_ref, ua_ref, ub_ref, da_ref, db_ref, out_ref, dense_ref, total_ref):
    groups = x_ref.shape[0] // GROUP
    gather = partial(group_place, (DENSE, GROUP), 0)
    mains = [gather(lambda sub, slot, h=h: main_place(sub, slot, h)) for h in range(2)]
    tails = {
        (u, c): gather(lambda sub, slot, u=u, c=c: tail_place(sub, slot, u, c))
        for u in range(2)
        for c in range(FOLD)
        if tail_used(u, c)
    }
    for g in range(groups):
        rows, dense = slice(g * GROUP, (g + 1) * GROUP), slice(g * DENSE, (g + 1) * DENSE)
        for h in range(2):
            dense_ref[dense, h * LANES : (h + 1) * LANES] = dot(mains[h], x_ref[rows, :]).astype(BF16)
        for u in range(2):
            dense_ref[dense, MAIN + u * PIECE : MAIN + (u + 1) * PIECE] = sum(
                dot(tails[u, c], x_ref[rows, c * PIECE : (c + 1) * PIECE])
                for c in range(FOLD)
                if (u, c) in tails
            ).astype(BF16)
    x = dense_ref[...]
    hidden_a = (jax.nn.silu(dot(x, ga_ref[...])) * dot(x, ua_ref[...])).astype(BF16)
    hidden_b = (jax.nn.silu(dot(x, gb_ref[...])) * dot(x, ub_ref[...])).astype(BF16)
    for c in range(WIDTH // PIECE):
        columns = slice(c * PIECE, (c + 1) * PIECE)
        total_ref[:, columns] = (
            dot(hidden_a, da_ref[:, columns]) + dot(hidden_b, db_ref[:, columns])
        ).astype(BF16)
    scatter = partial(group_place, (GROUP, DENSE), 1)
    mains = [scatter(lambda sub, slot, h=h: main_place(sub, slot, h)) for h in range(2)]
    tails = {
        (u, c): scatter(lambda sub, slot, u=u, c=c: tail_place(sub, slot, u, c)) for u, c in tails
    }
    for g in range(groups):
        rows, dense = slice(g * GROUP, (g + 1) * GROUP), slice(g * DENSE, (g + 1) * DENSE)
        for c in range(FOLD):
            columns = slice(c * PIECE, (c + 1) * PIECE)
            total = sum(
                dot(mains[h], total_ref[dense, h * LANES + c * PIECE : h * LANES + (c + 1) * PIECE])
                for h in range(2)
            )
            for u in range(2):
                if (u, c) in tails:
                    total += dot(
                        tails[u, c], total_ref[dense, MAIN + u * PIECE : MAIN + (u + 1) * PIECE]
                    )
            out_ref[rows, columns] = total.astype(BF16)


def half_ffn(x, ga, gb, ua, ub, da, db):
    rows = x.shape[0]
    dense = rows // SUB * SLOTS
    hidden = ga.shape[1] + gb.shape[1]
    return pl.pallas_call(
        ffn_kernel,
        out_shape=jax.ShapeDtypeStruct(x.shape, BF16),
        in_specs=[VMEM] * 7,
        out_specs=VMEM,
        scratch_shapes=[pltpu.VMEM((dense, WIDTH), BF16), pltpu.VMEM((dense, WIDTH), BF16)],
        cost_estimate=pl.CostEstimate(
            flops=3_500_000_000,
            bytes_accessed=x.size * 4 + 6 * ga.size * 2,
            transcendentals=dense * hidden,
        ),
        compiler_params=pltpu.CompilerParams(vmem_limit_bytes=24 * 1024 * 1024),
        name="half_ffn",
    )(x, ga, gb, ua, ub, da, db)


def combine_kernel(own_ref, first_ref, second_ref, routes_ref, weight_ref, out_ref):
    del own_ref
    rows, tokens = first_ref.shape[0], out_ref.shape[0]
    by_first, named, rank, sub = slot_ranks(routes_ref, rows, tokens, 0)
    weight = jnp.where(by_first, weight_ref[0:1, :], weight_ref[1:2, :])

    def split(chosen):
        picked = jnp.where(chosen, weight, 0.0).T
        high = picked.astype(BF16)
        return high, (picked - high.astype(F32)).astype(BF16)

    parts = [[] for _ in range(WIDTH // PIECE)]
    for chunk, ref in enumerate((first_ref, second_ref)):
        slot = rank - chunk * SLOTS
        here = named & (slot < SLOTS)
        for h in range(2):
            chosen = split(here & main_place(sub, slot, h))
            for c in range(FOLD):
                parts[h * FOLD + c].append((chosen, ref, c))
        for u in range(2):
            for c in range(FOLD):
                if tail_used(u, c):
                    parts[2 * FOLD + u].append((split(here & tail_place(sub, slot, u, c)), ref, c))
    for j, terms in enumerate(parts):
        total = 0.0
        for (high, low), ref, c in terms:
            values = ref[:, c * PIECE : (c + 1) * PIECE]
            total += dot(high, values) + dot(low, values)
        out_ref[:, j * PIECE : (j + 1) * PIECE] = total.astype(BF16)


def combine(values, routes_t, weight_t, own, tokens):
    return pl.pallas_call(
        combine_kernel,
        out_shape=jax.ShapeDtypeStruct((tokens, WIDTH), BF16),
        grid_spec=pltpu.PrefetchScalarGridSpec(
            num_scalar_prefetch=1,
            grid=(1,),
            in_specs=[
                VMEM,
                VMEM,
                pl.BlockSpec((K, tokens), lambda i, own: (0, own[0])),
                pl.BlockSpec((K, tokens), lambda i, own: (0, own[0])),
            ],
            out_specs=pl.BlockSpec((tokens, WIDTH), lambda i, own: (0, 0)),
        ),
        cost_estimate=pl.CostEstimate(flops=2_000_000_000, bytes_accessed=2_100_000, transcendentals=0),
        compiler_params=pltpu.CompilerParams(vmem_limit_bytes=24 * 1024 * 1024),
        name="combine",
    )(own, *values, routes_t, weight_t)


def exchanged(rows):
    experts = rows.shape[0] // SUB
    out = lax.all_to_all(
        rows.reshape(experts, SUB, LANES), "ep", split_axis=0, concat_axis=0, tiled=True
    )
    return out.reshape(rows.shape)


def on_device(
    pool_in,
    w_pool,
    pool_scale,
    w_out,
    expert_in,
    ffn_gain,
    routes,
    route_weight,
    w_gate,
    w_up,
    w_down,
):
    rows_here = pool_in.shape[0]
    tokens = routes.shape[0] // lax.axis_size("tp")
    experts = lax.axis_size("ep") * w_gate.shape[0]
    own = lax.axis_index("tp").astype(jnp.int32).reshape(1)
    routes_t, weight_t = routes.T, route_weight.T
    before = passed_along(pool_in[rows_here - (WMAX - 1) :], ("ep", "tp"), 1)

    gate, up, down = w_gate[0], w_up[0], w_down[0]
    gate_b, up_b, down_b = swapped(gate, 0), swapped(up, 0), swapped(down, 0)
    ffn = lambda x: half_ffn(x, gate, gate_b, up, up_b, down, down_b)

    mine, back, kept, results, returned = [], [], [], [], []
    for n in range(CHUNKS):
        sent = send_rows(expert_in, ffn_gain, routes_t, own, experts, n)
        mine.append(exchanged(sent))
    for n in range(CHUNKS):
        theirs = swapped(mine[n], 1)
        partial_sum = ffn(theirs)
        back.append(swapped(partial_sum, 1))
        kept.append(ffn(mine[n]))
    for n in range(CHUNKS):
        results.append((kept[n].astype(F32) + back[n].astype(F32)).astype(BF16))
        returned.append(exchanged(results[n]))
    expert_out = combine(returned, routes_t, weight_t, own, tokens)

    extended = jnp.concatenate([before, pool_in], axis=0).astype(F32)
    positions = (
        lax.axis_index(("ep", "tp")) * rows_here + jnp.arange(rows_here)
    ).astype(F32)
    pooled = pooled_rows(extended, positions)
    group_count = w_pool.shape[0]
    grouped = jnp.einsum(
        "tgc,gcd->tgd",
        pooled.reshape(rows_here, group_count, GDIM),
        w_pool,
        preferred_element_type=F32,
    )
    scaled = (grouped.reshape(rows_here, -1) * pool_scale).astype(BF16)
    mixer_out = dot(scaled, w_out).astype(BF16)
    return (mixer_out, expert_out)


def solution(mesh):
    placed = (
        P(("ep", "tp"), None),
        P(),
        P(),
        P(),
        P("ep", None),
        P(),
        P("ep", None),
        P("ep", None),
        P("ep", None, "tp"),
        P("ep", None, "tp"),
        P("ep", "tp", None),
    )
    return jax.shard_map(
        on_device,
        mesh=mesh,
        in_specs=placed,
        out_specs=(P(("ep", "tp"), None), P(("ep", "tp"), None)),
        check_vma=False,
    )
```

time: 151 us -> 155 us (1.026)
  the two profiles are of different devices: /device:TPU:96 before, /device:TPU:1 now
where the time goes in v2:
time: 155 us
  waiting for transfers between devices  58.4 us (38%)
  starting transfers between devices  53.4 us (34%)
  Pallas kernels  33.1 us (21%)
  other arithmetic  4.77 us (3%)
  matrix products  4.18 us (3%)
    all_to_all x4, starting transfers between devices, exchanged(): lax.all_to_all(rows.reshape(experts, SUB, LANES), 'ep', split_axis=0, con...  41.6 us
    all_to_all x4, waiting for transfers between devices, exchanged(): lax.all_to_all(rows.reshape(experts, SUB, LANES), 'ep', split_axis=0, con...  35.5 us
    pallas_call x4, Pallas kernels, half_ffn(): pl.pallas_call(ffn_kernel, out_shape=jax.ShapeDtypeStruct(x.shape, BF16),...  23.1 us
    ppermute x7, waiting for transfers between devices, swapped(): return lax.ppermute(array, ('ep', 'tp'), pairs)  22.9 us
    ppermute x7, starting transfers between devices, swapped(): return lax.ppermute(array, ('ep', 'tp'), pairs)  8.45 us
    pallas_call x2, Pallas kernels, send_rows(): pl.pallas_call(partial(send_kernel, chunk * SLOTS), out_shape=jax.ShapeDt...  6.53 us
    reshape x2, other arithmetic, exchanged(): rows.reshape(experts, SUB, LANES)  4.39 us
    pallas_call x1, Pallas kernels, combine(): pl.pallas_call(combine_kernel, out_shape=jax.ShapeDtypeStruct((tokens, WI...  3.46 us
  transfers between devices with their start and end apart: 12, of which 7 were waited for; matrix products, arithmetic and copies ran while one was open for 6% of the time, Pallas kernels for 17%

profile of v2, /device:TPU:1, one launch (start us, length us, event | category | flops | bytes accessed | tf_op | source)
XLA Modules:
  0.0 154.7 jit_solution(13633034256513646134)
XLA Ops:
  0.6 3.3 %send_rows.3 = bf16[512,768]{1,0:T(8,128)(2,1)} custom-call(s32[1]{0:T(128)} %bitcast.2.own_ref, bf16[512,2048]{1,0:T(8,128)(2,1)} %rows_ref.3, f32[1,2048]{1,0:T(1,128)} %bitcast.50, s32[2,512]{1,0:T(2,128)} %bitcast.44), custom_call_target="tpu_custom_call" | custom-call | flops 2000000000 | bytes 2100000 | tf_op jit(solution)/shard_map/send_rows/pallas_call | solution.py:123
  3.9 13.1 %all-to-all-start.2 = ((bf16[64,8,768]{2,1,0:T(8,128)(2,1)}), bf16[64,8,768]{2,1,0:T(8,128)(2,1)S(1)}, u32[]{:S(2)}, u32[]{:S(2)}) async-start(bf16[64,8,768]{2,1,0:T(8,128)(2,1)} %bitcast.49), calls=%async_computation.2 | async-start | bytes 1572864 | tf_op jit(solution)/shard_map/all_to_all | solution.py:270
  17.1 2.8 %collective-permute-start.1 = (bf16[2048,256]{1,0:T(8,128)(2,1)S(1)}, bf16[2048,256]{1,0:T(8,128)(2,1)}, u32[]{:S(2)}, u32[]{:S(2)}) collective-permute-start(bf16[2048,256]{1,0:T(8,128)(2,1)S(1)} %bitcast.39), channel_id=1, source_target_pairs={{0,1},{1,0},{2,3},{3,2},{4,7},{5,6},{6,5},{7,4},{8,9},{9,8},{10,11... | collective-permute-start | bytes 3145736 | tf_op jit(solution)/shard_map/ppermute | solution.py:44
  20.0 2.6 %collective-permute-start.3 = (bf16[256,2048]{1,0:T(8,128)(2,1)}, bf16[256,2048]{1,0:T(8,128)(2,1)}, u32[]{:S(2)}, u32[]{:S(2)}) collective-permute-start(bf16[256,2048]{1,0:T(8,128)(2,1)} %bitcast.9.da_ref), channel_id=1, source_target_pairs={{0,1},{1,0},{2,3},{3,2},{4,7},{5,6},{6,5},{7,4},{8,9},{9,8},{10,11... | collective-permute-start | bytes 3145736 | tf_op jit(solution)/shard_map/ppermute | solution.py:44
  22.6 3.2 %send_rows.2 = bf16[512,768]{1,0:T(8,128)(2,1)} custom-call(s32[1]{0:T(128)} %bitcast.2.own_ref, bf16[512,2048]{1,0:T(8,128)(2,1)} %rows_ref.3, f32[1,2048]{1,0:T(1,128)} %bitcast.51, s32[2,512]{1,0:T(2,128)} %bitcast.45), custom_call_target="tpu_custom_call" | custom-call | flops 2000000000 | bytes 2100000 | tf_op jit(solution)/shard_map/send_rows/pallas_call | solution.py:123
  25.8 14.3 %all-to-all-done.2 = bf16[64,8,768]{2,1,0:T(8,128)(2,1)S(1)} async-done(((bf16[64,8,768]{2,1,0:T(8,128)(2,1)}), bf16[64,8,768]{2,1,0:T(8,128)(2,1)S(1)}, u32[]{:S(2)}, u32[]{:S(2)}) %all-to-all-start.2) | async-done | bytes 786464 | tf_op jit(solution)/shard_map/all_to_all | solution.py:270
  40.1 5.9 %all-to-all-start = ((bf16[64,8,768]{2,1,0:T(8,128)(2,1)}), bf16[64,8,768]{2,1,0:T(8,128)(2,1)S(1)}, u32[]{:S(2)}, u32[]{:S(2)}) async-start(bf16[64,8,768]{2,1,0:T(8,128)(2,1)} %bitcast.48), calls=%async_computation | async-start | bytes 1572864 | tf_op jit(solution)/shard_map/all_to_all | solution.py:270
  47.4 11.4 %collective-permute-done.3.db_ref = bf16[256,2048]{1,0:T(8,128)(2,1)} collective-permute-done((bf16[256,2048]{1,0:T(8,128)(2,1)}, bf16[256,2048]{1,0:T(8,128)(2,1)}, u32[]{:S(2)}, u32[]{:S(2)}) %collective-permute-start.3) | collective-permute-done | bytes 1048608 | tf_op jit(solution)/shard_map/ppermute | solution.py:44
  58.8 4.1 %collective-permute-done.6.x_ref = bf16[512,768]{1,0:T(8,128)(2,1)S(1)} collective-permute-done((bf16[512,768]{1,0:T(8,128)(2,1)S(1)}, bf16[512,768]{1,0:T(8,128)(2,1)S(1)}, u32[]{:S(2)}, u32[]{:S(2)}) %collective-permute-start.6) | collective-permute-done | bytes 786464 | tf_op jit(solution)/shard_map/ppermute | solution.py:44
  62.9 6.1 %half_ffn.7 = bf16[512,768]{1,0:T(8,128)(2,1)} custom-call(bf16[512,768]{1,0:T(8,128)(2,1)S(1)} %collective-permute-done.6.x_ref, bf16[2048,256]{1,0:T(8,128)(2,1)S(1)} %bitcast.40, bf16[2048,256]{1,0:T(8,128)(2,1)} %collective-permute-done.1.gb_ref, bf16[2048,256]{1,0:T(8,128)(2,1)} %bitcast.8.ua_ref, bf16[2048,256]{1,0:T(8,128)(2,1)} %collective-permute-done.2.ub_ref, ...), custom_call_target="tpu_custom_call" | custom-call | flops 3500000000 | bytes 7864320 | tf_op jit(solution)/shard_map/half_ffn/pallas_call | solution.py:200
  70.6 5.3 %half_ffn.6 = bf16[512,768]{1,0:T(8,128)(2,1)S(1)} custom-call(bf16[512,768]{1,0:T(8,128)(2,1)S(1)} %bitcast.37, bf16[2048,256]{1,0:T(8,128)(2,1)S(1)} %bitcast.41, bf16[2048,256]{1,0:T(8,128)(2,1)} %collective-permute-done.1.gb_ref, bf16[2048,256]{1,0:T(8,128)(2,1)} %bitcast.8.ua_ref, bf16[2048,256]{1,0:T(8,128)(2,1)} %collective-permute-done.2.ub_ref, ...), custom_call_target="tpu_custom_call" | custom-call | flops 3500000000 | bytes 7864320 | tf_op jit(solution)/shard_map/half_ffn/pallas_call | solution.py:200
  75.9 4.6 %collective-permute-done.7 = bf16[512,768]{1,0:T(8,128)(2,1)} collective-permute-done((bf16[512,768]{1,0:T(8,128)(2,1)}, bf16[512,768]{1,0:T(8,128)(2,1)}, u32[]{:S(2)}, u32[]{:S(2)}) %collective-permute-start.7) | collective-permute-done | bytes 786464 | tf_op jit(solution)/shard_map/ppermute | solution.py:44
  80.5 2.2 %fusion.6 = bf16[64,8,768]{2,1,0:T(8,128)(2,1)} fusion(bf16[512,768]{1,0:T(8,128)(2,1)} %collective-permute-done.7, bf16[512,768]{1,0:T(8,128)(2,1)S(1)} %half_ffn.6), kind=kLoop, calls=%fused_computation.25 | loop fusion | flops 1572864 | bytes 2359296 | tf_op jit(solution)/shard_map/reshape | solution.py:271
  82.7 12.7 %all-to-all-start.3 = ((bf16[64,8,768]{2,1,0:T(8,128)(2,1)}), bf16[64,8,768]{2,1,0:T(8,128)(2,1)S(1)}, u32[]{:S(2)}, u32[]{:S(2)}) async-start(bf16[64,8,768]{2,1,0:T(8,128)(2,1)} %fusion.6), calls=%async_computation.3 | async-start | bytes 1572864 | tf_op jit(solution)/shard_map/all_to_all | solution.py:270
  95.5 6.4 %half_ffn.5 = bf16[512,768]{1,0:T(8,128)(2,1)} custom-call(bf16[512,768]{1,0:T(8,128)(2,1)} %collective-permute-done.4.x_ref, bf16[2048,256]{1,0:T(8,128)(2,1)S(1)} %bitcast.42, bf16[2048,256]{1,0:T(8,128)(2,1)} %collective-permute-done.1.gb_ref, bf16[2048,256]{1,0:T(8,128)(2,1)} %bitcast.8.ua_ref, bf16[2048,256]{1,0:T(8,128)(2,1)} %collective-permute-done.2.ub_ref, ...), custom_call_target="tpu_custom_call" | custom-call | flops 3500000000 | bytes 7864320 | tf_op jit(solution)/shard_map/half_ffn/pallas_call | solution.py:200
  101.9 3.4 %collective-permute-start = (bf16[15,1024]{1,0:T(8,128)(2,1)S(1)}, bf16[15,1024]{1,0:T(8,128)(2,1)S(1)}, u32[]{:S(2)}, u32[]{:S(2)}) collective-permute-start(bf16[15,1024]{1,0:T(8,128)(2,1)S(1)} %slice.52), channel_id=1, source_target_pairs={{0,1},{1,2},{2,3},{3,4},{4,5},{5,6},{6,7},{7,8},{8,9},{9,10},{10,1... | collective-permute-start | bytes 92168 | tf_op jit(solution)/shard_map/ppermute | solution.py:34
  105.4 5.3 %half_ffn.4 = bf16[512,768]{1,0:T(8,128)(2,1)S(1)} custom-call(bf16[512,768]{1,0:T(8,128)(2,1)S(1)} %bitcast.34, bf16[2048,256]{1,0:T(8,128)(2,1)S(1)} %bitcast.43, bf16[2048,256]{1,0:T(8,128)(2,1)} %collective-permute-done.1.gb_ref, bf16[2048,256]{1,0:T(8,128)(2,1)} %bitcast.8.ua_ref, bf16[2048,256]{1,0:T(8,128)(2,1)} %collective-permute-done.2.ub_ref, ...), custom_call_target="tpu_custom_call" | custom-call | flops 3500000000 | bytes 7864320 | tf_op jit(solution)/shard_map/half_ffn/pallas_call | solution.py:200
  110.6 2.7 %collective-permute-done.5 = bf16[512,768]{1,0:T(8,128)(2,1)} collective-permute-done((bf16[512,768]{1,0:T(8,128)(2,1)}, bf16[512,768]{1,0:T(8,128)(2,1)}, u32[]{:S(2)}, u32[]{:S(2)}) %collective-permute-start.5) | collective-permute-done | bytes 786464 | tf_op jit(solution)/shard_map/ppermute | solution.py:44
  113.3 2.2 %fusion.5 = bf16[64,8,768]{2,1,0:T(8,128)(2,1)} fusion(bf16[512,768]{1,0:T(8,128)(2,1)} %collective-permute-done.5, bf16[512,768]{1,0:T(8,128)(2,1)S(1)} %half_ffn.4), kind=kLoop, calls=%fused_computation.24 | loop fusion | flops 1572864 | bytes 2359296 | tf_op jit(solution)/shard_map/reshape | solution.py:271
  115.5 2.9 %all-to-all-done.3 = bf16[64,8,768]{2,1,0:T(8,128)(2,1)S(1)} async-done(((bf16[64,8,768]{2,1,0:T(8,128)(2,1)}), bf16[64,8,768]{2,1,0:T(8,128)(2,1)S(1)}, u32[]{:S(2)}, u32[]{:S(2)}) %all-to-all-start.3) | async-done | bytes 786464 | tf_op jit(solution)/shard_map/all_to_all | solution.py:270
  118.4 9.8 %all-to-all-start.1 = ((bf16[64,8,768]{2,1,0:T(8,128)(2,1)}), bf16[64,8,768]{2,1,0:T(8,128)(2,1)S(1)}, u32[]{:S(2)}, u32[]{:S(2)}) async-start(bf16[64,8,768]{2,1,0:T(8,128)(2,1)} %fusion.5), calls=%async_computation.1 | async-start | bytes 1572864 | tf_op jit(solution)/shard_map/all_to_all | solution.py:270
  130.7 2.2 %convolution_convert_fusion = bf16[256,2048]{1,0:T(8,128)(2,1)} fusion(bf16[256,1024]{0,1:T(8,128)(2,1)S(1)} %fusion.3, bf16[1024,2048]{1,0:T(8,128)(2,1)S(1)} %copy-done.6), kind=kOutput, calls=%fused_computation | convolution fusion | flops 1074266112 | bytes 5767168 | tf_op jit(solution)/shard_map/dot_general | solution.py:73
  132.9 18.4 %all-to-all-done.1 = bf16[64,8,768]{2,1,0:T(8,128)(2,1)S(1)} async-done(((bf16[64,8,768]{2,1,0:T(8,128)(2,1)}), bf16[64,8,768]{2,1,0:T(8,128)(2,1)S(1)}, u32[]{:S(2)}, u32[]{:S(2)}) %all-to-all-start.1) | async-done | bytes 786464 | tf_op jit(solution)/shard_map/all_to_all | solution.py:270
  151.3 3.5 %combine.1 = bf16[128,2048]{1,0:T(8,128)(2,1)} custom-call(s32[1]{0:T(128)} %bitcast.2.own_ref, bf16[512,768]{1,0:T(8,128)(2,1)S(1)} %bitcast.38, bf16[512,768]{1,0:T(8,128)(2,1)S(1)} %bitcast.35, s32[2,512]{1,0:T(2,128)S(1)} %bitcast.46, f32[2,512]{1,0:T(2,128)S(1)} %bitcast.47), custom_call_target="tpu_custom_call" | custom-call | flops 2000000000 | bytes 2100000 | tf_op jit(solution)/shard_map/combine/pallas_call | solution.py:248
  (32 shorter events, 5.4 us)
Async XLA Ops:
  0.6 127.8 %copy-start = (bf16[8,128,128]{2,1,0:T(8,128)(2,1)S(1)}, bf16[8,128,128]{2,1,0:T(8,128)(2,1)}, u32[]{:S(2)}) copy-start(bf16[8,128,128]{2,1,0:T(8,128)(2,1)} %param.12) | copy-start | bytes 786436
  3.9 13.1 %copy-start.1 = (bf16[1,2048,256]{2,1,0:T(8,128)(2,1)S(1)}, bf16[1,2048,256]{2,1,0:T(8,128)(2,1)}, u32[]{:S(2)}) copy-start(bf16[1,2048,256]{2,1,0:T(8,128)(2,1)} %param.19) | copy-start | bytes 3145732
  3.9 36.1 %all-to-all-start.2 = ((bf16[64,8,768]{2,1,0:T(8,128)(2,1)}), bf16[64,8,768]{2,1,0:T(8,128)(2,1)S(1)}, u32[]{:S(2)}, u32[]{:S(2)}) async-start(bf16[64,8,768]{2,1,0:T(8,128)(2,1)} %bitcast.49), calls=%async_computation.2 | async-start | bytes 1572864 | tf_op jit(solution)/shard_map/all_to_all | solution.py:270
  17.1 30.3 %collective-permute-start.1 = (bf16[2048,256]{1,0:T(8,128)(2,1)S(1)}, bf16[2048,256]{1,0:T(8,128)(2,1)}, u32[]{:S(2)}, u32[]{:S(2)}) collective-permute-start(bf16[2048,256]{1,0:T(8,128)(2,1)S(1)} %bitcast.39), channel_id=1, source_target_pairs={{0,1},{1,0},{2,3},{3,2},{4,7},{5,6},{6,5},{7,4},{8,9},{9,8},{10,11... | collective-permute-start | bytes 3145736 | tf_op jit(solution)/shard_map/ppermute | solution.py:44
  19.9 27.5 %collective-permute-start.2 = (bf16[2048,256]{1,0:T(8,128)(2,1)}, bf16[2048,256]{1,0:T(8,128)(2,1)}, u32[]{:S(2)}, u32[]{:S(2)}) collective-permute-start(bf16[2048,256]{1,0:T(8,128)(2,1)} %bitcast.8.ua_ref), channel_id=1, source_target_pairs={{0,1},{1,0},{2,3},{3,2},{4,7},{5,6},{6,5},{7,4},{8,9},{9,8},{10,11... | collective-permute-start | bytes 3145736 | tf_op jit(solution)/shard_map/ppermute | solution.py:44
  20.0 38.8 %collective-permute-start.3 = (bf16[256,2048]{1,0:T(8,128)(2,1)}, bf16[256,2048]{1,0:T(8,128)(2,1)}, u32[]{:S(2)}, u32[]{:S(2)}) collective-permute-start(bf16[256,2048]{1,0:T(8,128)(2,1)} %bitcast.9.da_ref), channel_id=1, source_target_pairs={{0,1},{1,0},{2,3},{3,2},{4,7},{5,6},{6,5},{7,4},{8,9},{9,8},{10,11... | collective-permute-start | bytes 3145736 | tf_op jit(solution)/shard_map/ppermute | solution.py:44
  40.1 30.3 %all-to-all-start = ((bf16[64,8,768]{2,1,0:T(8,128)(2,1)}), bf16[64,8,768]{2,1,0:T(8,128)(2,1)S(1)}, u32[]{:S(2)}, u32[]{:S(2)}) async-start(bf16[64,8,768]{2,1,0:T(8,128)(2,1)} %bitcast.48), calls=%async_computation | async-start | bytes 1572864 | tf_op jit(solution)/shard_map/all_to_all | solution.py:270
  46.0 16.9 %collective-permute-start.6 = (bf16[512,768]{1,0:T(8,128)(2,1)S(1)}, bf16[512,768]{1,0:T(8,128)(2,1)S(1)}, u32[]{:S(2)}, u32[]{:S(2)}) collective-permute-start(bf16[512,768]{1,0:T(8,128)(2,1)S(1)} %bitcast.36), channel_id=1, source_target_pairs={{0,3},{1,2},{2,1},{3,0},{4,5},{5,4},{6,7},{7,6},{8,11},{9,10},{10,... | collective-permute-start | bytes 2359304 | tf_op jit(solution)/shard_map/ppermute | solution.py:44
  69.1 11.5 %collective-permute-start.7 = (bf16[512,768]{1,0:T(8,128)(2,1)}, bf16[512,768]{1,0:T(8,128)(2,1)}, u32[]{:S(2)}, u32[]{:S(2)}) collective-permute-start(bf16[512,768]{1,0:T(8,128)(2,1)} %half_ffn.7), channel_id=1, source_target_pairs={{0,3},{1,2},{2,1},{3,0},{4,5},{5,4},{6,7},{7,6},{8,11},{9,10},{10,... | collective-permute-start | bytes 2359304 | tf_op jit(solution)/shard_map/ppermute | solution.py:44
  70.4 25.1 %collective-permute-start.4 = (bf16[512,768]{1,0:T(8,128)(2,1)S(1)}, bf16[512,768]{1,0:T(8,128)(2,1)}, u32[]{:S(2)}, u32[]{:S(2)}) collective-permute-start(bf16[512,768]{1,0:T(8,128)(2,1)S(1)} %bitcast.33), channel_id=1, source_target_pairs={{0,3},{1,2},{2,1},{3,0},{4,5},{5,4},{6,7},{7,6},{8,11},{9,10},{10,... | collective-permute-start | bytes 2359304 | tf_op jit(solution)/shard_map/ppermute | solution.py:44
  82.7 35.7 %all-to-all-start.3 = ((bf16[64,8,768]{2,1,0:T(8,128)(2,1)}), bf16[64,8,768]{2,1,0:T(8,128)(2,1)S(1)}, u32[]{:S(2)}, u32[]{:S(2)}) async-start(bf16[64,8,768]{2,1,0:T(8,128)(2,1)} %fusion.6), calls=%async_computation.3 | async-start | bytes 1572864 | tf_op jit(solution)/shard_map/all_to_all | solution.py:270
  95.4 6.5 %copy-start.4 = (bf16[256,1024]{1,0:T(8,128)(2,1)S(1)}, bf16[256,1024]{1,0:T(8,128)(2,1)}, u32[]{:S(2)}) copy-start(bf16[256,1024]{1,0:T(8,128)(2,1)} %param.11) | copy-start | bytes 1572868
  101.9 11.5 %collective-permute-start.5 = (bf16[512,768]{1,0:T(8,128)(2,1)}, bf16[512,768]{1,0:T(8,128)(2,1)}, u32[]{:S(2)}, u32[]{:S(2)}) collective-permute-start(bf16[512,768]{1,0:T(8,128)(2,1)} %half_ffn.5), channel_id=1, source_target_pairs={{0,3},{1,2},{2,1},{3,0},{4,5},{5,4},{6,7},{7,6},{8,11},{9,10},{10,... | collective-permute-start | bytes 2359304 | tf_op jit(solution)/shard_map/ppermute | solution.py:44
  101.9 26.4 %collective-permute-start = (bf16[15,1024]{1,0:T(8,128)(2,1)S(1)}, bf16[15,1024]{1,0:T(8,128)(2,1)S(1)}, u32[]{:S(2)}, u32[]{:S(2)}) collective-permute-start(bf16[15,1024]{1,0:T(8,128)(2,1)S(1)} %slice.52), channel_id=1, source_target_pairs={{0,1},{1,2},{2,3},{3,4},{4,5},{5,6},{6,7},{7,8},{8,9},{9,10},{10,1... | collective-permute-start | bytes 92168 | tf_op jit(solution)/shard_map/ppermute | solution.py:34
  118.4 32.8 %all-to-all-start.1 = ((bf16[64,8,768]{2,1,0:T(8,128)(2,1)}), bf16[64,8,768]{2,1,0:T(8,128)(2,1)S(1)}, u32[]{:S(2)}, u32[]{:S(2)}) async-start(bf16[64,8,768]{2,1,0:T(8,128)(2,1)} %fusion.5), calls=%async_computation.1 | async-start | bytes 1572864 | tf_op jit(solution)/shard_map/all_to_all | solution.py:270
  128.4 2.0 %copy-start.5 = (f32[1024]{0:T(1024)S(1)}, f32[1024]{0:T(1024)}, u32[]{:S(2)}) copy-start(f32[1024]{0:T(1024)} %param.13) | copy-start | bytes 12292
  128.5 2.2 %copy-start.6 = (bf16[1024,2048]{1,0:T(8,128)(2,1)S(1)}, bf16[1024,2048]{1,0:T(8,128)(2,1)}, u32[]{:S(2)}) copy-start(bf16[1024,2048]{1,0:T(8,128)(2,1)} %param.14) | copy-start | bytes 12582916
  130.7 20.6 %copy-start.2 = (s32[512,2]{0,1:T(2,128)S(1)}, s32[512,2]{0,1:T(2,128)}, u32[]{:S(2)}) copy-start(s32[512,2]{0,1:T(2,128)} %param.17) | copy-start | bytes 12292
  130.7 20.6 %copy-start.3 = (f32[512,2]{0,1:T(2,128)S(1)}, f32[512,2]{0,1:T(2,128)}, u32[]{:S(2)}) copy-start(f32[512,2]{0,1:T(2,128)} %param.18) | copy-start | bytes 12292

commit v3 on v2

--- a/solution.py
+++ b/solution.py
@@ -21,8 +21,10 @@
 FOLD = LANES // PIECE
 MAIN = 2 * LANES
 WIDTH = MAIN + 2 * PIECE
-GROUP = 128
-DENSE = GROUP // SUB * SLOTS
+EXPERTS_G = 32
+GROUP = EXPERTS_G * SUB
+DENSE = EXPERTS_G * SLOTS
+SMALL = 16 * 1024 * 1024
 BF16 = jnp.bfloat16
 F32 = jnp.float32
 VMEM = pl.BlockSpec(memory_space=pltpu.VMEM)
@@ -138,131 +140,184 @@
     )(own, expert_in, gain.reshape(1, width), routes_t)
 
 
-def group_place(shape, dense_axis, where):
+def places(shape, dense_axis, where):
     dense = lax.broadcasted_iota(jnp.int32, shape, dense_axis)
     row = lax.broadcasted_iota(jnp.int32, shape, 1 - dense_axis)
-    return as_bf16((dense // SLOTS == row // SUB) & where(row % SUB, dense % SLOTS))
-
-
-def ffn_kernel(x_ref, ga_ref, gb_ref, ua_ref, ub_ref, da_ref, db_ref, out_ref, dense_ref, total_ref):
-    groups = x_ref.shape[0] // GROUP
-    gather = partial(group_place, (DENSE, GROUP), 0)
-    mains = [gather(lambda sub, slot, h=h: main_place(sub, slot, h)) for h in range(2)]
-    tails = {
-        (u, c): gather(lambda sub, slot, u=u, c=c: tail_place(sub, slot, u, c))
-        for u in range(2)
-        for c in range(FOLD)
-        if tail_used(u, c)
-    }
-    for g in range(groups):
-        rows, dense = slice(g * GROUP, (g + 1) * GROUP), slice(g * DENSE, (g + 1) * DENSE)
-        for h in range(2):
-            dense_ref[dense, h * LANES : (h + 1) * LANES] = dot(mains[h], x_ref[rows, :]).astype(BF16)
-        for u in range(2):
-            dense_ref[dense, MAIN + u * PIECE : MAIN + (u + 1) * PIECE] = sum(
-                dot(tails[u, c], x_ref[rows, c * PIECE : (c + 1) * PIECE])
-                for c in range(FOLD)
-                if (u, c) in tails
+    return as_bf16((dense % EXPERTS_G == row // SUB) & where(row % SUB, dense // EXPERTS_G))
+
+
+def group_maps(shape, dense_axis, c):
+    maps = [places(shape, dense_axis, lambda sub, slot, h=h: main_place(sub, slot, h)) for h in range(2)]
+    for u in range(2):
+        if tail_used(u, c):
+            maps.append(places(shape, dense_axis, lambda sub, slot, u=u: tail_place(sub, slot, u, c)))
+    return maps
+
+
+def dense_columns(c):
+    starts = [h * LANES + c * PIECE for h in range(2)]
+    return starts + [MAIN + u * PIECE for u in range(2) if tail_used(u, c)]
+
+
+def unpack_kernel(x_ref, out_ref):
+    experts = x_ref.shape[0] // SUB
+    tails = {}
+    for c in range(FOLD):
+        maps = jnp.concatenate(group_maps((DENSE, GROUP), 0, c), axis=0)
+        for g in range(experts // EXPERTS_G):
+            found = dot(maps, x_ref[g * GROUP : (g + 1) * GROUP, c * PIECE : (c + 1) * PIECE])
+            for n, start in enumerate(dense_columns(c)):
+                block = found[n * DENSE : (n + 1) * DENSE]
+                if start >= MAIN:
+                    tails[start, g] = tails[start, g] + block if (start, g) in tails else block
+                    continue
+                for k in range(SLOTS):
+                    to = k * experts + g * EXPERTS_G
+                    out_ref[to : to + EXPERTS_G, start : start + PIECE] = block[
+                        k * EXPERTS_G : (k + 1) * EXPERTS_G
+                    ].astype(BF16)
+    for (start, g), block in tails.items():
+        for k in range(SLOTS):
+            to = k * experts + g * EXPERTS_G
+            out_ref[to : to + EXPERTS_G, start : start + PIECE] = block[
+                k * EXPERTS_G : (k + 1) * EXPERTS_G
+            ].astype(BF16)
+
+
+def unpack(x):
+    rows = x.shape[0] // SUB * SLOTS
+    return pl.pallas_call(
+        unpack_kernel,
+        out_shape=jax.ShapeDtypeStruct((rows, WIDTH), BF16),
+        in_specs=[VMEM],
+        out_specs=VMEM,
+        cost_estimate=pl.CostEstimate(flops=800_000_000, bytes_accessed=x.size * 4, transcendentals=0),
+        compiler_params=pltpu.CompilerParams(vmem_limit_bytes=SMALL),
+        name="unpack",
+    )(x)
+
+
+def pack_kernel(a_ref, b_ref, out_ref):
+    experts = out_ref.shape[0] // SUB
+    for c in range(FOLD):
+        maps = jnp.concatenate(group_maps((GROUP, DENSE), 1, c), axis=1)
+        for g in range(experts // EXPERTS_G):
+            pieces = []
+            for start in dense_columns(c):
+                for k in range(SLOTS):
+                    here = slice(k * experts + g * EXPERTS_G, k * experts + (g + 1) * EXPERTS_G)
+                    columns = slice(start, start + PIECE)
+                    pieces.append(
+                        (a_ref[here, columns].astype(F32) + b_ref[here, columns].astype(F32)).astype(BF16)
+                    )
+            out_ref[g * GROUP : (g + 1) * GROUP, c * PIECE : (c + 1) * PIECE] = dot(
+                maps, jnp.concatenate(pieces, axis=0)
             ).astype(BF16)
-    x = dense_ref[...]
+
+
+def pack_sum(a, b):
+    rows = a.shape[0] // SLOTS * SUB
+    return pl.pallas_call(
+        pack_kernel,
+        out_shape=jax.ShapeDtypeStruct((rows, LANES), BF16),
+        in_specs=[VMEM] * 2,
+        out_specs=VMEM,
+        cost_estimate=pl.CostEstimate(flops=800_000_000, bytes_accessed=a.size * 6, transcendentals=0),
+        compiler_params=pltpu.CompilerParams(vmem_limit_bytes=SMALL),
+        name="pack_sum",
+    )(a, b)
+
+
+def ffn_kernel(x_ref, ga_ref, gb_ref, ua_ref, ub_ref, da_ref, db_ref, out_ref):
+    x = x_ref[...]
     hidden_a = (jax.nn.silu(dot(x, ga_ref[...])) * dot(x, ua_ref[...])).astype(BF16)
     hidden_b = (jax.nn.silu(dot(x, gb_ref[...])) * dot(x, ub_ref[...])).astype(BF16)
-    for c in range(WIDTH // PIECE):
-        columns = slice(c * PIECE, (c + 1) * PIECE)
-        total_ref[:, columns] = (
+    step = 2 * PIECE
+    for c in range(WIDTH // step):
+        columns = slice(c * step, (c + 1) * step)
+        out_ref[:, columns] = (
             dot(hidden_a, da_ref[:, columns]) + dot(hidden_b, db_ref[:, columns])
         ).astype(BF16)
-    scatter = partial(group_place, (GROUP, DENSE), 1)
-    mains = [scatter(lambda sub, slot, h=h: main_place(sub, slot, h)) for h in range(2)]
-    tails = {
-        (u, c): scatter(lambda sub, slot, u=u, c=c: tail_place(sub, slot, u, c)) for u, c in tails
-    }
-    for g in range(groups):
-        rows, dense = slice(g * GROUP, (g + 1) * GROUP), slice(g * DENSE, (g + 1) * DENSE)
-        for c in range(FOLD):
-            columns = slice(c * PIECE, (c + 1) * PIECE)
-            total = sum(
-                dot(mains[h], total_ref[dense, h * LANES + c * PIECE : h * LANES + (c + 1) * PIECE])
-                for h in range(2)
-            )
-            for u in range(2):
-                if (u, c) in tails:
-                    total += dot(
-                        tails[u, c], total_ref[dense, MAIN + u * PIECE : MAIN + (u + 1) * PIECE]
-                    )
-            out_ref[rows, columns] = total.astype(BF16)
 
 
 def half_ffn(x, ga, gb, ua, ub, da, db):
-    rows = x.shape[0]
-    dense = rows // SUB * SLOTS
     hidden = ga.shape[1] + gb.shape[1]
     return pl.pallas_call(
         ffn_kernel,
         out_shape=jax.ShapeDtypeStruct(x.shape, BF16),
         in_specs=[VMEM] * 7,
         out_specs=VMEM,
-        scratch_shapes=[pltpu.VMEM((dense, WIDTH), BF16), pltpu.VMEM((dense, WIDTH), BF16)],
         cost_estimate=pl.CostEstimate(
-            flops=3_500_000_000,
+            flops=3_000_000_000,
             bytes_accessed=x.size * 4 + 6 * ga.size * 2,
-            transcendentals=dense * hidden,
+            transcendentals=x.shape[0] * hidden,
         ),
-        compiler_params=pltpu.CompilerParams(vmem_limit_bytes=24 * 1024 * 1024),
+        compiler_params=pltpu.CompilerParams(vmem_limit_bytes=SMALL),
         name="half_ffn",
     )(x, ga, gb, ua, ub, da, db)
 
 
-def combine_kernel(own_ref, first_ref, second_ref, routes_ref, weight_ref, out_ref):
+def combine_kernel(base, own_ref, values_ref, routes_ref, weight_ref, *refs):
     del own_ref
-    rows, tokens = first_ref.shape[0], out_ref.shape[0]
-    by_first, named, rank, sub = slot_ranks(routes_ref, rows, tokens, 0)
-    weight = jnp.where(by_first, weight_ref[0:1, :], weight_ref[1:2, :])
-
-    def split(chosen):
-        picked = jnp.where(chosen, weight, 0.0).T
-        high = picked.astype(BF16)
-        return high, (picked - high.astype(F32)).astype(BF16)
-
-    parts = [[] for _ in range(WIDTH // PIECE)]
-    for chunk, ref in enumerate((first_ref, second_ref)):
-        slot = rank - chunk * SLOTS
-        here = named & (slot < SLOTS)
-        for h in range(2):
-            chosen = split(here & main_place(sub, slot, h))
-            for c in range(FOLD):
-                parts[h * FOLD + c].append((chosen, ref, c))
-        for u in range(2):
-            for c in range(FOLD):
-                if tail_used(u, c):
-                    parts[2 * FOLD + u].append((split(here & tail_place(sub, slot, u, c)), ref, c))
-    for j, terms in enumerate(parts):
+    *before_ref, out_ref = refs
+    rows, tokens = values_ref.shape[0], out_ref.shape[0]
+    routes = jnp.transpose(routes_ref[...].astype(F32)).astype(jnp.int32)
+    weights = jnp.transpose(weight_ref[...])
+    row = lax.broadcasted_iota(jnp.int32, (tokens, rows), 1)
+    expert, sub = row // SUB, row % SUB
+    by_first, by_second = expert == routes[:, 0:1], expert == routes[:, 1:2]
+    named = by_first | by_second
+    earlier = lax.broadcasted_iota(jnp.int32, (tokens, tokens), 1) < lax.broadcasted_iota(
+        jnp.int32, (tokens, tokens), 0
+    )
+    slot = dot(as_bf16(earlier), as_bf16(named)).astype(jnp.int32) - base
+    weight = jnp.where(
+        named & (slot < SLOTS), jnp.where(by_first, weights[:, 0:1], weights[:, 1:2]), 0.0
+    )
+    high = weight.astype(BF16).astype(F32)
+    low = weight - high
+
+    def taken(chosen, columns):
+        values = values_ref[:, columns]
+        return dot(jnp.where(chosen, high, 0.0).astype(BF16), values) + dot(
+            jnp.where(chosen, low, 0.0).astype(BF16), values
+        )
+
+    def put(total, columns):
+        if before_ref:
+            total += before_ref[0][:, columns]
+        out_ref[:, columns] = total.astype(out_ref.dtype)
+
+    for h in range(2):
+        put(taken(main_place(sub, slot, h), slice(0, LANES)), slice(h * LANES, (h + 1) * LANES))
+    for u in range(2):
         total = 0.0
-        for (high, low), ref, c in terms:
-            values = ref[:, c * PIECE : (c + 1) * PIECE]
-            total += dot(high, values) + dot(low, values)
-        out_ref[:, j * PIECE : (j + 1) * PIECE] = total.astype(BF16)
-
-
-def combine(values, routes_t, weight_t, own, tokens):
+        for c in range(FOLD):
+            if tail_used(u, c):
+                total += taken(tail_place(sub, slot, u, c), slice(c * PIECE, (c + 1) * PIECE))
+        put(total, slice(MAIN + u * PIECE, MAIN + (u + 1) * PIECE))
+
+
+def combine(chunk, values, routes_t, weight_t, own, tokens, before=None):
+    rest = () if before is None else (before,)
     return pl.pallas_call(
-        combine_kernel,
-        out_shape=jax.ShapeDtypeStruct((tokens, WIDTH), BF16),
+        partial(combine_kernel, chunk * SLOTS),
+        out_shape=jax.ShapeDtypeStruct((tokens, WIDTH), F32 if before is None else BF16),
         grid_spec=pltpu.PrefetchScalarGridSpec(
             num_scalar_prefetch=1,
             grid=(1,),
             in_specs=[
                 VMEM,
-                VMEM,
                 pl.BlockSpec((K, tokens), lambda i, own: (0, own[0])),
                 pl.BlockSpec((K, tokens), lambda i, own: (0, own[0])),
-            ],
-            out_specs=pl.BlockSpec((tokens, WIDTH), lambda i, own: (0, 0)),
+            ]
+            + [VMEM] * len(rest),
+            out_specs=VMEM if before is None else pl.BlockSpec((tokens, WIDTH), lambda i, own: (0, 0)),
         ),
-        cost_estimate=pl.CostEstimate(flops=2_000_000_000, bytes_accessed=2_100_000, transcendentals=0),
-        compiler_params=pltpu.CompilerParams(vmem_limit_bytes=24 * 1024 * 1024),
+        cost_estimate=pl.CostEstimate(flops=1_500_000_000, bytes_accessed=2_100_000, transcendentals=0),
+        compiler_params=pltpu.CompilerParams(vmem_limit_bytes=SMALL),
         name="combine",
-    )(own, *values, routes_t, weight_t)
+    )(own, values, routes_t, weight_t, *rest)
 
 
 def exchanged(rows):
@@ -297,19 +352,20 @@
     gate_b, up_b, down_b = swapped(gate, 0), swapped(up, 0), swapped(down, 0)
     ffn = lambda x: half_ffn(x, gate, gate_b, up, up_b, down, down_b)
 
-    mine, back, kept, results, returned = [], [], [], [], []
+    mine = []
     for n in range(CHUNKS):
         sent = send_rows(expert_in, ffn_gain, routes_t, own, experts, n)
         mine.append(exchanged(sent))
+    expert_out = None
     for n in range(CHUNKS):
-        theirs = swapped(mine[n], 1)
+        rows = unpack(mine[n])
+        theirs = swapped(rows, 1)
         partial_sum = ffn(theirs)
-        back.append(swapped(partial_sum, 1))
-        kept.append(ffn(mine[n]))
-    for n in range(CHUNKS):
-        results.append((kept[n].astype(F32) + back[n].astype(F32)).astype(BF16))
-        returned.append(exchanged(results[n]))
-    expert_out = combine(returned, routes_t, weight_t, own, tokens)
+        back = swapped(partial_sum, 1)
+        kept = ffn(rows)
+        results = pack_sum(kept, back)
+        returned = exchanged(results)
+        expert_out = combine(n, returned, routes_t, weight_t, own, tokens, expert_out)
 
     extended = jnp.concatenate([before, pool_in], axis=0).astype(F32)
     positions = (

time: 155 us -> 161 us (1.039)
  starting transfers between devices: 53.4 us -> 59.9 us
  other arithmetic: 4.77 us -> 1.39 us
  waiting for transfers between devices: 58.4 us -> 55.2 us
  local copies, waits for them, and re-layouts: 0.07 us -> 2.99 us
  Pallas kernels: 33.1 us -> 35.8 us
    pallas_call x1 -> x6, Pallas kernels: 3.46 us -> 12.1 us  [the longest x2 5.82 us: pack_sum(): pl.pallas_call(pack_kernel, out_shape=jax.ShapeDtypeStruct((rows, LANES),...]
    all_to_all x4, starting transfers between devices: 41.6 us -> 48.5 us  [exchanged(): lax.all_to_all(rows.reshape(experts, SUB, LANES), 'ep', split_axis=0, con...]
    pallas_call x4, Pallas kernels: 23.1 us -> 17.1 us  [half_ffn(): pl.pallas_call(ffn_kernel, out_shape=jax.ShapeDtypeStruct(x.shape, BF16),...]
    reshape x2 -> x0, other arithmetic: 4.39 us -> none  [exchanged(): rows.reshape(experts, SUB, LANES)]
    all_to_all x4, waiting for transfers between devices: 35.5 us -> 31.7 us  [exchanged(): lax.all_to_all(rows.reshape(experts, SUB, LANES), 'ep', split_axis=0, con...]
    unnamed x14 -> x24, local copies, waits for them, and re-layouts: 0.06 us -> 2.97 us
  transfers between devices with their start and end apart: 12 -> 12, of which waited for: 7 -> 7; matrix products, arithmetic and copies ran while one was open for 6% -> 3% of each run, Pallas kernels for 17% -> 19%
where the time goes in v3:
time: 161 us; the launch traced here: 160 us
  starting transfers between devices  59.9 us (37%)
  waiting for transfers between devices  55.2 us (34%)
  Pallas kernels  35.8 us (22%)
  matrix products  4.17 us (3%)
  local copies, waits for them, and re-layouts  2.99 us (2%)
    all_to_all x4, starting transfers between devices, exchanged(): lax.all_to_all(rows.reshape(experts, SUB, LANES), 'ep', split_axis=0, con...  48.5 us
    all_to_all x4, waiting for transfers between devices, exchanged(): lax.all_to_all(rows.reshape(experts, SUB, LANES), 'ep', split_axis=0, con...  31.7 us
    ppermute x7, waiting for transfers between devices, swapped(): return lax.ppermute(array, ('ep', 'tp'), pairs)  23.5 us
    pallas_call x4, Pallas kernels, half_ffn(): pl.pallas_call(ffn_kernel, out_shape=jax.ShapeDtypeStruct(x.shape, BF16),...  17.1 us
    ppermute x7, starting transfers between devices, swapped(): return lax.ppermute(array, ('ep', 'tp'), pairs)  9.5 us
    pallas_call x2, Pallas kernels, send_rows(): pl.pallas_call(partial(send_kernel, chunk * SLOTS), out_shape=jax.ShapeDt...  6.54 us
    pallas_call x2, Pallas kernels, pack_sum(): pl.pallas_call(pack_kernel, out_shape=jax.ShapeDtypeStruct((rows, LANES),...  5.82 us
    pallas_call x2, Pallas kernels, combine(): pl.pallas_call(partial(combine_kernel, chunk * SLOTS), out_shape=jax.Shap...  4.49 us
  transfers between devices with their start and end apart: 12, of which 7 were waited for; matrix products, arithmetic and copies ran while one was open for 3% of the time, Pallas kernels for 19%

profile of v3, /device:TPU:1, one launch (start us, length us, event | category | flops | bytes accessed | tf_op | source)
XLA Modules:
  0.0 160.3 jit_solution(17967266631762568449)
XLA Ops:
  0.6 3.3 %send_rows.3 = bf16[512,768]{1,0:T(8,128)(2,1)} custom-call(s32[1]{0:T(128)} %bitcast.2.own_ref, bf16[512,2048]{1,0:T(8,128)(2,1)} %rows_ref.3, f32[1,2048]{1,0:T(1,128)} %bitcast.48, s32[2,512]{1,0:T(2,128)} %bitcast.40), custom_call_target="tpu_custom_call" | custom-call | flops 2000000000 | bytes 2100000 | tf_op jit(solution)/shard_map/send_rows/pallas_call | solution.py:125
  3.9 13.1 %all-to-all-start.2 = ((bf16[64,8,768]{2,1,0:T(8,128)(2,1)}), bf16[64,8,768]{2,1,0:T(8,128)(2,1)S(1)}, u32[]{:S(2)}, u32[]{:S(2)}) async-start(bf16[64,8,768]{2,1,0:T(8,128)(2,1)} %bitcast.47), calls=%async_computation.2 | async-start | bytes 1572864 | tf_op jit(solution)/shard_map/all_to_all | solution.py:325
  17.1 2.8 %collective-permute-start.1 = (bf16[2048,256]{1,0:T(8,128)(2,1)S(1)}, bf16[2048,256]{1,0:T(8,128)(2,1)}, u32[]{:S(2)}, u32[]{:S(2)}) collective-permute-start(bf16[2048,256]{1,0:T(8,128)(2,1)S(1)} %bitcast.35), channel_id=1, source_target_pairs={{0,1},{1,0},{2,3},{3,2},{4,7},{5,6},{6,5},{7,4},{8,9},{9,8},{10,11... | collective-permute-start | bytes 3145736 | tf_op jit(solution)/shard_map/ppermute | solution.py:46
  20.0 2.6 %collective-permute-start.3 = (bf16[256,2048]{1,0:T(8,128)(2,1)}, bf16[256,2048]{1,0:T(8,128)(2,1)}, u32[]{:S(2)}, u32[]{:S(2)}) collective-permute-start(bf16[256,2048]{1,0:T(8,128)(2,1)} %bitcast.9.da_ref), channel_id=1, source_target_pairs={{0,1},{1,0},{2,3},{3,2},{4,7},{5,6},{6,5},{7,4},{8,9},{9,8},{10,11... | collective-permute-start | bytes 3145736 | tf_op jit(solution)/shard_map/ppermute | solution.py:46
  22.6 3.2 %send_rows.2 = bf16[512,768]{1,0:T(8,128)(2,1)} custom-call(s32[1]{0:T(128)} %bitcast.2.own_ref, bf16[512,2048]{1,0:T(8,128)(2,1)} %rows_ref.3, f32[1,2048]{1,0:T(1,128)} %bitcast.49, s32[2,512]{1,0:T(2,128)} %bitcast.41), custom_call_target="tpu_custom_call" | custom-call | flops 2000000000 | bytes 2100000 | tf_op jit(solution)/shard_map/send_rows/pallas_call | solution.py:125
  25.8 14.2 %all-to-all-done.2 = bf16[64,8,768]{2,1,0:T(8,128)(2,1)S(1)} async-done(((bf16[64,8,768]{2,1,0:T(8,128)(2,1)}), bf16[64,8,768]{2,1,0:T(8,128)(2,1)S(1)}, u32[]{:S(2)}, u32[]{:S(2)}) %all-to-all-start.2) | async-done | bytes 786464 | tf_op jit(solution)/shard_map/all_to_all | solution.py:325
  40.1 5.9 %all-to-all-start = ((bf16[64,8,768]{2,1,0:T(8,128)(2,1)}), bf16[64,8,768]{2,1,0:T(8,128)(2,1)S(1)}, u32[]{:S(2)}, u32[]{:S(2)}) async-start(bf16[64,8,768]{2,1,0:T(8,128)(2,1)} %bitcast.46), calls=%async_computation | async-start | bytes 1572864 | tf_op jit(solution)/shard_map/all_to_all | solution.py:325
  48.7 9.6 %collective-permute-done.3.db_ref = bf16[256,2048]{1,0:T(8,128)(2,1)} collective-permute-done((bf16[256,2048]{1,0:T(8,128)(2,1)}, bf16[256,2048]{1,0:T(8,128)(2,1)}, u32[]{:S(2)}, u32[]{:S(2)}) %collective-permute-start.3) | collective-permute-done | bytes 1048608 | tf_op jit(solution)/shard_map/ppermute | solution.py:46
  58.3 4.6 %collective-permute-done.6.x_ref = bf16[192,2048]{1,0:T(8,128)(2,1)S(1)} collective-permute-done((bf16[192,2048]{1,0:T(8,128)(2,1)S(1)}, bf16[192,2048]{1,0:T(8,128)(2,1)S(1)}, u32[]{:S(2)}, u32[]{:S(2)}) %collective-permute-start.6) | collective-permute-done | bytes 786464 | tf_op jit(solution)/shard_map/ppermute | solution.py:46
  62.9 4.9 %half_ffn.7 = bf16[192,2048]{1,0:T(8,128)(2,1)} custom-call(bf16[192,2048]{1,0:T(8,128)(2,1)S(1)} %collective-permute-done.6.x_ref, bf16[2048,256]{1,0:T(8,128)(2,1)S(1)} %bitcast.36, bf16[2048,256]{1,0:T(8,128)(2,1)} %collective-permute-done.1.gb_ref, bf16[2048,256]{1,0:T(8,128)(2,1)} %bitcast.8.ua_ref, bf16[2048,256]{1,0:T(8,128)(2,1)} %collective-permute-done.2.ub_ref, ...), custom_call_target="tpu_custom_call" | custom-call | flops 3000000000 | bytes 7864320 | tf_op jit(solution)/shard_map/half_ffn/pallas_call | solution.py:245
  71.6 4.0 %half_ffn.6.a_ref = bf16[192,2048]{1,0:T(8,128)(2,1)S(1)} custom-call(bf16[192,2048]{1,0:T(8,128)(2,1)S(1)} %copy-done.3, bf16[2048,256]{1,0:T(8,128)(2,1)S(1)} %bitcast.37, bf16[2048,256]{1,0:T(8,128)(2,1)} %collective-permute-done.1.gb_ref, bf16[2048,256]{1,0:T(8,128)(2,1)} %bitcast.8.ua_ref, bf16[2048,256]{1,0:T(8,128)(2,1)} %collective-permute-done.2.ub_ref, ...), custom_call_target="tpu_custom_call" | custom-call | flops 3000000000 | bytes 7864320 | tf_op jit(solution)/shard_map/half_ffn/pallas_call | solution.py:245
  75.6 3.7 %collective-permute-done.7.b_ref = bf16[192,2048]{1,0:T(8,128)(2,1)} collective-permute-done((bf16[192,2048]{1,0:T(8,128)(2,1)}, bf16[192,2048]{1,0:T(8,128)(2,1)}, u32[]{:S(2)}, u32[]{:S(2)}) %collective-permute-start.7) | collective-permute-done | bytes 786464 | tf_op jit(solution)/shard_map/ppermute | solution.py:46
  79.3 2.9 %pack_sum.3 = bf16[512,768]{1,0:T(8,128)(2,1)} custom-call(bf16[192,2048]{1,0:T(8,128)(2,1)S(1)} %half_ffn.6.a_ref, bf16[192,2048]{1,0:T(8,128)(2,1)} %collective-permute-done.7.b_ref), custom_call_target="tpu_custom_call" | custom-call | flops 800000000 | bytes 2359296 | tf_op jit(solution)/shard_map/pack_sum/pallas_call | solution.py:220
  82.2 13.0 %all-to-all-start.3 = ((bf16[64,8,768]{2,1,0:T(8,128)(2,1)}), bf16[64,8,768]{2,1,0:T(8,128)(2,1)S(1)}, u32[]{:S(2)}, u32[]{:S(2)}) async-start(bf16[64,8,768]{2,1,0:T(8,128)(2,1)} %bitcast.15), calls=%async_computation.3 | async-start | bytes 1572864 | tf_op jit(solution)/shard_map/all_to_all | solution.py:325
  95.3 1.9 %collective-permute-start = (bf16[15,1024]{1,0:T(8,128)(2,1)S(1)}, bf16[15,1024]{1,0:T(8,128)(2,1)S(1)}, u32[]{:S(2)}, u32[]{:S(2)}) collective-permute-start(bf16[15,1024]{1,0:T(8,128)(2,1)S(1)} %slice.52), channel_id=1, source_target_pairs={{0,1},{1,2},{2,3},{3,4},{4,5},{5,6},{6,7},{7,8},{8,9},{9,10},{10,1... | collective-permute-start | bytes 92168 | tf_op jit(solution)/shard_map/ppermute | solution.py:36
  99.2 4.0 %half_ffn.5 = bf16[192,2048]{1,0:T(8,128)(2,1)S(1)} custom-call(bf16[192,2048]{1,0:T(8,128)(2,1)S(1)} %copy-done.5, bf16[2048,256]{1,0:T(8,128)(2,1)S(1)} %bitcast.38, bf16[2048,256]{1,0:T(8,128)(2,1)} %collective-permute-done.1.gb_ref, bf16[2048,256]{1,0:T(8,128)(2,1)} %bitcast.8.ua_ref, bf16[2048,256]{1,0:T(8,128)(2,1)} %collective-permute-done.2.ub_ref, ...), custom_call_target="tpu_custom_call" | custom-call | flops 3000000000 | bytes 7864320 | tf_op jit(solution)/shard_map/half_ffn/pallas_call | solution.py:245
  104.6 4.2 %half_ffn.4.a_ref = bf16[192,2048]{1,0:T(8,128)(2,1)S(1)} custom-call(bf16[192,2048]{1,0:T(8,128)(2,1)} %unpack.2.x_ref, bf16[2048,256]{1,0:T(8,128)(2,1)S(1)} %bitcast.39, bf16[2048,256]{1,0:T(8,128)(2,1)} %collective-permute-done.1.gb_ref, bf16[2048,256]{1,0:T(8,128)(2,1)} %bitcast.8.ua_ref, bf16[2048,256]{1,0:T(8,128)(2,1)} %collective-permute-done.2.ub_ref, ...), custom_call_target="tpu_custom_call" | custom-call | flops 3000000000 | bytes 7864320 | tf_op jit(solution)/shard_map/half_ffn/pallas_call | solution.py:245
  108.8 5.7 %collective-permute-done.5.b_ref = bf16[192,2048]{1,0:T(8,128)(2,1)} collective-permute-done((bf16[192,2048]{1,0:T(8,128)(2,1)S(1)}, bf16[192,2048]{1,0:T(8,128)(2,1)}, u32[]{:S(2)}, u32[]{:S(2)}) %collective-permute-start.5) | collective-permute-done | bytes 786464 | tf_op jit(solution)/shard_map/ppermute | solution.py:46
  114.5 2.9 %pack_sum.2 = bf16[512,768]{1,0:T(8,128)(2,1)} custom-call(bf16[192,2048]{1,0:T(8,128)(2,1)S(1)} %half_ffn.4.a_ref, bf16[192,2048]{1,0:T(8,128)(2,1)} %collective-permute-done.5.b_ref), custom_call_target="tpu_custom_call" | custom-call | flops 800000000 | bytes 2359296 | tf_op jit(solution)/shard_map/pack_sum/pallas_call | solution.py:220
  118.2 16.4 %all-to-all-start.1 = ((bf16[64,8,768]{2,1,0:T(8,128)(2,1)}), bf16[64,8,768]{2,1,0:T(8,128)(2,1)S(1)}, u32[]{:S(2)}, u32[]{:S(2)}) async-start(bf16[64,8,768]{2,1,0:T(8,128)(2,1)} %bitcast.10), calls=%async_computation.1 | async-start | bytes 1572864 | tf_op jit(solution)/shard_map/all_to_all | solution.py:325
  134.7 1.9 %fusion.5 = f32[8,256,128]{1,2,0:T(8,128)S(1)} fusion(bf16[8,128,128]{2,1,0:T(8,128)(2,1)S(1)} %copy-done, f32[1024]{0:T(1024)S(1)} %select_select_fusion, f32[256]{0:T(256)S(1)} %convert_add_fusion, pred[1024]{0:T(1024)(128)(4,1)S(1)} %get-tuple-element.5, pred[1024]{0:T(1024)(128)(4,1)S(1)} %get-tuple-element.4, ...), kind=kOutput, calls=%fused_computation.23 | convolution fusion | flops 73138176 | bytes 18097152 | tf_op jit(solution)/shard_map/tgc,gcd->tgd/dot_general | solution.py:376
  136.9 2.2 %convolution_convert_fusion = bf16[256,2048]{1,0:T(8,128)(2,1)} fusion(bf16[256,1024]{0,1:T(8,128)(2,1)S(1)} %fusion.3, bf16[1024,2048]{1,0:T(8,128)(2,1)S(1)} %copy-done.11), kind=kOutput, calls=%fused_computation | convolution fusion | flops 1074266112 | bytes 5767168 | tf_op jit(solution)/shard_map/dot_general | solution.py:75
  141.0 16.6 %all-to-all-done.1 = bf16[64,8,768]{2,1,0:T(8,128)(2,1)S(1)} async-done(((bf16[64,8,768]{2,1,0:T(8,128)(2,1)}), bf16[64,8,768]{2,1,0:T(8,128)(2,1)S(1)}, u32[]{:S(2)}, u32[]{:S(2)}) %all-to-all-start.1) | async-done | bytes 786464 | tf_op jit(solution)/shard_map/all_to_all | solution.py:325
  157.7 2.6 %combine.3 = bf16[128,2048]{1,0:T(8,128)(2,1)} custom-call(s32[1]{0:T(128)} %bitcast.2.own_ref, bf16[512,768]{1,0:T(8,128)(2,1)S(1)} %bitcast.34, s32[2,512]{1,0:T(2,128)S(1)} %bitcast.43, f32[2,512]{1,0:T(2,128)S(1)} %bitcast.45, f32[128,2048]{1,0:T(8,128)S(1)} %combine.2.refs_0_), custom_call_target="tpu_custom_call" | custom-call | flops 1500000000 | bytes 2100000 | tf_op jit(solution)/shard_map/combine/pallas_call | solution.py:303
  (45 shorter events, 13.0 us)
Async XLA Ops:
  0.6 134.0 %copy-start = (bf16[8,128,128]{2,1,0:T(8,128)(2,1)S(1)}, bf16[8,128,128]{2,1,0:T(8,128)(2,1)}, u32[]{:S(2)}) copy-start(bf16[8,128,128]{2,1,0:T(8,128)(2,1)} %param.12) | copy-start | bytes 786436
  3.9 13.1 %copy-start.1 = (bf16[1,2048,256]{2,1,0:T(8,128)(2,1)S(1)}, bf16[1,2048,256]{2,1,0:T(8,128)(2,1)}, u32[]{:S(2)}) copy-start(bf16[1,2048,256]{2,1,0:T(8,128)(2,1)} %param.19) | copy-start | bytes 3145732
  3.9 36.1 %all-to-all-start.2 = ((bf16[64,8,768]{2,1,0:T(8,128)(2,1)}), bf16[64,8,768]{2,1,0:T(8,128)(2,1)S(1)}, u32[]{:S(2)}, u32[]{:S(2)}) async-start(bf16[64,8,768]{2,1,0:T(8,128)(2,1)} %bitcast.47), calls=%async_computation.2 | async-start | bytes 1572864 | tf_op jit(solution)/shard_map/all_to_all | solution.py:325
  17.1 31.7 %collective-permute-start.1 = (bf16[2048,256]{1,0:T(8,128)(2,1)S(1)}, bf16[2048,256]{1,0:T(8,128)(2,1)}, u32[]{:S(2)}, u32[]{:S(2)}) collective-permute-start(bf16[2048,256]{1,0:T(8,128)(2,1)S(1)} %bitcast.35), channel_id=1, source_target_pairs={{0,1},{1,0},{2,3},{3,2},{4,7},{5,6},{6,5},{7,4},{8,9},{9,8},{10,11... | collective-permute-start | bytes 3145736 | tf_op jit(solution)/shard_map/ppermute | solution.py:46
  19.9 28.9 %collective-permute-start.2 = (bf16[2048,256]{1,0:T(8,128)(2,1)}, bf16[2048,256]{1,0:T(8,128)(2,1)}, u32[]{:S(2)}, u32[]{:S(2)}) collective-permute-start(bf16[2048,256]{1,0:T(8,128)(2,1)} %bitcast.8.ua_ref), channel_id=1, source_target_pairs={{0,1},{1,0},{2,3},{3,2},{4,7},{5,6},{6,5},{7,4},{8,9},{9,8},{10,11... | collective-permute-start | bytes 3145736 | tf_op jit(solution)/shard_map/ppermute | solution.py:46
  20.0 38.3 %collective-permute-start.3 = (bf16[256,2048]{1,0:T(8,128)(2,1)}, bf16[256,2048]{1,0:T(8,128)(2,1)}, u32[]{:S(2)}, u32[]{:S(2)}) collective-permute-start(bf16[256,2048]{1,0:T(8,128)(2,1)} %bitcast.9.da_ref), channel_id=1, source_target_pairs={{0,1},{1,0},{2,3},{3,2},{4,7},{5,6},{6,5},{7,4},{8,9},{9,8},{10,11... | collective-permute-start | bytes 3145736 | tf_op jit(solution)/shard_map/ppermute | solution.py:46
  40.1 29.1 %all-to-all-start = ((bf16[64,8,768]{2,1,0:T(8,128)(2,1)}), bf16[64,8,768]{2,1,0:T(8,128)(2,1)S(1)}, u32[]{:S(2)}, u32[]{:S(2)}) async-start(bf16[64,8,768]{2,1,0:T(8,128)(2,1)} %bitcast.46), calls=%async_computation | async-start | bytes 1572864 | tf_op jit(solution)/shard_map/all_to_all | solution.py:325
  46.5 16.5 %collective-permute-start.6 = (bf16[192,2048]{1,0:T(8,128)(2,1)S(1)}, bf16[192,2048]{1,0:T(8,128)(2,1)S(1)}, u32[]{:S(2)}, u32[]{:S(2)}) collective-permute-start(bf16[192,2048]{1,0:T(8,128)(2,1)S(1)} %unpack.3.x_ref), channel_id=1, source_target_pairs={{0,3},{1,2},{2,1},{3,0},{4,5},{5,4},{6,7},{7,6},{8,11},{9,10},{10,... | collective-permute-start | bytes 2359304 | tf_op jit(solution)/shard_map/ppermute | solution.py:46
  47.8 0.9 copy-start.2
  67.8 11.5 %collective-permute-start.7 = (bf16[192,2048]{1,0:T(8,128)(2,1)}, bf16[192,2048]{1,0:T(8,128)(2,1)}, u32[]{:S(2)}, u32[]{:S(2)}) collective-permute-start(bf16[192,2048]{1,0:T(8,128)(2,1)} %half_ffn.7), channel_id=1, source_target_pairs={{0,3},{1,2},{2,1},{3,0},{4,5},{5,4},{6,7},{7,6},{8,11},{9,10},{10,... | collective-permute-start | bytes 2359304 | tf_op jit(solution)/shard_map/ppermute | solution.py:46
  69.1 2.5 %copy-start.3 = (bf16[192,2048]{1,0:T(8,128)(2,1)S(1)}, bf16[192,2048]{1,0:T(8,128)(2,1)}, u32[]{:S(2)}) copy-start(bf16[192,2048]{1,0:T(8,128)(2,1)} %copy-done.2) | copy-start | bytes 2359300
  70.5 26.7 %collective-permute-start.4 = (bf16[192,2048]{1,0:T(8,128)(2,1)}, bf16[192,2048]{1,0:T(8,128)(2,1)S(1)}, u32[]{:S(2)}, u32[]{:S(2)}) collective-permute-start(bf16[192,2048]{1,0:T(8,128)(2,1)} %unpack.2.x_ref), channel_id=1, source_target_pairs={{0,3},{1,2},{2,1},{3,0},{4,5},{5,4},{6,7},{7,6},{8,11},{9,10},{10,... | collective-permute-start | bytes 2359304 | tf_op jit(solution)/shard_map/ppermute | solution.py:46
  82.2 13.1 %copy-start.9 = (bf16[256,1024]{1,0:T(8,128)(2,1)S(1)}, bf16[256,1024]{1,0:T(8,128)(2,1)}, u32[]{:S(2)}) copy-start(bf16[256,1024]{1,0:T(8,128)(2,1)} %param.11) | copy-start | bytes 1572868
  82.2 36.0 %all-to-all-start.3 = ((bf16[64,8,768]{2,1,0:T(8,128)(2,1)}), bf16[64,8,768]{2,1,0:T(8,128)(2,1)S(1)}, u32[]{:S(2)}, u32[]{:S(2)}) async-start(bf16[64,8,768]{2,1,0:T(8,128)(2,1)} %bitcast.15), calls=%async_computation.3 | async-start | bytes 1572864 | tf_op jit(solution)/shard_map/all_to_all | solution.py:325
  95.3 8.2 %collective-permute-start = (bf16[15,1024]{1,0:T(8,128)(2,1)S(1)}, bf16[15,1024]{1,0:T(8,128)(2,1)S(1)}, u32[]{:S(2)}, u32[]{:S(2)}) collective-permute-start(bf16[15,1024]{1,0:T(8,128)(2,1)S(1)} %slice.52), channel_id=1, source_target_pairs={{0,1},{1,2},{2,3},{3,4},{4,5},{5,6},{6,7},{7,8},{8,9},{9,10},{10,1... | collective-permute-start | bytes 92168 | tf_op jit(solution)/shard_map/ppermute | solution.py:36
  97.2 0.9 copy-start.4
  98.1 1.1 copy-start.5
  103.2 11.3 %collective-permute-start.5 = (bf16[192,2048]{1,0:T(8,128)(2,1)S(1)}, bf16[192,2048]{1,0:T(8,128)(2,1)}, u32[]{:S(2)}, u32[]{:S(2)}) collective-permute-start(bf16[192,2048]{1,0:T(8,128)(2,1)S(1)} %half_ffn.5), channel_id=1, source_target_pairs={{0,3},{1,2},{2,1},{3,0},{4,5},{5,4},{6,7},{7,6},{8,11},{9,10},{10,... | collective-permute-start | bytes 2359304 | tf_op jit(solution)/shard_map/ppermute | solution.py:46
  117.5 17.2 %copy-start.8 = (f32[271,1024]{1,0:T(8,128)S(1)}, f32[271,1024]{1,0:T(8,128)}, u32[]{:S(2)}) copy-start(f32[271,1024]{1,0:T(8,128)} %maximum_convert_fusion) | copy-start | bytes 3330052
  118.2 39.4 %all-to-all-start.1 = ((bf16[64,8,768]{2,1,0:T(8,128)(2,1)}), bf16[64,8,768]{2,1,0:T(8,128)(2,1)S(1)}, u32[]{:S(2)}, u32[]{:S(2)}) async-start(bf16[64,8,768]{2,1,0:T(8,128)(2,1)} %bitcast.10), calls=%async_computation.1 | async-start | bytes 1572864 | tf_op jit(solution)/shard_map/all_to_all | solution.py:325
  134.7 2.0 %copy-start.10 = (f32[1024]{0:T(1024)S(1)}, f32[1024]{0:T(1024)}, u32[]{:S(2)}) copy-start(f32[1024]{0:T(1024)} %param.13) | copy-start | bytes 12292
  134.7 2.2 %copy-start.11 = (bf16[1024,2048]{1,0:T(8,128)(2,1)S(1)}, bf16[1024,2048]{1,0:T(8,128)(2,1)}, u32[]{:S(2)}) copy-start(bf16[1024,2048]{1,0:T(8,128)(2,1)} %param.14) | copy-start | bytes 12582916
  136.9 2.3 %copy-start.6 = (s32[512,2]{0,1:T(2,128)S(1)}, s32[512,2]{0,1:T(2,128)}, u32[]{:S(2)}) copy-start(s32[512,2]{0,1:T(2,128)} %param.17) | copy-start | bytes 12292
  136.9 2.3 %copy-start.7 = (f32[512,2]{0,1:T(2,128)S(1)}, f32[512,2]{0,1:T(2,128)}, u32[]{:S(2)}) copy-start(f32[512,2]{0,1:T(2,128)} %param.18) | copy-start | bytes 12292

commit v4 on v3

--- a/solution.py
+++ b/solution.py
@@ -28,6 +28,7 @@
 BF16 = jnp.bfloat16
 F32 = jnp.float32
 VMEM = pl.BlockSpec(memory_space=pltpu.VMEM)
+HBM = pl.BlockSpec(memory_space=pltpu.HBM)
 
 
 def passed_along(array, axis, by):
@@ -100,22 +101,30 @@
     return any((r * FOLD + c - piece) % 2 == 0 for r in range(SUB - 2 * SLOTS))
 
 
-def send_kernel(base, own_ref, rows_ref, gain_ref, routes_ref, out_ref):
-    del own_ref
+def send_kernel(base, own_ref, rows_hbm, gain_ref, routes_ref, out_ref, rows_ref, sem):
     tokens = rows_ref.shape[0]
+    copy = pltpu.make_async_copy(
+        rows_hbm.at[pl.ds(pl.multiple_of(own_ref[0] * tokens, tokens), tokens)], rows_ref, sem
+    )
+    copy.start()
+    _, named, rank, sub = slot_ranks(routes_ref, out_ref.shape[0], tokens, base)
+    mains = jnp.concatenate([as_bf16(named & main_place(sub, rank, h)) for h in range(2)], axis=1)
+    copy.wait()
     features = rows_ref[...].astype(F32)
     inverse = lax.rsqrt(jnp.mean(features * features, axis=-1, keepdims=True) + EPS)
     normed = (features * inverse * gain_ref[...]).astype(BF16)
-    _, named, rank, sub = slot_ranks(routes_ref, out_ref.shape[0], tokens, base)
-    low = as_bf16(named & main_place(sub, rank, 0))
-    high = as_bf16(named & main_place(sub, rank, 1))
     for c in range(FOLD):
         columns = slice(c * PIECE, (c + 1) * PIECE)
-        total = dot(low, normed[:, columns]) + dot(high, normed[:, LANES:][:, columns])
-        for u in range(2):
-            if tail_used(u, c):
-                tail = as_bf16(named & tail_place(sub, rank, u, c))
-                total += dot(tail, normed[:, MAIN + u * PIECE : MAIN + (u + 1) * PIECE])
+        used = [u for u in range(2) if tail_used(u, c)]
+        tails = jnp.concatenate([as_bf16(named & tail_place(sub, rank, u, c)) for u in used], axis=1)
+        total = dot(
+            mains, jnp.concatenate([normed[:, columns], normed[:, LANES:][:, columns]], axis=0)
+        ) + dot(
+            tails,
+            jnp.concatenate(
+                [normed[:, MAIN + u * PIECE : MAIN + (u + 1) * PIECE] for u in used], axis=0
+            ),
+        )
         out_ref[:, columns] = total.astype(BF16)
 
 
@@ -129,11 +138,12 @@
             num_scalar_prefetch=1,
             grid=(1,),
             in_specs=[
-                pl.BlockSpec((tokens, width), lambda i, own: (own[0], 0)),
+                HBM,
                 pl.BlockSpec((1, width), lambda i, own: (0, 0)),
                 pl.BlockSpec((K, tokens), lambda i, own: (0, own[0])),
             ],
-            out_specs=pl.BlockSpec((experts * SUB, LANES), lambda i, own: (0, 0)),
+            out_specs=VMEM,
+            scratch_shapes=[pltpu.VMEM((tokens, width), BF16), pltpu.SemaphoreType.DMA],
         ),
         cost_estimate=pl.CostEstimate(flops=2_000_000_000, bytes_accessed=2_100_000, transcendentals=128),
         name="send_rows",
@@ -159,7 +169,7 @@
     return starts + [MAIN + u * PIECE for u in range(2) if tail_used(u, c)]
 
 
-def unpack_kernel(x_ref, out_ref):
+def unpack(x_ref, out_ref):
     experts = x_ref.shape[0] // SUB
     tails = {}
     for c in range(FOLD):
@@ -184,19 +194,6 @@
             ].astype(BF16)
 
 
-def unpack(x):
-    rows = x.shape[0] // SUB * SLOTS
-    return pl.pallas_call(
-        unpack_kernel,
-        out_shape=jax.ShapeDtypeStruct((rows, WIDTH), BF16),
-        in_specs=[VMEM],
-        out_specs=VMEM,
-        cost_estimate=pl.CostEstimate(flops=800_000_000, bytes_accessed=x.size * 4, transcendentals=0),
-        compiler_params=pltpu.CompilerParams(vmem_limit_bytes=SMALL),
-        name="unpack",
-    )(x)
-
-
 def pack_kernel(a_ref, b_ref, out_ref):
     experts = out_ref.shape[0] // SUB
     for c in range(FOLD):
@@ -228,10 +225,25 @@
     )(a, b)
 
 
-def ffn_kernel(x_ref, ga_ref, gb_ref, ua_ref, ub_ref, da_ref, db_ref, out_ref):
-    x = x_ref[...]
+def ffn_kernel(x_ref, *refs):
+    sources, out_ref, dense_ref, held, sems = refs[:6], refs[6], refs[7], refs[8:14], refs[14]
+    copies = [
+        pltpu.make_async_copy(source, ref, sems.at[n])
+        for n, (source, ref) in enumerate(zip(sources, held))
+    ]
+    for copy in copies:
+        copy.start()
+    ga_ref, ua_ref, gb_ref, ub_ref, da_ref, db_ref = held
+    unpack(x_ref, dense_ref)
+    x = dense_ref[...]
+    copies[0].wait()
+    copies[1].wait()
     hidden_a = (jax.nn.silu(dot(x, ga_ref[...])) * dot(x, ua_ref[...])).astype(BF16)
+    copies[2].wait()
+    copies[3].wait()
     hidden_b = (jax.nn.silu(dot(x, gb_ref[...])) * dot(x, ub_ref[...])).astype(BF16)
+    copies[4].wait()
+    copies[5].wait()
     step = 2 * PIECE
     for c in range(WIDTH // step):
         columns = slice(c * step, (c + 1) * step)
@@ -241,20 +253,25 @@
 
 
 def half_ffn(x, ga, gb, ua, ub, da, db):
+    weights = (ga, ua, gb, ub, da, db)
+    dense = x.shape[0] // SUB * SLOTS
     hidden = ga.shape[1] + gb.shape[1]
     return pl.pallas_call(
         ffn_kernel,
-        out_shape=jax.ShapeDtypeStruct(x.shape, BF16),
-        in_specs=[VMEM] * 7,
+        out_shape=jax.ShapeDtypeStruct((dense, WIDTH), BF16),
+        in_specs=[VMEM] + [HBM] * 6,
         out_specs=VMEM,
+        scratch_shapes=[pltpu.VMEM((dense, WIDTH), BF16)]
+        + [pltpu.VMEM(w.shape, BF16) for w in weights]
+        + [pltpu.SemaphoreType.DMA((6,))],
         cost_estimate=pl.CostEstimate(
-            flops=3_000_000_000,
+            flops=3_500_000_000,
             bytes_accessed=x.size * 4 + 6 * ga.size * 2,
-            transcendentals=x.shape[0] * hidden,
+            transcendentals=dense * hidden,
         ),
         compiler_params=pltpu.CompilerParams(vmem_limit_bytes=SMALL),
         name="half_ffn",
-    )(x, ga, gb, ua, ub, da, db)
+    )(x, *weights)
 
 
 def combine_kernel(base, own_ref, values_ref, routes_ref, weight_ref, *refs):
@@ -277,25 +294,25 @@
     high = weight.astype(BF16).astype(F32)
     low = weight - high
 
-    def taken(chosen, columns):
-        values = values_ref[:, columns]
-        return dot(jnp.where(chosen, high, 0.0).astype(BF16), values) + dot(
-            jnp.where(chosen, low, 0.0).astype(BF16), values
-        )
-
-    def put(total, columns):
+    def split(chosen):
+        return [jnp.where(chosen, part, 0.0).astype(BF16) for part in (high, low)]
+
+    totals = {}
+    mains = [part for h in range(2) for part in split(main_place(sub, slot, h))]
+    for c in range(FOLD):
+        maps = list(mains)
+        for u in range(2):
+            if tail_used(u, c):
+                maps += split(tail_place(sub, slot, u, c))
+        found = dot(jnp.concatenate(maps, axis=0), values_ref[:, c * PIECE : (c + 1) * PIECE])
+        for n, start in enumerate(dense_columns(c)):
+            block = found[2 * n * tokens : (2 * n + 1) * tokens] + found[(2 * n + 1) * tokens : (2 * n + 2) * tokens]
+            totals[start] = totals[start] + block if start in totals else block
+    for start, total in totals.items():
+        columns = slice(start, start + PIECE)
         if before_ref:
             total += before_ref[0][:, columns]
         out_ref[:, columns] = total.astype(out_ref.dtype)
-
-    for h in range(2):
-        put(taken(main_place(sub, slot, h), slice(0, LANES)), slice(h * LANES, (h + 1) * LANES))
-    for u in range(2):
-        total = 0.0
-        for c in range(FOLD):
-            if tail_used(u, c):
-                total += taken(tail_place(sub, slot, u, c), slice(c * PIECE, (c + 1) * PIECE))
-        put(total, slice(MAIN + u * PIECE, MAIN + (u + 1) * PIECE))
 
 
 def combine(chunk, values, routes_t, weight_t, own, tokens, before=None):
@@ -349,7 +366,8 @@
     before = passed_along(pool_in[rows_here - (WMAX - 1) :], ("ep", "tp"), 1)
 
     gate, up, down = w_gate[0], w_up[0], w_down[0]
-    gate_b, up_b, down_b = swapped(gate, 0), swapped(up, 0), swapped(down, 0)
+    gate_b = swapped(gate, 0)
+    up_b, down_b = swapped(up, 0), swapped(down, 0)
     ffn = lambda x: half_ffn(x, gate, gate_b, up, up_b, down, down_b)
 
     mine = []
@@ -358,11 +376,10 @@
         mine.append(exchanged(sent))
     expert_out = None
     for n in range(CHUNKS):
-        rows = unpack(mine[n])
-        theirs = swapped(rows, 1)
+        theirs = swapped(mine[n], 1)
         partial_sum = ffn(theirs)
         back = swapped(partial_sum, 1)
-        kept = ffn(rows)
+        kept = ffn(mine[n])
         results = pack_sum(kept, back)
         returned = exchanged(results)
         expert_out = combine(n, returned, routes_t, weight_t, own, tokens, expert_out)

time: 161 us -> 160 us (level)
  matrix products: 4.17 us -> 12.8 us
  Pallas kernels: 35.8 us -> 29.7 us
  waiting for transfers between devices: 55.2 us -> 50.7 us
  local copies, waits for them, and re-layouts: 2.99 us -> 7.4 us
  starting transfers between devices: 59.9 us -> 56.3 us
    dot_general x1, matrix products: 1.93 us -> 10.5 us  [on_device(): jnp.einsum('tgc,gcd->tgd', pooled.reshape(rows_here, group_count, GDIM),...]
    all_to_all x4, waiting for transfers between devices: 31.7 us -> 23.6 us  [exchanged(): lax.all_to_all(rows.reshape(experts, SUB, LANES), 'ep', split_axis=0, con...]
    pallas_call x6 -> x4, Pallas kernels: 18.9 us -> 13.7 us  [half_ffn(): pl.pallas_call(ffn_kernel, out_shape=jax.ShapeDtypeStruct((dense, WIDTH),...]
    unnamed x24 -> x26, local copies, waits for them, and re-layouts: 2.97 us -> 7.39 us
    ppermute x7, waiting for transfers between devices: 23.5 us -> 27.1 us  [swapped(): return lax.ppermute(array, ('ep', 'tp'), pairs)]
    all_to_all x4, starting transfers between devices: 48.5 us -> 45.8 us  [exchanged(): lax.all_to_all(rows.reshape(experts, SUB, LANES), 'ep', split_axis=0, con...]
  transfers between devices with their start and end apart: 12 -> 12, of which waited for: 7 -> 7; matrix products, arithmetic and copies ran while one was open for 3% -> 9% of each run, Pallas kernels for 19% -> 15%
where the time goes in v4:
time: 160 us; the launch traced here: 159 us
  starting transfers between devices  56.3 us (35%)
  waiting for transfers between devices  50.7 us (32%)
  Pallas kernels  29.7 us (19%)
  matrix products  12.8 us (8%)
  local copies, waits for them, and re-layouts  7.4 us (5%)
    all_to_all x4, starting transfers between devices, exchanged(): lax.all_to_all(rows.reshape(experts, SUB, LANES), 'ep', split_axis=0, con...  45.8 us
    ppermute x7, waiting for transfers between devices, swapped(): return lax.ppermute(array, ('ep', 'tp'), pairs)  27.1 us
    all_to_all x4, waiting for transfers between devices, exchanged(): lax.all_to_all(rows.reshape(experts, SUB, LANES), 'ep', split_axis=0, con...  23.6 us
    pallas_call x4, Pallas kernels, half_ffn(): pl.pallas_call(ffn_kernel, out_shape=jax.ShapeDtypeStruct((dense, WIDTH),...  13.7 us
    dot_general x1, matrix products, on_device(): jnp.einsum('tgc,gcd->tgd', pooled.reshape(rows_here, group_count, GDIM),...  10.5 us
    ppermute x7, starting transfers between devices, swapped(): return lax.ppermute(array, ('ep', 'tp'), pairs)  8.61 us
    unnamed x26, local copies, waits for them, and re-layouts  7.39 us
    pallas_call x2, Pallas kernels, send_rows(): pl.pallas_call(partial(send_kernel, chunk * SLOTS), out_shape=jax.ShapeDt...  7.02 us
  transfers between devices with their start and end apart: 12, of which 7 were waited for; matrix products, arithmetic and copies ran while one was open for 9% of the time, Pallas kernels for 15%

profile of v4, /device:TPU:1, one launch (start us, length us, event | category | flops | bytes accessed | tf_op | source)
XLA Modules:
  0.0 159.2 jit_solution(13015560952661861481)
XLA Ops:
  0.6 3.5 %send_rows.3 = bf16[512,768]{1,0:T(8,128)(2,1)} custom-call(s32[1]{0:T(128)} %bitcast.2.own_ref, bf16[512,2048]{1,0:T(8,128)(2,1)} %rows_hbm.3, f32[1,2048]{1,0:T(1,128)} %bitcast.60, s32[2,512]{1,0:T(2,128)} %bitcast.52), custom_call_target="tpu_custom_call" | custom-call | flops 2000000000 | bytes 2100000 | tf_op jit(solution)/shard_map/send_rows/pallas_call | solution.py:134
  4.2 13.1 %all-to-all-start.2 = ((bf16[64,8,768]{2,1,0:T(8,128)(2,1)}), bf16[64,8,768]{2,1,0:T(8,128)(2,1)S(1)}, u32[]{:S(2)}, u32[]{:S(2)}) async-start(bf16[64,8,768]{2,1,0:T(8,128)(2,1)} %bitcast.59), calls=%async_computation.2 | async-start | bytes 1572864 | tf_op jit(solution)/shard_map/all_to_all | solution.py:342
  17.4 2.8 %collective-permute-start.1 = (bf16[2048,256]{1,0:T(8,128)(2,1)S(1)}, bf16[2048,256]{1,0:T(8,128)(2,1)}, u32[]{:S(2)}, u32[]{:S(2)}) collective-permute-start(bf16[2048,256]{1,0:T(8,128)(2,1)S(1)} %bitcast.37), channel_id=1, source_target_pairs={{0,1},{1,0},{2,3},{3,2},{4,7},{5,6},{6,5},{7,4},{8,9},{9,8},{10,11... | collective-permute-start | bytes 3145736 | tf_op jit(solution)/shard_map/ppermute | solution.py:47
  20.3 2.6 %collective-permute-start.3 = (bf16[256,2048]{1,0:T(8,128)(2,1)}, bf16[256,2048]{1,0:T(8,128)(2,1)}, u32[]{:S(2)}, u32[]{:S(2)}) collective-permute-start(bf16[256,2048]{1,0:T(8,128)(2,1)} %bitcast.47), channel_id=1, source_target_pairs={{0,1},{1,0},{2,3},{3,2},{4,7},{5,6},{6,5},{7,4},{8,9},{9,8},{10,11... | collective-permute-start | bytes 3145736 | tf_op jit(solution)/shard_map/ppermute | solution.py:47
  22.8 3.5 %send_rows.2 = bf16[512,768]{1,0:T(8,128)(2,1)} custom-call(s32[1]{0:T(128)} %bitcast.2.own_ref, bf16[512,2048]{1,0:T(8,128)(2,1)} %rows_hbm.3, f32[1,2048]{1,0:T(1,128)} %bitcast.61, s32[2,512]{1,0:T(2,128)} %bitcast.53), custom_call_target="tpu_custom_call" | custom-call | flops 2000000000 | bytes 2100000 | tf_op jit(solution)/shard_map/send_rows/pallas_call | solution.py:134
  26.3 14.0 %all-to-all-done.2 = bf16[64,8,768]{2,1,0:T(8,128)(2,1)S(1)} async-done(((bf16[64,8,768]{2,1,0:T(8,128)(2,1)}), bf16[64,8,768]{2,1,0:T(8,128)(2,1)S(1)}, u32[]{:S(2)}, u32[]{:S(2)}) %all-to-all-start.2) | async-done | bytes 786464 | tf_op jit(solution)/shard_map/all_to_all | solution.py:342
  40.3 5.9 %all-to-all-start = ((bf16[64,8,768]{2,1,0:T(8,128)(2,1)}), bf16[64,8,768]{2,1,0:T(8,128)(2,1)S(1)}, u32[]{:S(2)}, u32[]{:S(2)}) async-start(bf16[64,8,768]{2,1,0:T(8,128)(2,1)} %bitcast.58), calls=%async_computation | async-start | bytes 1572864 | tf_op jit(solution)/shard_map/all_to_all | solution.py:342
  47.6 11.4 %collective-permute-done.3.refs_5_ = bf16[256,2048]{1,0:T(8,128)(2,1)} collective-permute-done((bf16[256,2048]{1,0:T(8,128)(2,1)}, bf16[256,2048]{1,0:T(8,128)(2,1)}, u32[]{:S(2)}, u32[]{:S(2)}) %collective-permute-start.3) | collective-permute-done | bytes 1048608 | tf_op jit(solution)/shard_map/ppermute | solution.py:47
  59.1 4.1 %collective-permute-done.6.x_ref = bf16[512,768]{1,0:T(8,128)(2,1)S(1)} collective-permute-done((bf16[512,768]{1,0:T(8,128)(2,1)S(1)}, bf16[512,768]{1,0:T(8,128)(2,1)S(1)}, u32[]{:S(2)}, u32[]{:S(2)}) %collective-permute-start.6) | collective-permute-done | bytes 786464 | tf_op jit(solution)/shard_map/ppermute | solution.py:47
  65.6 3.8 %half_ffn.7 = bf16[192,2048]{1,0:T(8,128)(2,1)} custom-call(bf16[512,768]{1,0:T(8,128)(2,1)S(1)} %collective-permute-done.6.x_ref, bf16[2048,256]{1,0:T(8,128)(2,1)S(1)} %bitcast.38, bf16[2048,256]{1,0:T(8,128)(2,1)S(1)} %bitcast.43, bf16[2048,256]{1,0:T(8,128)(2,1)} %collective-permute-done.1.refs_2_, bf16[2048,256]{1,0:T(8,128)(2,1)} %collective-permute-done.2.refs_3_, ...), custom_call_target="tpu_custom_call" | custom-call | flops 3500000000 | bytes 7864320 | tf_op jit(solution)/shard_map/half_ffn/pallas_call | solution.py:259
  73.5 2.9 %half_ffn.6.a_ref = bf16[192,2048]{1,0:T(8,128)(2,1)S(1)} custom-call(bf16[512,768]{1,0:T(8,128)(2,1)S(1)} %bitcast.35, bf16[2048,256]{1,0:T(8,128)(2,1)S(1)} %bitcast.39, bf16[2048,256]{1,0:T(8,128)(2,1)S(1)} %bitcast.44, bf16[2048,256]{1,0:T(8,128)(2,1)} %collective-permute-done.1.refs_2_, bf16[2048,256]{1,0:T(8,128)(2,1)} %collective-permute-done.2.refs_3_, ...), custom_call_target="tpu_custom_call" | custom-call | flops 3500000000 | bytes 7864320 | tf_op jit(solution)/shard_map/half_ffn/pallas_call | solution.py:259
  76.4 4.6 %collective-permute-done.7.b_ref = bf16[192,2048]{1,0:T(8,128)(2,1)} collective-permute-done((bf16[192,2048]{1,0:T(8,128)(2,1)}, bf16[192,2048]{1,0:T(8,128)(2,1)}, u32[]{:S(2)}, u32[]{:S(2)}) %collective-permute-start.7) | collective-permute-done | bytes 786464 | tf_op jit(solution)/shard_map/ppermute | solution.py:47
  81.0 2.9 %pack_sum.3 = bf16[512,768]{1,0:T(8,128)(2,1)} custom-call(bf16[192,2048]{1,0:T(8,128)(2,1)S(1)} %half_ffn.6.a_ref, bf16[192,2048]{1,0:T(8,128)(2,1)} %collective-permute-done.7.b_ref), custom_call_target="tpu_custom_call" | custom-call | flops 800000000 | bytes 2359296 | tf_op jit(solution)/shard_map/pack_sum/pallas_call | solution.py:217
  83.9 12.9 %all-to-all-start.3 = ((bf16[64,8,768]{2,1,0:T(8,128)(2,1)}), bf16[64,8,768]{2,1,0:T(8,128)(2,1)S(1)}, u32[]{:S(2)}, u32[]{:S(2)}) async-start(bf16[64,8,768]{2,1,0:T(8,128)(2,1)} %bitcast.15), calls=%async_computation.3 | async-start | bytes 1572864 | tf_op jit(solution)/shard_map/all_to_all | solution.py:342
  96.8 1.9 %collective-permute-start = (bf16[15,1024]{1,0:T(8,128)(2,1)S(1)}, bf16[15,1024]{1,0:T(8,128)(2,1)S(1)}, u32[]{:S(2)}, u32[]{:S(2)}) collective-permute-start(bf16[15,1024]{1,0:T(8,128)(2,1)S(1)} %slice.52), channel_id=1, source_target_pairs={{0,1},{1,2},{2,3},{3,4},{4,5},{5,6},{6,7},{7,8},{8,9},{9,10},{10,1... | collective-permute-start | bytes 92168 | tf_op jit(solution)/shard_map/ppermute | solution.py:37
  101.2 4.0 %half_ffn.5 = bf16[192,2048]{1,0:T(8,128)(2,1)S(1)} custom-call(bf16[512,768]{1,0:T(8,128)(2,1)} %collective-permute-done.4.x_ref, bf16[2048,256]{1,0:T(8,128)(2,1)S(1)} %bitcast.40, bf16[2048,256]{1,0:T(8,128)(2,1)S(1)} %bitcast.45, bf16[2048,256]{1,0:T(8,128)(2,1)} %collective-permute-done.1.refs_2_, bf16[2048,256]{1,0:T(8,128)(2,1)} %collective-permute-done.2.refs_3_, ...), custom_call_target="tpu_custom_call" | custom-call | flops 3500000000 | bytes 7864320 | tf_op jit(solution)/shard_map/half_ffn/pallas_call | solution.py:259
  106.6 2.9 %half_ffn.4.a_ref = bf16[192,2048]{1,0:T(8,128)(2,1)S(1)} custom-call(bf16[512,768]{1,0:T(8,128)(2,1)S(1)} %bitcast.32, bf16[2048,256]{1,0:T(8,128)(2,1)S(1)} %bitcast.41, bf16[2048,256]{1,0:T(8,128)(2,1)S(1)} %bitcast.46, bf16[2048,256]{1,0:T(8,128)(2,1)} %collective-permute-done.1.refs_2_, bf16[2048,256]{1,0:T(8,128)(2,1)} %collective-permute-done.2.refs_3_, ...), custom_call_target="tpu_custom_call" | custom-call | flops 3500000000 | bytes 7864320 | tf_op jit(solution)/shard_map/half_ffn/pallas_call | solution.py:259
  109.5 6.9 %collective-permute-done.5.b_ref = bf16[192,2048]{1,0:T(8,128)(2,1)S(1)} collective-permute-done((bf16[192,2048]{1,0:T(8,128)(2,1)S(1)}, bf16[192,2048]{1,0:T(8,128)(2,1)S(1)}, u32[]{:S(2)}, u32[]{:S(2)}) %collective-permute-start.5) | collective-permute-done | bytes 786464 | tf_op jit(solution)/shard_map/ppermute | solution.py:47
  116.5 1.8 %pack_sum.2 = bf16[512,768]{1,0:T(8,128)(2,1)} custom-call(bf16[192,2048]{1,0:T(8,128)(2,1)S(1)} %half_ffn.4.a_ref, bf16[192,2048]{1,0:T(8,128)(2,1)S(1)} %collective-permute-done.5.b_ref), custom_call_target="tpu_custom_call" | custom-call | flops 800000000 | bytes 2359296 | tf_op jit(solution)/shard_map/pack_sum/pallas_call | solution.py:217
  119.8 13.9 %all-to-all-start.1 = ((bf16[64,8,768]{2,1,0:T(8,128)(2,1)}), bf16[64,8,768]{2,1,0:T(8,128)(2,1)S(1)}, u32[]{:S(2)}, u32[]{:S(2)}) async-start(bf16[64,8,768]{2,1,0:T(8,128)(2,1)} %bitcast.10), calls=%async_computation.1 | async-start | bytes 1572864 | tf_op jit(solution)/shard_map/all_to_all | solution.py:342
  133.7 10.5 %fusion.5 = f32[8,256,128]{1,2,0:T(8,128)S(1)} fusion(bf16[8,128,128]{2,1,0:T(8,128)(2,1)S(1)} %copy-done, f32[1024]{0:T(1024)S(1)} %select_select_fusion, f32[256]{0:T(256)S(1)} %convert_add_fusion, pred[1024]{0:T(1024)(128)(4,1)S(1)} %get-tuple-element.5, pred[1024]{0:T(1024)(128)(4,1)S(1)} %get-tuple-element.4, ...), kind=kOutput, calls=%fused_computation.23 | convolution fusion | flops 73138176 | bytes 18097152 | tf_op jit(solution)/shard_map/tgc,gcd->tgd/dot_general | solution.py:393
  144.5 2.2 %convolution_convert_fusion = bf16[256,2048]{1,0:T(8,128)(2,1)} fusion(bf16[256,1024]{0,1:T(8,128)(2,1)S(1)} %fusion.3, bf16[1024,2048]{1,0:T(8,128)(2,1)S(1)} %copy-done.12), kind=kOutput, calls=%fused_computation | convolution fusion | flops 1074266112 | bytes 5767168 | tf_op jit(solution)/shard_map/dot_general | solution.py:76
  148.5 8.1 %all-to-all-done.1 = bf16[64,8,768]{2,1,0:T(8,128)(2,1)S(1)} async-done(((bf16[64,8,768]{2,1,0:T(8,128)(2,1)}), bf16[64,8,768]{2,1,0:T(8,128)(2,1)S(1)}, u32[]{:S(2)}, u32[]{:S(2)}) %all-to-all-start.1) | async-done | bytes 786464 | tf_op jit(solution)/shard_map/all_to_all | solution.py:342
  156.6 2.6 %combine.3 = bf16[128,2048]{1,0:T(8,128)(2,1)} custom-call(s32[1]{0:T(128)} %bitcast.2.own_ref, bf16[512,768]{1,0:T(8,128)(2,1)S(1)} %bitcast.36, s32[2,512]{1,0:T(2,128)S(1)} %bitcast.55, f32[2,512]{1,0:T(2,128)S(1)} %bitcast.57, f32[128,2048]{1,0:T(8,128)S(1)} %combine.2.refs_0_), custom_call_target="tpu_custom_call" | custom-call | flops 1500000000 | bytes 2100000 | tf_op jit(solution)/shard_map/combine/pallas_call | solution.py:320
  (45 shorter events, 15.3 us)
Async XLA Ops:
  0.6 133.0 %copy-start = (bf16[8,128,128]{2,1,0:T(8,128)(2,1)S(1)}, bf16[8,128,128]{2,1,0:T(8,128)(2,1)}, u32[]{:S(2)}) copy-start(bf16[8,128,128]{2,1,0:T(8,128)(2,1)} %param.12) | copy-start | bytes 786436
  4.2 13.1 %copy-start.1 = (bf16[1,2048,256]{2,1,0:T(8,128)(2,1)S(1)}, bf16[1,2048,256]{2,1,0:T(8,128)(2,1)}, u32[]{:S(2)}) copy-start(bf16[1,2048,256]{2,1,0:T(8,128)(2,1)} %param.19) | copy-start | bytes 3145732
  4.2 36.1 %all-to-all-start.2 = ((bf16[64,8,768]{2,1,0:T(8,128)(2,1)}), bf16[64,8,768]{2,1,0:T(8,128)(2,1)S(1)}, u32[]{:S(2)}, u32[]{:S(2)}) async-start(bf16[64,8,768]{2,1,0:T(8,128)(2,1)} %bitcast.59), calls=%async_computation.2 | async-start | bytes 1572864 | tf_op jit(solution)/shard_map/all_to_all | solution.py:342
  17.4 30.3 %collective-permute-start.1 = (bf16[2048,256]{1,0:T(8,128)(2,1)S(1)}, bf16[2048,256]{1,0:T(8,128)(2,1)}, u32[]{:S(2)}, u32[]{:S(2)}) collective-permute-start(bf16[2048,256]{1,0:T(8,128)(2,1)S(1)} %bitcast.37), channel_id=1, source_target_pairs={{0,1},{1,0},{2,3},{3,2},{4,7},{5,6},{6,5},{7,4},{8,9},{9,8},{10,11... | collective-permute-start | bytes 3145736 | tf_op jit(solution)/shard_map/ppermute | solution.py:47
  20.2 27.5 %collective-permute-start.2 = (bf16[2048,256]{1,0:T(8,128)(2,1)}, bf16[2048,256]{1,0:T(8,128)(2,1)}, u32[]{:S(2)}, u32[]{:S(2)}) collective-permute-start(bf16[2048,256]{1,0:T(8,128)(2,1)} %bitcast.42), channel_id=1, source_target_pairs={{0,1},{1,0},{2,3},{3,2},{4,7},{5,6},{6,5},{7,4},{8,9},{9,8},{10,11... | collective-permute-start | bytes 3145736 | tf_op jit(solution)/shard_map/ppermute | solution.py:47
  20.3 38.8 %collective-permute-start.3 = (bf16[256,2048]{1,0:T(8,128)(2,1)}, bf16[256,2048]{1,0:T(8,128)(2,1)}, u32[]{:S(2)}, u32[]{:S(2)}) collective-permute-start(bf16[256,2048]{1,0:T(8,128)(2,1)} %bitcast.47), channel_id=1, source_target_pairs={{0,1},{1,0},{2,3},{3,2},{4,7},{5,6},{6,5},{7,4},{8,9},{9,8},{10,11... | collective-permute-start | bytes 3145736 | tf_op jit(solution)/shard_map/ppermute | solution.py:47
  40.3 30.5 %all-to-all-start = ((bf16[64,8,768]{2,1,0:T(8,128)(2,1)}), bf16[64,8,768]{2,1,0:T(8,128)(2,1)S(1)}, u32[]{:S(2)}, u32[]{:S(2)}) async-start(bf16[64,8,768]{2,1,0:T(8,128)(2,1)} %bitcast.58), calls=%async_computation | async-start | bytes 1572864 | tf_op jit(solution)/shard_map/all_to_all | solution.py:342
  46.3 16.9 %collective-permute-start.6 = (bf16[512,768]{1,0:T(8,128)(2,1)S(1)}, bf16[512,768]{1,0:T(8,128)(2,1)S(1)}, u32[]{:S(2)}, u32[]{:S(2)}) collective-permute-start(bf16[512,768]{1,0:T(8,128)(2,1)S(1)} %bitcast.34), channel_id=1, source_target_pairs={{0,3},{1,2},{2,1},{3,0},{4,5},{5,4},{6,7},{7,6},{8,11},{9,10},{10,... | collective-permute-start | bytes 2359304 | tf_op jit(solution)/shard_map/ppermute | solution.py:47
  63.2 1.2 copy-start.2
  64.4 1.2 copy-start.5
  69.5 11.5 %collective-permute-start.7 = (bf16[192,2048]{1,0:T(8,128)(2,1)}, bf16[192,2048]{1,0:T(8,128)(2,1)}, u32[]{:S(2)}, u32[]{:S(2)}) collective-permute-start(bf16[192,2048]{1,0:T(8,128)(2,1)} %half_ffn.7), channel_id=1, source_target_pairs={{0,3},{1,2},{2,1},{3,0},{4,5},{5,4},{6,7},{7,6},{8,11},{9,10},{10,... | collective-permute-start | bytes 2359304 | tf_op jit(solution)/shard_map/ppermute | solution.py:47
  70.8 27.9 %collective-permute-start.4 = (bf16[512,768]{1,0:T(8,128)(2,1)S(1)}, bf16[512,768]{1,0:T(8,128)(2,1)}, u32[]{:S(2)}, u32[]{:S(2)}) collective-permute-start(bf16[512,768]{1,0:T(8,128)(2,1)S(1)} %bitcast.31), channel_id=1, source_target_pairs={{0,3},{1,2},{2,1},{3,0},{4,5},{5,4},{6,7},{7,6},{8,11},{9,10},{10,... | collective-permute-start | bytes 2359304 | tf_op jit(solution)/shard_map/ppermute | solution.py:47
  71.0 1.2 copy-start.3
  72.2 1.2 copy-start.6
  83.9 12.9 %copy-start.10 = (bf16[256,1024]{1,0:T(8,128)(2,1)S(1)}, bf16[256,1024]{1,0:T(8,128)(2,1)}, u32[]{:S(2)}) copy-start(bf16[256,1024]{1,0:T(8,128)(2,1)} %param.11) | copy-start | bytes 1572868
  83.9 35.9 %all-to-all-start.3 = ((bf16[64,8,768]{2,1,0:T(8,128)(2,1)}), bf16[64,8,768]{2,1,0:T(8,128)(2,1)S(1)}, u32[]{:S(2)}, u32[]{:S(2)}) async-start(bf16[64,8,768]{2,1,0:T(8,128)(2,1)} %bitcast.15), calls=%async_computation.3 | async-start | bytes 1572864 | tf_op jit(solution)/shard_map/all_to_all | solution.py:342
  96.8 8.7 %collective-permute-start = (bf16[15,1024]{1,0:T(8,128)(2,1)S(1)}, bf16[15,1024]{1,0:T(8,128)(2,1)S(1)}, u32[]{:S(2)}, u32[]{:S(2)}) collective-permute-start(bf16[15,1024]{1,0:T(8,128)(2,1)S(1)} %slice.52), channel_id=1, source_target_pairs={{0,1},{1,2},{2,3},{3,4},{4,5},{5,6},{6,7},{7,8},{8,9},{9,10},{10,1... | collective-permute-start | bytes 92168 | tf_op jit(solution)/shard_map/ppermute | solution.py:37
  98.8 1.2 copy-start.4
  105.3 11.2 %collective-permute-start.5 = (bf16[192,2048]{1,0:T(8,128)(2,1)S(1)}, bf16[192,2048]{1,0:T(8,128)(2,1)S(1)}, u32[]{:S(2)}, u32[]{:S(2)}) collective-permute-start(bf16[192,2048]{1,0:T(8,128)(2,1)S(1)} %half_ffn.5), channel_id=1, source_target_pairs={{0,3},{1,2},{2,1},{3,0},{4,5},{5,4},{6,7},{7,6},{8,11},{9,10},{10,... | collective-permute-start | bytes 2359304 | tf_op jit(solution)/shard_map/ppermute | solution.py:47
  119.8 36.9 %all-to-all-start.1 = ((bf16[64,8,768]{2,1,0:T(8,128)(2,1)}), bf16[64,8,768]{2,1,0:T(8,128)(2,1)S(1)}, u32[]{:S(2)}, u32[]{:S(2)}) async-start(bf16[64,8,768]{2,1,0:T(8,128)(2,1)} %bitcast.10), calls=%async_computation.1 | async-start | bytes 1572864 | tf_op jit(solution)/shard_map/all_to_all | solution.py:342
  133.7 10.6 %copy-start.11 = (f32[1024]{0:T(1024)S(1)}, f32[1024]{0:T(1024)}, u32[]{:S(2)}) copy-start(f32[1024]{0:T(1024)} %param.13) | copy-start | bytes 12292
  133.7 10.8 %copy-start.12 = (bf16[1024,2048]{1,0:T(8,128)(2,1)S(1)}, bf16[1024,2048]{1,0:T(8,128)(2,1)}, u32[]{:S(2)}) copy-start(bf16[1024,2048]{1,0:T(8,128)(2,1)} %param.14) | copy-start | bytes 12582916
  144.5 2.3 %copy-start.8 = (s32[512,2]{0,1:T(2,128)S(1)}, s32[512,2]{0,1:T(2,128)}, u32[]{:S(2)}) copy-start(s32[512,2]{0,1:T(2,128)} %param.17) | copy-start | bytes 12292
  144.5 2.3 %copy-start.9 = (f32[512,2]{0,1:T(2,128)S(1)}, f32[512,2]{0,1:T(2,128)}, u32[]{:S(2)}) copy-start(f32[512,2]{0,1:T(2,128)} %param.18) | copy-start | bytes 12292
  (1 other events, 1.2 us)

commit v5 on v4

v5 whole, which is shorter than its diff:
```python
from functools import partial

import jax
import jax.numpy as jnp
from jax import lax
from jax.experimental import pallas as pl
from jax.experimental.pallas import tpu as pltpu
from jax.sharding import PartitionSpec as P


GDIM = 128
WMAX = 16
K = 2
EPS = 0.05

CHUNKS = 2
SLOTS = 3
SUB = 8
LANES = 768
PIECE = 256
FOLD = LANES // PIECE
MAIN = 2 * LANES
WIDTH = MAIN + 2 * PIECE
CORES = 2
EXPERTS_G = 32
GROUP = EXPERTS_G * SUB
DENSE = EXPERTS_G * SLOTS
SMALL = 16 * 1024 * 1024
LARGE = 52 * 1024 * 1024
BF16 = jnp.bfloat16
F32 = jnp.float32
VMEM = pl.BlockSpec(memory_space=pltpu.VMEM)
ANY = pl.BlockSpec(memory_space=pl.ANY)


def passed_along(array, axis, by):
    length = lax.axis_size(axis)
    pairs = [(i, i + by) for i in range(length) if 0 <= i + by < length]
    return lax.ppermute(array, axis, pairs)


def swapped(array, flip):
    eps, tps = lax.axis_size("ep"), lax.axis_size("tp")
    pairs = []
    for e in range(eps):
        for y in range(tps):
            other = y ^ 1 if (e + flip) % 2 == 0 else tps - 1 - y
            pairs.append((e * tps + y, e * tps + other))
    return lax.ppermute(array, ("ep", "tp"), pairs)


def window_sizes(width):
    group_of = jnp.arange(width) // GDIM
    level = group_of % 4
    return jnp.where(
        level == 0, 2.0, jnp.where(level == 1, 4.0, jnp.where(level == 2, 8.0, 16.0))
    ).astype(F32)


def pooled_rows(extended, positions):
    extent = extended.shape[0] - (WMAX - 1)
    window = window_sizes(extended.shape[1])
    running = jnp.zeros((extent, extended.shape[1]), F32)
    picked = running
    for offset in range(WMAX):
        running = running + extended[WMAX - 1 - offset : WMAX - 1 - offset + extent]
        if offset + 1 in (2, 4, 8, 16):
            picked = jnp.where(window[None, :] == offset + 1, running, picked)
    counted = jnp.minimum(positions[:, None] + 1.0, window[None, :])
    return (picked / counted - extended[WMAX - 1 :]).astype(BF16)


def as_bf16(mask):
    return mask.astype(F32).astype(BF16)


def dot(a, b):
    return jnp.dot(a, b, preferred_element_type=F32)


def slot_ranks(meta, core, rows, base):
    tokens = meta.shape[1]
    row = lax.broadcasted_iota(jnp.int32, (rows, tokens), 0)
    expert, sub = (row // SUB * CORES + core).astype(F32), row % SUB
    by_first, by_second = expert == meta[0:1, :], expert == meta[1:2, :]
    named = by_first | by_second
    before = lax.broadcasted_iota(jnp.int32, (tokens, tokens), 0) < lax.broadcasted_iota(
        jnp.int32, (tokens, tokens), 1
    )
    rank = dot(as_bf16(named), as_bf16(before)).astype(jnp.int32) - base
    return named, rank, sub


def main_place(sub, slot, half):
    return (sub == 2 * slot + half) & (sub < 2 * SLOTS) & (slot >= 0)


def tail_place(sub, slot, piece, c):
    return (sub >= 2 * SLOTS) & ((sub - 2 * SLOTS) * FOLD + c == 2 * slot + piece) & (slot >= 0)


def tail_used(piece, c):
    return any((r * FOLD + c - piece) % 2 == 0 for r in range(SUB - 2 * SLOTS))


def norm_kernel(place_ref, rows_ref, gain_ref, out_ref):
    del place_ref
    features = rows_ref[...].astype(F32)
    inverse = lax.rsqrt(jnp.mean(features * features, axis=-1, keepdims=True) + EPS)
    out_ref[...] = (features * inverse * gain_ref[...]).astype(BF16)


def normalized(expert_in, gain, place):
    tokens, width = expert_in.shape[0] // lax.axis_size("tp"), expert_in.shape[1]
    return pl.pallas_call(
        norm_kernel,
        out_shape=jax.ShapeDtypeStruct((tokens, width), BF16),
        grid_spec=pltpu.PrefetchScalarGridSpec(
            num_scalar_prefetch=1,
            grid=(1,),
            in_specs=[
                pl.BlockSpec((tokens, width), lambda i, place: (place[0], 0)),
                pl.BlockSpec((1, width), lambda i, place: (0, 0)),
            ],
            out_specs=pl.BlockSpec((tokens, width), lambda i, place: (0, 0)),
        ),
        cost_estimate=pl.CostEstimate(flops=1_000_000_000, bytes_accessed=1_100_000, transcendentals=128),
        name="normalized",
    )(place, expert_in, gain.reshape(1, width))


def send_kernel(base, place_ref, own_ref, twin_ref, own_meta_ref, twin_meta_ref, out_ref):
    for side, (normed, meta_ref) in enumerate(((own_ref, own_meta_ref), (twin_ref, twin_meta_ref))):
        named, rank, sub = slot_ranks(meta_ref[...], place_ref[1], out_ref.shape[0], base)
        mains = jnp.concatenate([as_bf16(named & main_place(sub, rank, h)) for h in range(2)], axis=1)
        for c in range(FOLD):
            used = [u for u in range(2) if tail_used(u, c)]
            tails = [as_bf16(named & tail_place(sub, rank, u, c)) for u in used]
            total = dot(
                mains,
                jnp.concatenate(
                    [normed[:, h * LANES + c * PIECE : h * LANES + (c + 1) * PIECE] for h in range(2)],
                    axis=0,
                ),
            ) + dot(
                jnp.concatenate(tails, axis=1),
                jnp.concatenate(
                    [normed[:, MAIN + u * PIECE : MAIN + (u + 1) * PIECE] for u in used], axis=0
                ),
            )
            out_ref[:, side * LANES + c * PIECE : side * LANES + (c + 1) * PIECE] = total.astype(BF16)


def send_rows(own, twin, own_meta, twin_meta, place, chips, chunk):
    tokens = own.shape[0]
    meta = pl.BlockSpec((2 * K, tokens), lambda i, place: (0, place[0]))
    return pl.pallas_call(
        partial(send_kernel, chunk * SLOTS),
        out_shape=jax.ShapeDtypeStruct((chips * SUB, CORES * LANES), BF16),
        grid_spec=pltpu.PrefetchScalarGridSpec(
            num_scalar_prefetch=1,
            grid=(1,),
            in_specs=[VMEM, VMEM, meta, meta],
            out_specs=VMEM,
        ),
        cost_estimate=pl.CostEstimate(flops=2_000_000_000, bytes_accessed=2_100_000, transcendentals=0),
        compiler_params=pltpu.CompilerParams(vmem_limit_bytes=SMALL),
        name="send_rows",
    )(place, own, twin, own_meta, twin_meta)


def places(shape, dense_axis, where):
    dense = lax.broadcasted_iota(jnp.int32, shape, dense_axis)
    row = lax.broadcasted_iota(jnp.int32, shape, 1 - dense_axis)
    return as_bf16((dense % EXPERTS_G == row // SUB) & where(row % SUB, dense // EXPERTS_G))


def main_maps(shape, dense_axis):
    return [places(shape, dense_axis, lambda sub, slot, h=h: main_place(sub, slot, h)) for h in range(2)]


def tail_maps(shape, dense_axis, c):
    return [
        places(shape, dense_axis, lambda sub, slot, u=u: tail_place(sub, slot, u, c))
        for u in range(2)
        if tail_used(u, c)
    ]


def dense_columns(c):
    starts = [h * LANES + c * PIECE for h in range(2)]
    return starts + [MAIN + u * PIECE for u in range(2) if tail_used(u, c)]


def unpack(x_ref, out_ref):
    mains = main_maps((DENSE, GROUP), 0)
    tails = {}

    def put(block, side, start):
        for k in range(SLOTS):
            to = (k * CORES + side) * EXPERTS_G
            out_ref[to : to + EXPERTS_G, start : start + PIECE] = block[
                k * EXPERTS_G : (k + 1) * EXPERTS_G
            ].astype(BF16)

    for c in range(FOLD):
        maps = jnp.concatenate(mains + tail_maps((DENSE, GROUP), 0, c), axis=0)
        for side in range(CORES):
            at = side * LANES + c * PIECE
            found = dot(maps, x_ref[:, at : at + PIECE])
            for n, start in enumerate(dense_columns(c)):
                block = found[n * DENSE : (n + 1) * DENSE]
                if start < MAIN:
                    put(block, side, start)
                else:
                    tails[start, side] = tails[start, side] + block if (start, side) in tails else block
    for (start, side), block in tails.items():
        put(block, side, start)


def pack_kernel(a_ref, b_ref, out_ref):
    mains = main_maps((GROUP, DENSE), 1)
    for c in range(FOLD):
        maps = jnp.concatenate(mains + tail_maps((GROUP, DENSE), 1, c), axis=1)
        for side in range(CORES):
            pieces = []
            for start in dense_columns(c):
                columns = slice(start, start + PIECE)
                for k in range(SLOTS):
                    to = (k * CORES + side) * EXPERTS_G
                    here = slice(to, to + EXPERTS_G)
                    pieces.append(
                        (a_ref[here, columns].astype(F32) + b_ref[here, columns].astype(F32)).astype(BF16)
                    )
            at = side * LANES + c * PIECE
            out_ref[:, at : at + PIECE] = dot(maps, jnp.concatenate(pieces, axis=0)).astype(BF16)


def pack_sum(a, b):
    return pl.pallas_call(
        pack_kernel,
        out_shape=jax.ShapeDtypeStruct((GROUP, CORES * LANES), BF16),
        in_specs=[VMEM] * 2,
        out_specs=VMEM,
        cost_estimate=pl.CostEstimate(flops=800_000_000, bytes_accessed=a.size * 6, transcendentals=0),
        compiler_params=pltpu.CompilerParams(vmem_limit_bytes=SMALL),
        name="pack_sum",
    )(a, b)


def ffn_kernel(*refs):
    sources, out_ref, dense_ref, held, sems = refs[:7], refs[7], refs[8], refs[9:16], refs[16]
    rows, *copies = [
        pltpu.make_async_copy(source, ref, sems.at[n])
        for n, (source, ref) in enumerate(zip(sources, held))
    ]
    rows.start()
    for copy in copies:
        copy.start()
    x_ref, ga_ref, ua_ref, gb_ref, ub_ref, da_ref, db_ref = held
    rows.wait()
    unpack(x_ref, dense_ref)
    x = dense_ref[...]
    copies[0].wait()
    copies[1].wait()
    hidden_a = (jax.nn.silu(dot(x, ga_ref[...])) * dot(x, ua_ref[...])).astype(BF16)
    copies[2].wait()
    copies[3].wait()
    hidden_b = (jax.nn.silu(dot(x, gb_ref[...])) * dot(x, ub_ref[...])).astype(BF16)
    copies[4].wait()
    copies[5].wait()
    step = 2 * PIECE
    for c in range(WIDTH // step):
        columns = slice(c * step, (c + 1) * step)
        out_ref[:, columns] = (
            dot(hidden_a, da_ref[:, columns]) + dot(hidden_b, db_ref[:, columns])
        ).astype(BF16)


def half_ffn(x, ga, gb, ua, ub, da, db):
    operands = (x, ga, ua, gb, ub, da, db)
    dense = x.size // WIDTH // SUB * SUB
    hidden = ga.shape[1] + gb.shape[1]
    return pl.pallas_call(
        ffn_kernel,
        out_shape=jax.ShapeDtypeStruct((dense, WIDTH), BF16),
        in_specs=[ANY] * 7,
        out_specs=VMEM,
        scratch_shapes=[pltpu.VMEM((dense, WIDTH), BF16)]
        + [pltpu.VMEM(operand.shape, BF16) for operand in operands]
        + [pltpu.SemaphoreType.DMA((7,))],
        cost_estimate=pl.CostEstimate(
            flops=3_500_000_000,
            bytes_accessed=x.size * 4 + 6 * ga.size * 2,
            transcendentals=dense * hidden,
        ),
        compiler_params=pltpu.CompilerParams(vmem_limit_bytes=LARGE),
        name="half_ffn",
    )(*operands)


def combine_kernel(base, last, place_ref, values_ref, own_meta_ref, twin_meta_ref, *refs):
    if last:
        sources, out_refs, before_refs, sems = refs[:2], refs[2:4], refs[4:6], refs[6]
        copies = [
            pltpu.make_async_copy(source, ref, sems.at[n])
            for n, (source, ref) in enumerate(zip(sources, before_refs))
        ]
        for copy in copies:
            copy.start()
    else:
        out_refs = refs
    rows = values_ref.shape[0]
    for side, meta_ref in enumerate((own_meta_ref, twin_meta_ref)):
        tokens = meta_ref.shape[1]
        meta = jnp.transpose(meta_ref[...])
        row = lax.broadcasted_iota(jnp.int32, (tokens, rows), 1)
        expert, sub = (row // SUB * CORES + place_ref[1]).astype(F32), row % SUB
        by_first, by_second = expert == meta[:, 0:1], expert == meta[:, 1:2]
        named = by_first | by_second
        earlier = lax.broadcasted_iota(jnp.int32, (tokens, tokens), 1) < lax.broadcasted_iota(
            jnp.int32, (tokens, tokens), 0
        )
        slot = dot(as_bf16(earlier), as_bf16(named)).astype(jnp.int32) - base
        weight = jnp.where(
            named & (slot < SLOTS), jnp.where(by_first, meta[:, 2:3], meta[:, 3:4]), 0.0
        )
        high = weight.astype(BF16).astype(F32)
        low = weight - high

        def split(chosen):
            return [jnp.where(chosen, part, 0.0).astype(BF16) for part in (high, low)]

        totals = {}
        mains = [part for h in range(2) for part in split(main_place(sub, slot, h))]
        for c in range(FOLD):
            maps = list(mains)
            for u in range(2):
                if tail_used(u, c):
                    maps += split(tail_place(sub, slot, u, c))
            at = side * LANES + c * PIECE
            found = dot(jnp.concatenate(maps, axis=0), values_ref[:, at : at + PIECE])
            for n, start in enumerate(dense_columns(c)):
                block = (
                    found[2 * n * tokens : (2 * n + 1) * tokens]
                    + found[(2 * n + 1) * tokens : (2 * n + 2) * tokens]
                )
                totals[start] = totals[start] + block if start in totals else block
        if last:
            copies[side].wait()
        for start, total in totals.items():
            columns = slice(start, start + PIECE)
            if last:
                total += before_refs[side][:, columns]
            out_refs[side][:, columns] = total.astype(out_refs[side].dtype)


def combine(chunk, values, own_meta, twin_meta, place, tokens, before):
    last = bool(before)
    meta = pl.BlockSpec((2 * K, tokens), lambda i, place: (0, place[0]))
    return pl.pallas_call(
        partial(combine_kernel, chunk * SLOTS, last),
        out_shape=[
            jax.ShapeDtypeStruct((tokens, WIDTH), F32),
            jax.ShapeDtypeStruct((tokens, WIDTH), BF16 if last else F32),
        ],
        grid_spec=pltpu.PrefetchScalarGridSpec(
            num_scalar_prefetch=1,
            grid=(1,),
            in_specs=[VMEM, meta, meta] + [ANY] * len(before),
            out_specs=[VMEM] * 2,
            scratch_shapes=[pltpu.VMEM((tokens, WIDTH), F32)] * 2 + [pltpu.SemaphoreType.DMA((2,))]
            if last
            else [],
        ),
        cost_estimate=pl.CostEstimate(flops=1_500_000_000, bytes_accessed=2_100_000, transcendentals=0),
        compiler_params=pltpu.CompilerParams(vmem_limit_bytes=LARGE),
        name="combine",
    )(place, values, own_meta, twin_meta, *before)


def exchanged(rows):
    chips = rows.shape[0] // SUB
    out = lax.all_to_all(
        rows.reshape(chips, SUB, CORES * LANES),
        "ep",
        split_axis=0,
        concat_axis=0,
        tiled=True,
        axis_index_groups=[[CORES * i + c for i in range(chips)] for c in range(CORES)],
    )
    return out.reshape(rows.shape)


def twin_of(array):
    return lax.ppermute(array, "ep", [(i, i ^ 1) for i in range(lax.axis_size("ep"))])


def on_device(
    pool_in,
    w_pool,
    pool_scale,
    w_out,
    expert_in,
    ffn_gain,
    routes,
    route_weight,
    w_gate,
    w_up,
    w_down,
):
    rows_here = pool_in.shape[0]
    tokens = routes.shape[0] // lax.axis_size("tp")
    chips = lax.axis_size("ep") * w_gate.shape[0] // CORES
    place = jnp.stack([lax.axis_index("tp"), lax.axis_index("ep") % CORES]).astype(jnp.int32)
    own_meta = jnp.concatenate([routes.T.astype(F32), route_weight.T], axis=0)
    twin_meta = twin_of(own_meta)
    own_rows = normalized(expert_in, ffn_gain, place)
    twin_rows = twin_of(own_rows)
    before = passed_along(pool_in[rows_here - (WMAX - 1) :], ("ep", "tp"), 1)

    gate, up, down = w_gate[0], w_up[0], w_down[0]
    gate_b = swapped(gate, 0)
    up_b, down_b = swapped(up, 0), swapped(down, 0)
    ffn = lambda x: half_ffn(x, gate, gate_b, up, up_b, down, down_b)

    mine = []
    for n in range(CHUNKS):
        sent = send_rows(own_rows, twin_rows, own_meta, twin_meta, place, chips, n)
        mine.append(exchanged(sent))
    summed = ()
    for n in range(CHUNKS):
        theirs = swapped(mine[n], 1)
        partial_sum = ffn(theirs)
        back = swapped(partial_sum, 1)
        kept = ffn(mine[n])
        results = pack_sum(kept, back)
        returned = exchanged(results)
        summed = combine(n, returned, own_meta, twin_meta, place, tokens, summed)
    other = twin_of(summed[1])
    expert_out = (summed[0] + other.astype(F32)).astype(BF16)

    extended = jnp.concatenate([before, pool_in], axis=0).astype(F32)
    positions = (
        lax.axis_index(("ep", "tp")) * rows_here + jnp.arange(rows_here)
    ).astype(F32)
    pooled = pooled_rows(extended, positions)
    group_count = w_pool.shape[0]
    grouped = jnp.einsum(
        "tgc,gcd->tgd",
        pooled.reshape(rows_here, group_count, GDIM),
        w_pool,
        preferred_element_type=F32,
    )
    scaled = (grouped.reshape(rows_here, -1) * pool_scale).astype(BF16)
    mixer_out = dot(scaled, w_out).astype(BF16)
    return (mixer_out, expert_out)


def solution(mesh):
    placed = (
        P(("ep", "tp"), None),
        P(),
        P(),
        P(),
        P("ep", None),
        P(),
        P("ep", None),
        P("ep", None),
        P("ep", None, "tp"),
        P("ep", None, "tp"),
        P("ep", "tp", None),
    )
    return jax.shard_map(
        on_device,
        mesh=mesh,
        in_specs=placed,
        out_specs=(P(("ep", "tp"), None), P(("ep", "tp"), None)),
        check_vma=False,
    )
```

time: 160 us -> 154 us (0.963)
  the two profiles are of different devices: /device:TPU:1 before, /device:TPU:17 now
where the time goes in v5:
time: 154 us
  waiting for transfers between devices  63.6 us (41%)
  starting transfers between devices  45.6 us (30%)
  Pallas kernels  34.4 us (22%)
  matrix products  5.33 us (3%)
  local copies, waits for them, and re-layouts  2.07 us (1%)
  other arithmetic  1.87 us (1%)
    all_to_all x4, waiting for transfers between devices, exchanged(): lax.all_to_all(rows.reshape(chips, SUB, CORES * LANES), 'ep', split_axis=...  33.4 us
    all_to_all x4, starting transfers between devices, exchanged(): lax.all_to_all(rows.reshape(chips, SUB, CORES * LANES), 'ep', split_axis=...  32.5 us
    ppermute x7, waiting for transfers between devices, swapped(): return lax.ppermute(array, ('ep', 'tp'), pairs)  28.5 us
    pallas_call x4, Pallas kernels, half_ffn(): pl.pallas_call(ffn_kernel, out_shape=jax.ShapeDtypeStruct((dense, WIDTH),...  14.1 us
    pallas_call x2, Pallas kernels, combine(): pl.pallas_call(partial(combine_kernel, chunk * SLOTS, last), out_shape=[j...  7.88 us
    ppermute x7, starting transfers between devices, swapped(): return lax.ppermute(array, ('ep', 'tp'), pairs)  5.45 us
    ppermute x3, starting transfers between devices, twin_of(): lax.ppermute(array, 'ep', [(i, i ^ 1) for i in range(lax.axis_size('ep'))])  5.19 us
    pallas_call x2, Pallas kernels, send_rows(): pl.pallas_call(partial(send_kernel, chunk * SLOTS), out_shape=jax.ShapeDt...  4.81 us
  transfers between devices with their start and end apart: 15, of which 8 were waited for; matrix products, arithmetic and copies ran while one was open for 4% of the time, Pallas kernels for 16%

profile of v5, /device:TPU:17, one launch (start us, length us, event | category | flops | bytes accessed | tf_op | source)
XLA Modules:
  0.0 153.7 jit_solution(11995617850544598291)
XLA Ops:
  1.2 2.9 %normalized.1.own_ref = bf16[128,2048]{1,0:T(8,128)(2,1)} custom-call(s32[2]{0:T(128)} %pad_add_fusion.place_ref, bf16[512,2048]{1,0:T(8,128)(2,1)} %rows_ref.1, f32[1,2048]{1,0:T(1,128)} %bitcast.40), custom_call_target="tpu_custom_call" | custom-call | flops 1000000000 | bytes 1100000 | tf_op jit(solution)/shard_map/normalized/pallas_call | solution.py:115
  7.6 2.4 %send_rows.3 = bf16[256,1536]{1,0:T(8,128)(2,1)} custom-call(s32[2]{0:T(128)S(1)} %copy-done.3, bf16[128,2048]{1,0:T(8,128)(2,1)S(1)} %copy-done.1, bf16[128,2048]{1,0:T(8,128)(2,1)S(1)} %collective-permute-done.1.twin_ref, f32[4,512]{1,0:T(4,128)S(1)} %pad_maximum_fusion.own_meta_ref, f32[4,512]{1,0:T(4,128)S(1)} %collective-permute-done.2.twin_meta_ref), custom_call_target="tpu_custom_call" | custom-call | flops 2000000000 | bytes 2100000 | tf_op jit(solution)/shard_map/send_rows/pallas_call | solution.py:157
  10.0 11.2 %all-to-all-start.2 = ((bf16[32,8,1536]{2,1,0:T(8,128)(2,1)}), bf16[32,8,1536]{2,1,0:T(8,128)(2,1)S(1)}, u32[]{:S(2)}, u32[]{:S(2)}) async-start(bf16[32,8,1536]{2,1,0:T(8,128)(2,1)} %bitcast.14), calls=%async_computation.2 | async-start | bytes 1572864 | tf_op jit(solution)/shard_map/all_to_all | solution.py:384
  22.9 2.4 %send_rows.2 = bf16[256,1536]{1,0:T(8,128)(2,1)} custom-call(s32[2]{0:T(128)S(1)} %copy-done.3, bf16[128,2048]{1,0:T(8,128)(2,1)S(1)} %copy-done.2, bf16[128,2048]{1,0:T(8,128)(2,1)S(1)} %collective-permute-done.1.twin_ref, f32[4,512]{1,0:T(4,128)S(1)} %pad_maximum_fusion.own_meta_ref, f32[4,512]{1,0:T(4,128)S(1)} %collective-permute-done.2.twin_meta_ref), custom_call_target="tpu_custom_call" | custom-call | flops 2000000000 | bytes 2100000 | tf_op jit(solution)/shard_map/send_rows/pallas_call | solution.py:157
  25.3 17.2 %all-to-all-done.2 = bf16[32,8,1536]{2,1,0:T(8,128)(2,1)S(1)} async-done(((bf16[32,8,1536]{2,1,0:T(8,128)(2,1)}), bf16[32,8,1536]{2,1,0:T(8,128)(2,1)S(1)}, u32[]{:S(2)}, u32[]{:S(2)}) %all-to-all-start.2) | async-done | bytes 786464 | tf_op jit(solution)/shard_map/all_to_all | solution.py:384
  42.5 5.8 %all-to-all-start = ((bf16[32,8,1536]{2,1,0:T(8,128)(2,1)}), bf16[32,8,1536]{2,1,0:T(8,128)(2,1)S(1)}, u32[]{:S(2)}, u32[]{:S(2)}) async-start(bf16[32,8,1536]{2,1,0:T(8,128)(2,1)} %bitcast.7), calls=%async_computation | async-start | bytes 1572864 | tf_op jit(solution)/shard_map/all_to_all | solution.py:384
  49.4 13.1 %collective-permute-done.5.refs_6_ = bf16[256,2048]{1,0:T(8,128)(2,1)} collective-permute-done((bf16[256,2048]{1,0:T(8,128)(2,1)}, bf16[256,2048]{1,0:T(8,128)(2,1)}, u32[]{:S(2)}, u32[]{:S(2)}) %collective-permute-start.5) | collective-permute-done | bytes 1048608 | tf_op jit(solution)/shard_map/ppermute | solution.py:49
  62.5 5.0 %collective-permute-done.8.refs_0_ = bf16[256,1536]{1,0:T(8,128)(2,1)S(1)} collective-permute-done((bf16[256,1536]{1,0:T(8,128)(2,1)S(1)}, bf16[256,1536]{1,0:T(8,128)(2,1)S(1)}, u32[]{:S(2)}, u32[]{:S(2)}) %collective-permute-start.8) | collective-permute-done | bytes 786464 | tf_op jit(solution)/shard_map/ppermute | solution.py:49
  67.4 3.5 %half_ffn.7 = bf16[192,2048]{1,0:T(8,128)(2,1)S(1)} custom-call(bf16[256,1536]{1,0:T(8,128)(2,1)S(1)} %collective-permute-done.8.refs_0_, bf16[2048,256]{1,0:T(8,128)(2,1)} %bitcast.9.refs_1_, bf16[2048,256]{1,0:T(8,128)(2,1)} %bitcast.10.refs_2_, bf16[2048,256]{1,0:T(8,128)(2,1)} %collective-permute-done.3.refs_3_, ...), custom_call_target="tpu_custom_call" | custom-call | flops 3500000000 | bytes 7864320 | tf_op jit(solution)/shard_map/half_ffn/pallas_call | solution.py:284
  72.5 3.5 %half_ffn.6.a_ref = bf16[192,2048]{1,0:T(8,128)(2,1)S(1)} custom-call(bf16[256,1536]{1,0:T(8,128)(2,1)S(1)} %bitcast.37, bf16[2048,256]{1,0:T(8,128)(2,1)} %bitcast.9.refs_1_, bf16[2048,256]{1,0:T(8,128)(2,1)} %bitcast.10.refs_2_, bf16[2048,256]{1,0:T(8,128)(2,1)} %collective-permute-done.3.refs_3_, bf16[2048,256]{1,0:T(8,128)(2,1)} %collective-permute-done.4.refs_4_, ...), custom_call_target="tpu_custom_call" | custom-call | flops 3500000000 | bytes 7864320 | tf_op jit(solution)/shard_map/half_ffn/pallas_call | solution.py:284
  76.0 6.3 %collective-permute-done.9.b_ref = bf16[192,2048]{1,0:T(8,128)(2,1)} collective-permute-done((bf16[192,2048]{1,0:T(8,128)(2,1)S(1)}, bf16[192,2048]{1,0:T(8,128)(2,1)}, u32[]{:S(2)}, u32[]{:S(2)}) %collective-permute-start.9) | collective-permute-done | bytes 786464 | tf_op jit(solution)/shard_map/ppermute | solution.py:49
  82.3 3.0 %pack_sum.3 = bf16[256,1536]{1,0:T(8,128)(2,1)} custom-call(bf16[192,2048]{1,0:T(8,128)(2,1)S(1)} %half_ffn.6.a_ref, bf16[192,2048]{1,0:T(8,128)(2,1)} %collective-permute-done.9.b_ref), custom_call_target="tpu_custom_call" | custom-call | flops 800000000 | bytes 2359296 | tf_op jit(solution)/shard_map/pack_sum/pallas_call | solution.py:240
  85.3 9.5 %all-to-all-start.3 = ((bf16[32,8,1536]{2,1,0:T(8,128)(2,1)}), bf16[32,8,1536]{2,1,0:T(8,128)(2,1)S(1)}, u32[]{:S(2)}, u32[]{:S(2)}) async-start(bf16[32,8,1536]{2,1,0:T(8,128)(2,1)} %bitcast.16), calls=%async_computation.3 | async-start | bytes 1572864 | tf_op jit(solution)/shard_map/all_to_all | solution.py:384
  94.8 3.5 %half_ffn.5 = bf16[192,2048]{1,0:T(8,128)(2,1)S(1)} custom-call(bf16[256,1536]{1,0:T(8,128)(2,1)S(1)} %collective-permute-done.6.refs_0_, bf16[2048,256]{1,0:T(8,128)(2,1)} %bitcast.9.refs_1_, bf16[2048,256]{1,0:T(8,128)(2,1)} %bitcast.10.refs_2_, bf16[2048,256]{1,0:T(8,128)(2,1)} %collective-permute-done.3.refs_3_, ...), custom_call_target="tpu_custom_call" | custom-call | flops 3500000000 | bytes 7864320 | tf_op jit(solution)/shard_map/half_ffn/pallas_call | solution.py:284
  99.5 2.4 %collective-permute-start = (bf16[15,1024]{1,0:T(8,128)(2,1)S(1)}, bf16[15,1024]{1,0:T(8,128)(2,1)S(1)}, u32[]{:S(2)}, u32[]{:S(2)}) collective-permute-start(bf16[15,1024]{1,0:T(8,128)(2,1)S(1)} %slice.52), channel_id=1, source_target_pairs={{0,1},{1,2},{2,3},{3,4},{4,5},{5,6},{6,7},{7,8},{8,9},{9,10},{10,1... | collective-permute-start | bytes 92168 | tf_op jit(solution)/shard_map/ppermute | solution.py:39
  101.9 3.5 %half_ffn.4.a_ref = bf16[192,2048]{1,0:T(8,128)(2,1)S(1)} custom-call(bf16[256,1536]{1,0:T(8,128)(2,1)S(1)} %bitcast.35, bf16[2048,256]{1,0:T(8,128)(2,1)} %bitcast.9.refs_1_, bf16[2048,256]{1,0:T(8,128)(2,1)} %bitcast.10.refs_2_, bf16[2048,256]{1,0:T(8,128)(2,1)} %collective-permute-done.3.refs_3_, bf16[2048,256]{1,0:T(8,128)(2,1)} %collective-permute-done.4.refs_4_, ...), custom_call_target="tpu_custom_call" | custom-call | flops 3500000000 | bytes 7864320 | tf_op jit(solution)/shard_map/half_ffn/pallas_call | solution.py:284
  105.4 4.2 %collective-permute-done.7.b_ref = bf16[192,2048]{1,0:T(8,128)(2,1)S(1)} collective-permute-done((bf16[192,2048]{1,0:T(8,128)(2,1)S(1)}, bf16[192,2048]{1,0:T(8,128)(2,1)S(1)}, u32[]{:S(2)}, u32[]{:S(2)}) %collective-permute-start.7) | collective-permute-done | bytes 786464 | tf_op jit(solution)/shard_map/ppermute | solution.py:49
  111.4 4.1 %all-to-all-done.3 = bf16[32,8,1536]{2,1,0:T(8,128)(2,1)S(1)} async-done(((bf16[32,8,1536]{2,1,0:T(8,128)(2,1)}), bf16[32,8,1536]{2,1,0:T(8,128)(2,1)S(1)}, u32[]{:S(2)}, u32[]{:S(2)}) %all-to-all-start.3) | async-done | bytes 786464 | tf_op jit(solution)/shard_map/all_to_all | solution.py:384
  115.5 6.0 %all-to-all-start.1 = ((bf16[32,8,1536]{2,1,0:T(8,128)(2,1)}), bf16[32,8,1536]{2,1,0:T(8,128)(2,1)S(1)}, u32[]{:S(2)}, u32[]{:S(2)}) async-start(bf16[32,8,1536]{2,1,0:T(8,128)(2,1)} %bitcast.12), calls=%async_computation.1 | async-start | bytes 1572864 | tf_op jit(solution)/shard_map/all_to_all | solution.py:384
  121.7 3.1 %fusion.5 = f32[8,256,128]{1,2,0:T(8,128)} fusion(bf16[8,128,128]{2,1,0:T(8,128)(2,1)S(1)} %copy-done, f32[1024]{0:T(1024)S(1)} %select_select_fusion, f32[256]{0:T(256)S(1)} %convert_add_fusion, pred[1024]{0:T(1024)(128)(4,1)S(1)} %get-tuple-element.13, pred[1024]{0:T(1024)(128)(4,1)S(1)} %get-tuple-element.12, pred[1024]{0:T(1024)(128)(4,1)S(1)} %get-tuple-element.11, ...), kind=kOutput, calls=%fused_computation.24 | convolution fusion | flops 73138176 | bytes 18097152 | tf_op jit(solution)/shard_map/tgc,gcd->tgd/dot_general | solution.py:449
  124.8 3.4 %combine.2 = (f32[128,2048]{1,0:T(8,128)S(1)}, f32[128,2048]{1,0:T(8,128)}) custom-call(s32[2]{0:T(128)S(1)} %copy-done.3, bf16[256,1536]{1,0:T(8,128)(2,1)S(1)} %bitcast.33, f32[4,512]{1,0:T(4,128)S(1)} %pad_maximum_fusion.own_meta_ref, f32[4,512]{1,0:T(4,128)S(1)} %collective-permute-done.2.twin_meta_ref), custom_call_target="tpu_custom_call" | custom-call | flops 1500000000 | bytes 2100000 | tf_op jit(solution)/shard_map/combine/pallas_call | solution.py:361
  129.2 12.2 %all-to-all-done.1 = bf16[32,8,1536]{2,1,0:T(8,128)(2,1)S(1)} async-done(((bf16[32,8,1536]{2,1,0:T(8,128)(2,1)}), bf16[32,8,1536]{2,1,0:T(8,128)(2,1)S(1)}, u32[]{:S(2)}, u32[]{:S(2)}) %all-to-all-start.1) | async-done | bytes 786464 | tf_op jit(solution)/shard_map/all_to_all | solution.py:384
  141.3 4.5 %combine.3 = (f32[128,2048]{1,0:T(8,128)}, bf16[128,2048]{1,0:T(8,128)(2,1)S(1)}) custom-call(s32[2]{0:T(128)S(1)} %copy-done.3, bf16[256,1536]{1,0:T(8,128)(2,1)S(1)} %bitcast.38, f32[4,512]{1,0:T(4,128)S(1)} %pad_maximum_fusion.own_meta_ref, f32[4,512]{1,0:T(4,128)S(1)} %collective-permute-done.2.twin_meta_ref, f32[128,2048]{1,0:T(8,128)} %copy-done.4, ...), custom_call_target="tpu_custom_call" | custom-call | flops 1500000000 | bytes 2100000 | tf_op jit(solution)/shard_map/combine/pallas_call | solution.py:361
  145.9 4.4 %collective-permute-start.10 = (bf16[128,2048]{1,0:T(8,128)(2,1)S(1)}, bf16[128,2048]{1,0:T(8,128)(2,1)S(1)}, u32[]{:S(2)}, u32[]{:S(2)}) collective-permute-start(bf16[128,2048]{1,0:T(8,128)(2,1)S(1)} %get-tuple-element.9), channel_id=1, source_target_pairs={{0,4},{4,0},{8,12},{12,8},{16,20},{20,16},{24,28},{28,24},{32,36},... | collective-permute-start | bytes 1572872 | tf_op jit(solution)/shard_map/ppermute | solution.py:396
  (54 shorter events, 15.9 us)
Async XLA Ops:
  0.6 121.1 %copy-start = (bf16[8,128,128]{2,1,0:T(8,128)(2,1)S(1)}, bf16[8,128,128]{2,1,0:T(8,128)(2,1)}, u32[]{:S(2)}) copy-start(bf16[8,128,128]{2,1,0:T(8,128)(2,1)} %param.12) | copy-start | bytes 786436
  1.2 3.6 %copy-start.9 = (s32[512,2]{0,1:T(2,128)S(1)}, s32[512,2]{0,1:T(2,128)}, u32[]{:S(2)}) copy-start(s32[512,2]{0,1:T(2,128)} %param.17) | copy-start | bytes 12292
  1.2 3.6 %copy-start.10 = (f32[512,2]{0,1:T(2,128)S(1)}, f32[512,2]{0,1:T(2,128)}, u32[]{:S(2)}) copy-start(f32[512,2]{0,1:T(2,128)} %param.18) | copy-start | bytes 12292
  1.2 5.3 %copy-start.3 = (s32[2]{0:T(128)S(1)}, s32[2]{0:T(128)}, u32[]{:S(2)}) copy-start(s32[2]{0:T(128)} %pad_add_fusion.place_ref) | copy-start | bytes 28
  4.1 2.4 %collective-permute-start.1 = (bf16[128,2048]{1,0:T(8,128)(2,1)}, bf16[128,2048]{1,0:T(8,128)(2,1)S(1)}, u32[]{:S(2)}, u32[]{:S(2)}) collective-permute-start(bf16[128,2048]{1,0:T(8,128)(2,1)} %normalized.1.own_ref), channel_id=1, source_target_pairs={{0,4},{4,0},{8,12},{12,8},{16,20},{20,16},{24,28},{28,24},{32,36},... | collective-permute-start | bytes 1572872 | tf_op jit(solution)/shard_map/ppermute | solution.py:396
  4.8 1.7 %collective-permute-start.2 = (f32[4,512]{1,0:T(4,128)S(1)}, f32[4,512]{1,0:T(4,128)S(1)}, u32[]{:S(2)}, u32[]{:S(2)}) collective-permute-start(f32[4,512]{1,0:T(4,128)S(1)} %pad_maximum_fusion.own_meta_ref), channel_id=1, source_target_pairs={{0,4},{4,0},{8,12},{12,8},{16,20},{20,16},{24,28},{28,24},{32,36},... | collective-permute-start | bytes 24584 | tf_op jit(solution)/shard_map/ppermute | solution.py:396
  10.0 12.9 %copy-start.2 = (bf16[128,2048]{1,0:T(8,128)(2,1)S(1)}, bf16[128,2048]{1,0:T(8,128)(2,1)}, u32[]{:S(2)}) copy-start(bf16[128,2048]{1,0:T(8,128)(2,1)} %normalized.1.own_ref) | copy-start | bytes 1572868
  10.0 32.5 %all-to-all-start.2 = ((bf16[32,8,1536]{2,1,0:T(8,128)(2,1)}), bf16[32,8,1536]{2,1,0:T(8,128)(2,1)S(1)}, u32[]{:S(2)}, u32[]{:S(2)}) async-start(bf16[32,8,1536]{2,1,0:T(8,128)(2,1)} %bitcast.14), calls=%async_computation.2 | async-start | bytes 1572864 | tf_op jit(solution)/shard_map/all_to_all | solution.py:384
  21.2 28.2 %collective-permute-start.3 = (bf16[2048,256]{1,0:T(8,128)(2,1)}, bf16[2048,256]{1,0:T(8,128)(2,1)}, u32[]{:S(2)}, u32[]{:S(2)}) collective-permute-start(bf16[2048,256]{1,0:T(8,128)(2,1)} %bitcast.9.refs_1_), channel_id=1, source_target_pairs={{0,1},{1,0},{2,3},{3,2},{4,7},{5,6},{6,5},{7,4},{8,9},{9,8},{10,11... | collective-permute-start | bytes 3145736 | tf_op jit(solution)/shard_map/ppermute | solution.py:49
  21.4 28.0 %collective-permute-start.4 = (bf16[2048,256]{1,0:T(8,128)(2,1)}, bf16[2048,256]{1,0:T(8,128)(2,1)}, u32[]{:S(2)}, u32[]{:S(2)}) collective-permute-start(bf16[2048,256]{1,0:T(8,128)(2,1)} %bitcast.10.refs_2_), channel_id=1, source_target_pairs={{0,1},{1,0},{2,3},{3,2},{4,7},{5,6},{6,5},{7,4},{8,9},{9,8},{10,11... | collective-permute-start | bytes 3145736 | tf_op jit(solution)/shard_map/ppermute | solution.py:49
  22.7 39.7 %collective-permute-start.5 = (bf16[256,2048]{1,0:T(8,128)(2,1)}, bf16[256,2048]{1,0:T(8,128)(2,1)}, u32[]{:S(2)}, u32[]{:S(2)}) collective-permute-start(bf16[256,2048]{1,0:T(8,128)(2,1)} %bitcast.11.refs_5_), channel_id=1, source_target_pairs={{0,1},{1,0},{2,3},{3,2},{4,7},{5,6},{6,5},{7,4},{8,9},{9,8},{10,11... | collective-permute-start | bytes 3145736 | tf_op jit(solution)/shard_map/ppermute | solution.py:49
  42.5 29.6 %all-to-all-start = ((bf16[32,8,1536]{2,1,0:T(8,128)(2,1)}), bf16[32,8,1536]{2,1,0:T(8,128)(2,1)S(1)}, u32[]{:S(2)}, u32[]{:S(2)}) async-start(bf16[32,8,1536]{2,1,0:T(8,128)(2,1)} %bitcast.7), calls=%async_computation | async-start | bytes 1572864 | tf_op jit(solution)/shard_map/all_to_all | solution.py:384
  48.3 19.1 %collective-permute-start.8 = (bf16[256,1536]{1,0:T(8,128)(2,1)S(1)}, bf16[256,1536]{1,0:T(8,128)(2,1)S(1)}, u32[]{:S(2)}, u32[]{:S(2)}) collective-permute-start(bf16[256,1536]{1,0:T(8,128)(2,1)S(1)} %bitcast.36), channel_id=1, source_target_pairs={{0,3},{1,2},{2,1},{3,0},{4,5},{5,4},{6,7},{7,6},{8,11},{9,10},{10,... | collective-permute-start | bytes 2359304 | tf_op jit(solution)/shard_map/ppermute | solution.py:49
  71.0 11.3 %collective-permute-start.9 = (bf16[192,2048]{1,0:T(8,128)(2,1)S(1)}, bf16[192,2048]{1,0:T(8,128)(2,1)}, u32[]{:S(2)}, u32[]{:S(2)}) collective-permute-start(bf16[192,2048]{1,0:T(8,128)(2,1)S(1)} %half_ffn.7), channel_id=1, source_target_pairs={{0,3},{1,2},{2,1},{3,0},{4,5},{5,4},{6,7},{7,6},{8,11},{9,10},{10,... | collective-permute-start | bytes 2359304 | tf_op jit(solution)/shard_map/ppermute | solution.py:49
  72.1 22.8 %collective-permute-start.6 = (bf16[256,1536]{1,0:T(8,128)(2,1)S(1)}, bf16[256,1536]{1,0:T(8,128)(2,1)S(1)}, u32[]{:S(2)}, u32[]{:S(2)}) collective-permute-start(bf16[256,1536]{1,0:T(8,128)(2,1)S(1)} %bitcast.34), channel_id=1, source_target_pairs={{0,3},{1,2},{2,1},{3,0},{4,5},{5,4},{6,7},{7,6},{8,11},{9,10},{10,... | collective-permute-start | bytes 2359304 | tf_op jit(solution)/shard_map/ppermute | solution.py:49
  85.3 30.2 %all-to-all-start.3 = ((bf16[32,8,1536]{2,1,0:T(8,128)(2,1)}), bf16[32,8,1536]{2,1,0:T(8,128)(2,1)S(1)}, u32[]{:S(2)}, u32[]{:S(2)}) async-start(bf16[32,8,1536]{2,1,0:T(8,128)(2,1)} %bitcast.16), calls=%async_computation.3 | async-start | bytes 1572864 | tf_op jit(solution)/shard_map/all_to_all | solution.py:384
  94.8 4.7 %copy-start.7 = (bf16[256,1024]{1,0:T(8,128)(2,1)S(1)}, bf16[256,1024]{1,0:T(8,128)(2,1)}, u32[]{:S(2)}) copy-start(bf16[256,1024]{1,0:T(8,128)(2,1)} %param.11) | copy-start | bytes 1572868
  98.4 11.2 %collective-permute-start.7 = (bf16[192,2048]{1,0:T(8,128)(2,1)S(1)}, bf16[192,2048]{1,0:T(8,128)(2,1)S(1)}, u32[]{:S(2)}, u32[]{:S(2)}) collective-permute-start(bf16[192,2048]{1,0:T(8,128)(2,1)S(1)} %half_ffn.5), channel_id=1, source_target_pairs={{0,3},{1,2},{2,1},{3,0},{4,5},{5,4},{6,7},{7,6},{8,11},{9,10},{10,... | collective-permute-start | bytes 2359304 | tf_op jit(solution)/shard_map/ppermute | solution.py:49
  99.5 22.1 %collective-permute-start = (bf16[15,1024]{1,0:T(8,128)(2,1)S(1)}, bf16[15,1024]{1,0:T(8,128)(2,1)S(1)}, u32[]{:S(2)}, u32[]{:S(2)}) collective-permute-start(bf16[15,1024]{1,0:T(8,128)(2,1)S(1)} %slice.52), channel_id=1, source_target_pairs={{0,1},{1,2},{2,3},{3,4},{4,5},{5,6},{6,7},{7,8},{8,9},{9,10},{10,1... | collective-permute-start | bytes 92168 | tf_op jit(solution)/shard_map/ppermute | solution.py:39
  115.5 25.8 %all-to-all-start.1 = ((bf16[32,8,1536]{2,1,0:T(8,128)(2,1)}), bf16[32,8,1536]{2,1,0:T(8,128)(2,1)S(1)}, u32[]{:S(2)}, u32[]{:S(2)}) async-start(bf16[32,8,1536]{2,1,0:T(8,128)(2,1)} %bitcast.12), calls=%async_computation.1 | async-start | bytes 1572864 | tf_op jit(solution)/shard_map/all_to_all | solution.py:384
  141.3 9.0 %copy-start.5 = (f32[8,256,128]{1,2,0:T(8,128)S(1)}, f32[8,256,128]{1,2,0:T(8,128)}, u32[]{:S(2)}) copy-start(f32[8,256,128]{1,2,0:T(8,128)} %fusion.5) | copy-start | bytes 3145732
  141.3 9.0 %copy-start.8 = (f32[1024]{0:T(1024)S(1)}, f32[1024]{0:T(1024)}, u32[]{:S(2)}) copy-start(f32[1024]{0:T(1024)} %param.13) | copy-start | bytes 12292
  141.3 9.2 %copy-start.11 = (bf16[1024,2048]{1,0:T(8,128)(2,1)S(1)}, bf16[1024,2048]{1,0:T(8,128)(2,1)}, u32[]{:S(2)}) copy-start(bf16[1024,2048]{1,0:T(8,128)(2,1)} %param.14) | copy-start | bytes 12582916
  145.9 6.9 %collective-permute-start.10 = (bf16[128,2048]{1,0:T(8,128)(2,1)S(1)}, bf16[128,2048]{1,0:T(8,128)(2,1)S(1)}, u32[]{:S(2)}, u32[]{:S(2)}) collective-permute-start(bf16[128,2048]{1,0:T(8,128)(2,1)S(1)} %get-tuple-element.9), channel_id=1, source_target_pairs={{0,4},{4,0},{8,12},{12,8},{16,20},{20,16},{24,28},{28,24},{32,36},... | collective-permute-start | bytes 1572872 | tf_op jit(solution)/shard_map/ppermute | solution.py:396
  (3 other events, 4.3 us)
